TPU v7x, 512 devices: a whole 4x4x16 slice. The times are simulated.
512 devices in a mesh: kv: 64 (over z, y), tp: 8 (over x, core).
Axes of the slice: x: 4, y: 4, z: 16, core: 2. Of those that a mesh axis runs over, the one named last changes fastest.
Arguments:
- tokens: bfloat16 [16384, 2048], P('kv'), may hold values from -40 to 40
- query_weight: bfloat16 [2048, 2048], P(None, 'tp'), may hold values from -0.125 to 0.125
- key_matrix: bfloat16 [2048, 1024], P(None, 'tp'), may hold values from -0.125 to 0.125
- value_matrix: bfloat16 [2048, 1024], P(None, 'tp'), may hold values from -0.125 to 0.125
- gate_weight: bfloat16 [2, 2048, 16], replicated, may hold values from -0.125 to 0.125
- key_pool_weight: float32 [16, 8], replicated, may hold values from -1.5 to 1.5
- value_pool_weight: float32 [16, 8], replicated, may hold values from -1.5 to 1.5
- out_weight: bfloat16 [2048, 2048], P('tp'), may hold values from -0.125 to 0.125
- chosen: int32 [256, 32], P('kv'), may hold values from 0 to 255, as said below
Outputs:
- mixed: bfloat16 [16384, 2048], P(('kv', 'tp'))
- log_sums: float32 [16384, 16], P('kv', 'tp')
Inputs may be any that keep to these rules, and one draw needn't show every extreme that they name: `chosen`: row i names only blocks <= i and names block i in its first column; a block may stand several times in a row and counts each time. The rows of one index of kv name, together, at most 2 distinct blocks held by any one other index, and exactly 2 of the index just before it whenever there is one.
All inputs are finite; a program needn't handle non-finite values.
Results may differ from a plain program's by a relative error of at most 0.018.
Values may be sent and summed in bfloat16 or wider, within the bound.
No kernel may reach another device: no remote copies, remote signals or barrier semaphores. Data moves between devices by JAX's collectives and lax.ppermute only.
A program may use at most 64 MiB of HBM per device.

v0:
```python
import jax
import jax.numpy as jnp
from jax import lax
from jax.sharding import Mesh
from jax.sharding import PartitionSpec as P

HEAD_SIZE = 128
BLOCK_LENGTH = 64
POOL_STRIDE = 16
PICKED_BLOCKS = 32
CAP = 2
KV = ("kv_0", "kv_1")
KV_TP = ("kv_0", "kv_1", "tp")


THETA = 10000.0
NEGATIVE = -1e30


def in_one_piece(arrays, axis, dim, along):
    ends, at = ([], 0)
    for a in arrays[:-1]:
        at += a.shape[along]
        ends.append(at)
    both = jnp.concatenate(arrays, axis=along)
    return tuple(jnp.split(lax.all_gather(both, axis, axis=dim, tiled=True), ends, axis=along))


def gather_axes(value, axes, dim):
    if not axes:
        return value
    nearer = lax.all_gather(value, axes[-1], axis=dim, tiled=True)
    return gather_axes(nearer, axes[:-1], dim)


def split_up(value, dim, count):
    before, after = (value.shape[:dim], value.shape[dim + 1 :])
    return jnp.moveaxis(value.reshape(*before, count, -1, *after), dim, 0)


def sum_at_owner(value, axis, dim):
    count = lax.axis_size(axis)
    pieces = lax.all_to_all(split_up(value, dim, count), axis, 0, 0, tiled=True)
    return jnp.sum(pieces.astype(jnp.float32), axis=0)


def apply_rotary(values_in, positions):
    half_width = values_in.shape[-1] // 2
    inverse = THETA ** (-jnp.arange(half_width, dtype=jnp.float32) / half_width)
    angles = positions.astype(jnp.float32)[:, None] * inverse[None, :]
    cosines = jnp.cos(angles)[:, None, :]
    sines = jnp.sin(angles)[:, None, :]
    front_half = values_in[..., :half_width]
    back_half = values_in[..., half_width:]
    return jnp.concatenate(
        [front_half * cosines - back_half * sines, back_half * cosines + front_half * sines],
        axis=-1,
    )


def shards(
    tokens,
    query_weight,
    key_matrix,
    value_matrix,
    gate_weight,
    key_pool_weight,
    value_pool_weight,
    out_weight,
    chosen,
):
    row_count = tokens.shape[0]
    kv_size = lax.axis_size(KV)
    own_index = lax.axis_index(KV)
    head_count = query_weight.shape[1] // HEAD_SIZE
    kv_heads = key_matrix.shape[1] // HEAD_SIZE
    group_count_heads = head_count // kv_heads
    start_point = own_index * row_count
    positions = start_point + jnp.arange(row_count, dtype=jnp.int32)
    query_proj = jnp.dot(tokens, query_weight, preferred_element_type=jnp.float32).reshape(
        row_count, head_count, HEAD_SIZE
    )
    key_projected = jnp.dot(tokens, key_matrix, preferred_element_type=jnp.float32).reshape(
        row_count, kv_heads, HEAD_SIZE
    )
    value_projected = jnp.dot(tokens, value_matrix, preferred_element_type=jnp.float32).reshape(
        row_count, kv_heads, HEAD_SIZE
    )
    query_states = apply_rotary(query_proj, positions).astype(jnp.bfloat16)
    key_states = apply_rotary(key_projected, positions).astype(jnp.bfloat16)
    value_states = value_projected.astype(jnp.bfloat16)
    head_start = lax.axis_index("tp") * head_count
    kv_start = lax.axis_index("tp") * kv_heads
    key_mix = lax.dynamic_slice_in_dim(key_pool_weight, kv_start, kv_heads, 1)
    value_mix = lax.dynamic_slice_in_dim(value_pool_weight, kv_start, kv_heads, 1)
    pooled_here = row_count // POOL_STRIDE
    block_ends = (
        start_point + POOL_STRIDE * jnp.arange(pooled_here, dtype=jnp.int32) + POOL_STRIDE - 1
    )
    compact_keys = apply_rotary(
        jnp.einsum(
            "cwyi,wy->cyi",
            key_projected.reshape(pooled_here, POOL_STRIDE, kv_heads, HEAD_SIZE),
            key_mix,
            precision=lax.Precision.HIGHEST,
        ),
        block_ends,
    ).astype(jnp.bfloat16)
    compact_values = jnp.einsum(
        "cwyi,wy->cyi",
        value_projected.reshape(pooled_here, POOL_STRIDE, kv_heads, HEAD_SIZE),
        value_mix,
        precision=lax.Precision.HIGHEST,
    ).astype(jnp.bfloat16)
    all_keys, all_values = in_one_piece((compact_keys, compact_values), KV, 0, 1)
    gate_cols = lax.dynamic_slice_in_dim(gate_weight, head_start, head_count, 2)
    gate_values = jax.nn.sigmoid(
        jnp.einsum("td,bdh->bth", tokens, gate_cols, preferred_element_type=jnp.float32)
    )
    score_scale = HEAD_SIZE ** (-0.5)
    grouped = query_states.reshape(row_count, kv_heads, group_count_heads, HEAD_SIZE)
    pooled_total = all_keys.shape[0]
    pooled_ends = POOL_STRIDE * jnp.arange(pooled_total, dtype=jnp.int32) + POOL_STRIDE - 1
    visible = (pooled_ends[None, :] <= positions[:, None]) | (
        jnp.arange(pooled_total)[None, :] == 0
    )
    scores = (
        jnp.einsum("qgjd,ngd->gjqn", grouped, all_keys, preferred_element_type=jnp.float32)
        * score_scale
    )
    masked = jnp.where(visible, scores, NEGATIVE)
    peak_value = jnp.max(masked, axis=-1, keepdims=True)
    exponent = jnp.where(visible, jnp.exp(masked - peak_value), 0.0)
    weights = (exponent / jnp.sum(exponent, axis=-1, keepdims=True)).astype(jnp.bfloat16)
    pooled_out = jnp.einsum(
        "gjqn,ngd->qgjd", weights, all_values, preferred_element_type=jnp.float32
    )
    row_width = kv_heads * 2 * HEAD_SIZE
    kv_rows = jnp.concatenate([key_states, value_states], axis=-1).reshape(row_count, row_width)
    per_dev = row_count // BLOCK_LENGTH
    block_total = kv_size * per_dev
    flattened = chosen.reshape(-1)
    block_ids = jnp.arange(block_total, dtype=jnp.int32)
    present = jnp.any(flattened[:, None] == block_ids[None, :], axis=0).reshape(kv_size, per_dev)
    ranking = jnp.cumsum(present.astype(jnp.int32), axis=1)
    slot_ids = jnp.arange(CAP, dtype=jnp.int32)
    wanted = present[:, :, None] & (ranking[:, :, None] == slot_ids[None, None, :] + 1)
    request = jnp.sum(
        jnp.where(wanted, jnp.arange(per_dev, dtype=jnp.int32)[None, :, None], 0), axis=1
    )
    local_blocks = kv_rows.reshape(per_dev, BLOCK_LENGTH, row_width)
    owners = chosen // per_dev
    within = chosen % per_dev
    slot_of = ranking.reshape(-1)[chosen] - 1
    pool_index = jnp.where(owners == own_index, within, per_dev + owners * CAP + slot_of)
    portion = gather_axes(kv_rows, KV, 0)
    owner_count = portion.shape[0] // row_count
    blocks = portion.reshape(owner_count, per_dev, BLOCK_LENGTH, row_width)
    taken = blocks[jnp.arange(owner_count, dtype=jnp.int32)[:, None], request]
    taken = taken.reshape(owner_count * CAP, BLOCK_LENGTH, row_width)
    pool_rows = jnp.concatenate([local_blocks, taken], axis=0)
    selected = pool_rows[pool_index]
    gathered = selected.reshape(per_dev, PICKED_BLOCKS * BLOCK_LENGTH, kv_heads, 2 * HEAD_SIZE)
    sel_keys = gathered[..., :HEAD_SIZE]
    sel_values = gathered[..., HEAD_SIZE:]
    block_queries = query_states.reshape(
        per_dev, BLOCK_LENGTH, kv_heads, group_count_heads, HEAD_SIZE
    )
    sel_scores = (
        jnp.einsum("bqgjd,bkgd->bgjqk", block_queries, sel_keys, preferred_element_type=jnp.float32)
        * score_scale
    )
    key_positions = (
        chosen[:, :, None] * BLOCK_LENGTH + jnp.arange(BLOCK_LENGTH, dtype=jnp.int32)[None, None, :]
    ).reshape(per_dev, PICKED_BLOCKS * BLOCK_LENGTH)
    query_positions = positions.reshape(per_dev, BLOCK_LENGTH)
    allowed = (key_positions[:, None, :] <= query_positions[:, :, None])[:, None, None]
    sel_masked = jnp.where(allowed, sel_scores, NEGATIVE)
    sel_peak = jnp.max(sel_masked, axis=-1, keepdims=True)
    sel_exp = jnp.where(allowed, jnp.exp(sel_masked - sel_peak), 0.0)
    sel_total = jnp.sum(sel_exp, axis=-1, keepdims=True)
    sel_weights = (sel_exp / sel_total).astype(jnp.bfloat16)
    sel_out = jnp.einsum(
        "bgjqk,bkgd->bqgjd", sel_weights, sel_values, preferred_element_type=jnp.float32
    )
    log_sums = jnp.transpose((sel_peak + jnp.log(sel_total))[..., 0], (0, 3, 1, 2)).reshape(
        row_count, head_count
    )
    attended = gate_values[0][:, :, None] * pooled_out.reshape(
        row_count, head_count, HEAD_SIZE
    ) + gate_values[1][:, :, None] * sel_out.reshape(row_count, head_count, HEAD_SIZE)
    attended = attended.astype(jnp.bfloat16).reshape(row_count, head_count * HEAD_SIZE)
    mixed = sum_at_owner(
        jnp.dot(attended, out_weight, preferred_element_type=jnp.float32).astype(jnp.bfloat16),
        "tp",
        0,
    ).astype(jnp.bfloat16)
    return (mixed, log_sums)


def solution(mesh):
    split = Mesh(mesh.devices.reshape(16, 4, mesh.shape["tp"]), ("kv_0", "kv_1", "tp"))
    placed = (
        P(KV, None),
        P(None, "tp"),
        P(None, "tp"),
        P(None, "tp"),
        P(),
        P(),
        P(),
        P("tp", None),
        P(KV, None),
    )
    return jax.shard_map(
        shards,
        mesh=split,
        in_specs=placed,
        out_specs=(P(KV_TP, None), P(KV, "tp")),
        check_vma=False,
    )
```

profile of v0, /device:TPU:1, one launch (start us, length us, event | category | flops | bytes accessed | tf_op | source)
XLA Modules:
  0.0 194.8 jit_solution(13167694768070338968)
XLA Ops:
  7.3 2.0 %fusion.66 = f32[256,128]{0,1:T(8,128)S(1)} fusion(bf16[256,2048]{1,0:T(8,128)(2,1)} %param.9, bf16[2048,128]{1,0:T(8,128)(2,1)} %param.11), kind=kOutput, calls=%fused_computation.121 | convolution fusion | flops 134217728 | bytes 1703936 | tf_op jit(solution)/shard_map/dot_general | solution.py:83
  9.3 0.3 fusion.32
  9.6 0.1 copy.66
  9.8 0.1 copy.67
  9.9 2.4 %fusion.65 = (bf16[256,128]{1,0:T(8,128)(2,1)S(1)}, f32[256,128]{1,0:T(8,128)}) fusion(bf16[256,2048]{1,0:T(8,128)(2,1)} %param.9, bf16[2048,128]{1,0:T(8,128)(2,1)} %param.12), kind=kOutput, calls=%fused_computation.120 | convolution fusion | flops 134250496 | bytes 1769472 | tf_op jit(solution)/shard_map/dot_general | solution.py:86
  12.4 12.6 %all-gather = bf16[1024,1,256]{2,0,1:T(8,128)(2,1)} all-gather(bf16[256,1,256]{2,0,1:T(8,128)(2,1)S(1)} %pad_maximum_fusion.1), channel_id=2, replica_groups=mesh['kv_0'=16,'kv_1'=4,'tp'=8] {'kv_1'}, dimensions={0}, use_global_device_ids=true | all-gather | bytes 655360 | tf_op jit(solution)/shard_map/all_gather | solution.py:32
  25.2 0.1 and.23
  25.4 0.6 copy.52
  25.9 0.2 reduce_window_sum.11
  26.2 0.1 reshape.482
  26.3 0.8 copy.41
  27.0 0.7 select_reduce_fusion
  27.8 0.1 reshape.490
  28.1 1.3 gather_fusion.1
  29.5 0.5 fusion.67
  30.1 0.1 copy.69
  30.2 0.1 copy.70
  30.7 1.1 fusion.54
  31.8 1.1 fusion.51
  33.0 0.1 fusion.41
  33.2 84.7 %all_gather.9 = bf16[1024,2,128]{2,0,1:T(8,128)(2,1)S(1)} all-gather(bf16[16,2,128]{2,0,1:T(8,128)(2,1)S(1)} %pad_maximum_fusion.3), channel_id=1, replica_groups=mesh['kv_0'=16,'kv_1'=4,'tp'=8] {'kv_0','kv_1'}, dimensions={0}, use_global_device_ids=true | all-gather | bytes 532480 | tf_op jit(solution)/shard_map/all_gather | solution.py:26
  117.9 1.2 multiply_cosine_fusion
  119.1 0.3 compare_or_fusion
  119.5 0.6 copy-done.4
  120.2 0.5 fusion.6
  120.7 0.6 fusion.7
  121.3 0.8 fusion.15
  122.1 0.1 copy.46
  122.2 1.3 fusion.14
  123.5 0.1 copy.40
  123.6 0.1 copy.47
  123.8 0.4 broadcast_compare_fusion
  124.2 18.7 %all-gather.4.cloned.1.call-done = bf16[16384,1,256]{2,0,1:T(8,128)(2,1)} async-done(((bf16[1024,1,256]{2,0,1:T(8,128)(2,1)}), bf16[16384,1,256]{2,0,1:T(8,128)(2,1)}) %all-gather.4.cloned.1.call-update) | async-done | bytes 8388624 | tf_op jit(solution)/shard_map/all_gather | solution.py:32
  142.9 6.2 %gather_fusion = bf16[128,64,256]{2,1,0:T(8,128)(2,1)} fusion(bf16[64,4,64,256]{3,2,1,0:T(8,128)(2,1)} %bitcast.158, s32[128]{0:T(128)S(1)} %reshape.490), kind=kCustom, calls=%fused_computation | custom fusion | bytes 8389632 | tf_op jit(solution)/shard_map/gather | solution.py:159
  149.1 3.9 %pad_maximum_fusion = bf16[132,64,256]{2,1,0:T(8,128)(2,1)} fusion(bf16[128,64,256]{2,1,0:T(8,128)(2,1)} %gather_fusion, bf16[4,64,128]{2,1,0:T(8,128)(2,1)S(1)} %bitcast.165, bf16[4,64,64]{2,1,0:T(8,128)(2,1)S(1)} %bitcast.167, bf16[4,64,64]{2,1,0:T(8,128)(2,1)S(1)} %bitcast.166), kind=kLoop, calls=%fused_computation.3 | loop fusion | flops 17301504 | bytes 8650752 | tf_op jit(solution)/shard_map/concatenate | solution.py:161
  153.0 5.1 %gather_fusion.2 = bf16[128,64,256]{2,1,0:T(8,128)(2,1)} fusion(bf16[132,64,256]{2,1,0:T(8,128)(2,1)} %pad_maximum_fusion, s32[1024]{0:T(1024)S(1)} %pad_clamp_fusion), kind=kCustom, calls=%fused_computation.2 | custom fusion | bytes 8389120 | tf_op jit(solution)/shard_map/gather | solution.py:162
  158.0 2.7 %fusion = (f32[4,2,64]{2,1,0:T(2,128)S(1)}, f32[4,2048,64,2]{1,2,3,0:T(8,128)S(1)}) fusion(pred[4,64,2048]{2,1,0:T(8,128)(4,1)S(1)} %broadcast_compare_fusion, bf16[4,2048,1,256]{3,1,0,2:T(8,128)(2,1)} %bitcast.156, bf16[4,64,2,64]{3,1,0,2:T(8,128)(2,1)S(1)} %bitcast.172, bf16[4,64,2,64]{3,1,0,2:T(8,128)(2,1)S(1)} %bitcast.171), kind=kOutput, calls=%fused_computation.7 | convolution fusion | flops 271842816 | bytes 6948864 | tf_op jit(solution)/shard_map/bqgjd,bkgd->bgjqk/dot_general | solution.py:170
  160.7 1.4 fusion.1
  162.2 0.7 copy-done.2
  162.9 1.9 fusion.8
  164.8 0.2 copy.57
  165.0 0.3 mul.201
  165.3 0.3 mul.229
  165.7 1.4 convolution_convert_fusion
  167.1 5.1 %all-to-all-start = ((bf16[8,32,2048]{2,1,0:T(8,128)(2,1)}), bf16[8,32,2048]{2,1,0:T(8,128)(2,1)S(1)}, u32[]{:S(2)}, u32[]{:S(2)}) async-start(bf16[8,32,2048]{2,1,0:T(8,128)(2,1)} %bitcast.50), calls=%async_computation | async-start | bytes 2097152 | tf_op jit(solution)/shard_map/all_to_all | solution.py:43
  172.2 0.7 reshape.489
  172.9 14.3 %all-to-all-done = bf16[8,32,2048]{2,1,0:T(8,128)(2,1)S(1)} async-done(((bf16[8,32,2048]{2,1,0:T(8,128)(2,1)}), bf16[8,32,2048]{2,1,0:T(8,128)(2,1)S(1)}, u32[]{:S(2)}, u32[]{:S(2)}) %all-to-all-start) | async-done | bytes 1048608 | tf_op jit(solution)/shard_map/all_to_all | solution.py:43
  187.2 0.8 reduce_sum.45
  (55 shorter events, 1.4 us)
Async XLA Ops:
  7.2 158.5 %copy-start = (bf16[256,2048]{1,0:T(8,128)(2,1)S(1)}, bf16[256,2048]{1,0:T(8,128)(2,1)}, u32[]{:S(2)}) copy-start(bf16[256,2048]{1,0:T(8,128)(2,1)} %param.16) | copy-start | bytes 3145732
  7.2 22.3 %copy-start.1 = (bf16[256,2048]{1,0:T(8,128)(2,1)S(1)}, bf16[256,2048]{1,0:T(8,128)(2,1)}, u32[]{:S(2)}) copy-start(bf16[256,2048]{1,0:T(8,128)(2,1)} %param.9) | copy-start | bytes 3145732
  7.2 17.8 %copy-start.8 = (s32[4,32]{1,0:T(4,128)S(1)}, s32[4,32]{1,0:T(4,128)}, u32[]{:S(2)}) copy-start(s32[4,32]{1,0:T(4,128)} %param.17) | copy-start | bytes 1540
  7.2 22.3 %copy-start.3 = (bf16[2048,256]{1,0:T(8,128)(2,1)S(1)}, bf16[2048,256]{1,0:T(8,128)(2,1)}, u32[]{:S(2)}) copy-start(bf16[2048,256]{1,0:T(8,128)(2,1)} %param.10) | copy-start | bytes 3145732
  7.2 135.7 %all-gather.4.cloned.1.call-start = ((), (), s32[]{:S(2)}) async-start(), calls=%async_computation.1 | async-start | bytes 8912896 | tf_op jit(solution)/shard_map/all_gather | solution.py:32
  7.3 2.3 %copy-start.9 = (f32[256]{0:T(256)}, f32[256]{0:T(256)S(1)}, u32[]{:S(2)}) copy-start(f32[256]{0:T(256)S(1)} %fusion.56) | copy-start | bytes 3076
  119.5 0.7 copy-start.4
  119.5 1.2 copy-start.6
  153.0 5.1 %copy-start.5 = (bf16[256,2,64]{2,0,1:T(8,128)(2,1)S(1)}, bf16[256,2,64]{2,0,1:T(8,128)(2,1)}, u32[]{:S(2)}) copy-start(bf16[256,2,64]{2,0,1:T(8,128)(2,1)} %copy-done.4) | copy-start | bytes 196612
  153.0 5.1 %copy-start.7 = (bf16[256,2,64]{2,0,1:T(8,128)(2,1)S(1)}, bf16[256,2,64]{2,0,1:T(8,128)(2,1)}, u32[]{:S(2)}) copy-start(bf16[256,2,64]{2,0,1:T(8,128)(2,1)} %copy-done.6) | copy-start | bytes 196612
  160.7 2.2 %copy-start.2 = (bf16[128,64,256]{2,1,0:T(8,128)(2,1)S(1)}, bf16[128,64,256]{2,1,0:T(8,128)(2,1)}, u32[]{:S(2)}) copy-start(bf16[128,64,256]{2,1,0:T(8,128)(2,1)} %gather_fusion.2) | copy-start | bytes 12582916
  167.1 20.1 %all-to-all-start = ((bf16[8,32,2048]{2,1,0:T(8,128)(2,1)}), bf16[8,32,2048]{2,1,0:T(8,128)(2,1)S(1)}, u32[]{:S(2)}, u32[]{:S(2)}) async-start(bf16[8,32,2048]{2,1,0:T(8,128)(2,1)} %bitcast.50), calls=%async_computation | async-start | bytes 2097152 | tf_op jit(solution)/shard_map/all_to_all | solution.py:43
Sparse Core Ops, SparseCore 0:
  25.1 117.6 all-gather.3
where the time goes:
time: 195 us
  blocking collectives  97.3 us (50%)
  waiting for transfers between devices  33 us (17%)
  local copies, waits for them, and re-layouts  18.8 us (10%)
  matrix products  15.8 us (8%)
  between operations  14.5 us (7%)
  other arithmetic  10.4 us (5%)
  starting transfers between devices  5.13 us (3%)
    all_gather x1, blocking collectives, in_one_piece(): lax.all_gather(both, axis, axis=dim, tiled=True)  84.7 us
    all_gather x1, waiting for transfers between devices, gather_axes(): nearer = lax.all_gather(value, axes[-1], axis=dim, tiled=True)  18.7 us
    all_to_all x1, waiting for transfers between devices, sum_at_owner(): pieces = lax.all_to_all(split_up(value, dim, count), axis, 0, 0, tiled=True)  14.3 us
    all_gather x1, blocking collectives, gather_axes(): nearer = lax.all_gather(value, axes[-1], axis=dim, tiled=True)  12.6 us
    gather x1, local copies, waits for them, and re-layouts, shards(): taken = blocks[jnp.arange(owner_count, dtype=jnp.int32)[:, None], request]  6.2 us
    all_to_all x1, starting transfers between devices, sum_at_owner(): pieces = lax.all_to_all(split_up(value, dim, count), axis, 0, 0, tiled=True)  5.09 us
    gather x1, local copies, waits for them, and re-layouts, shards(): selected = pool_rows[pool_index]  5.06 us
  transfers between devices with their start and end apart: 2, of which 2 were waited for; matrix products, arithmetic and copies ran while one was open for 7% of the time, Pallas kernels for 0%

commit v1 on v0

v1 whole, which is shorter than its diff:
```python
import jax
import jax.numpy as jnp
import numpy as np
from jax import lax
from jax.experimental import pallas as pl
from jax.experimental.pallas import tpu as pltpu
from jax.sharding import Mesh
from jax.sharding import PartitionSpec as P

HEAD_SIZE = 128
BLOCK = 64
POOL_STRIDE = 16
THETA = 10000.0
NEGATIVE = -1e30
FLOOR = -1e29
KV = ("z", "y")
SPAN = 256
STATS = 16
PER_STEP = 8
SCALE = HEAD_SIZE**-0.5


def rotary_tables(start, offsets):
    half = HEAD_SIZE // 2
    inverse = THETA ** (-np.arange(half, dtype=np.float64) / half)
    local = np.asarray(offsets, np.float64)[:, None] * inverse[None, :]
    cos_l = jnp.asarray(np.cos(local), jnp.float32)
    sin_l = jnp.asarray(np.sin(local), jnp.float32)
    starts = np.arange(64, dtype=np.float64)[:, None] * SPAN * inverse[None, :]
    cos_s = lax.dynamic_slice_in_dim(jnp.asarray(np.cos(starts), jnp.float32), start, 1, 0)
    sin_s = lax.dynamic_slice_in_dim(jnp.asarray(np.sin(starts), jnp.float32), start, 1, 0)
    return cos_l * cos_s - sin_l * sin_s, sin_l * cos_s + cos_l * sin_s


def rotate(value, cosines, sines):
    half = HEAD_SIZE // 2
    front, back = value[..., :half], value[..., half:]
    return jnp.concatenate([front * cosines - back * sines, back * cosines + front * sines], -1)


def chosen_kernel(meta_ref, ids_ref, q_ref, kv_ref, out_ref, acc_ref, m_ref, l_ref, lse_ref):
    z = meta_ref[0]
    y = meta_ref[1]
    row = lax.broadcasted_iota(jnp.int32, (BLOCK, HEAD_SIZE), 0)
    lane = lax.broadcasted_iota(jnp.int32, (1, HEAD_SIZE), 1)
    lane = jnp.where(lane >= BLOCK, lane - BLOCK, lane)

    for peer in range(4):
        for qb in range(4):
            acc_ref[qb] = jnp.zeros((HEAD_SIZE, HEAD_SIZE), jnp.float32)
            m_ref[qb] = jnp.full((1, HEAD_SIZE), FLOOR, jnp.float32)
            l_ref[qb] = jnp.zeros((1, HEAD_SIZE), jnp.float32)

        def group(k, carry, peer=peer):
            for qb in range(4):
                g = peer * 4 + qb
                qpos = (z * 4 + peer) * SPAN + qb * BLOCK + lane
                keys, values, bases = [], [], []
                for e in range(PER_STEP):
                    idx = ids_ref[g * 32 + k * PER_STEP + e]
                    none = idx < 0
                    safe = jnp.where(none, 0, idx)
                    at = pl.multiple_of(safe * BLOCK, BLOCK)
                    keys.append(kv_ref[pl.ds(at, BLOCK), :HEAD_SIZE])
                    values.append(kv_ref[pl.ds(at, BLOCK), HEAD_SIZE:])
                    base = ((safe // 4) * 4 + y) * SPAN + (safe % 4) * BLOCK
                    bases.append(jnp.where(none, 1 << 30, base))
                kg = jnp.concatenate(keys, 0)
                vg = jnp.concatenate(values, 0)
                q = q_ref[g * 128 : (g + 1) * 128, :]
                s = lax.dot_general(
                    kg, q, (((1,), (1,)), ((), ())), preferred_element_type=jnp.float32
                )
                slabs = []
                for e in range(PER_STEP):
                    slab = s[e * BLOCK : (e + 1) * BLOCK] * SCALE
                    seen = row <= (qpos - bases[e])
                    slabs.append(jnp.where(seen, slab, NEGATIVE))
                s = jnp.concatenate(slabs, 0)
                m_old = m_ref[qb]
                m_new = jnp.maximum(m_old, jnp.max(s, axis=0, keepdims=True))
                alpha = jnp.exp(m_old - m_new)
                p = jnp.exp(s - m_new)
                l_ref[qb] = l_ref[qb] * alpha + jnp.sum(p, axis=0, keepdims=True)
                m_ref[qb] = m_new
                pv = lax.dot_general(
                    vg,
                    p.astype(jnp.bfloat16),
                    (((0,), (0,)), ((), ())),
                    preferred_element_type=jnp.float32,
                )
                acc_ref[qb] = acc_ref[qb] * alpha + pv
            return carry

        count = meta_ref[2 + peer]
        lax.fori_loop(0, count, group, 0)
        for qb in range(4):
            total = l_ref[qb]
            some = total > 0.0
            safe_total = jnp.where(some, total, 1.0)
            normal = acc_ref[qb] / safe_total
            out = jnp.transpose(normal).astype(jnp.bfloat16)
            for half in range(2):
                for head in range(2):
                    out_ref[
                        peer * 2 + half,
                        qb * 32 : (qb + 1) * 32,
                        head * HEAD_SIZE : (head + 1) * HEAD_SIZE,
                    ] = out[head * BLOCK + half * 32 : head * BLOCK + half * 32 + 32]
            lse_ref[peer * 4 + qb : peer * 4 + qb + 1, :] = jnp.where(
                some, m_ref[qb] + jnp.log(safe_total), FLOOR
            )

    for peer in range(4):
        lse = lse_ref[peer * 4 : peer * 4 + 4, :]
        wide = jnp.concatenate(
            [
                jnp.concatenate([lse[0:1], lse[1:2]], 1),
                jnp.concatenate([lse[2:3], lse[3:4]], 1),
            ],
            0,
        )
        high = wide.astype(jnp.bfloat16).astype(jnp.float32)
        rest = wide - high
        middle = rest.astype(jnp.bfloat16).astype(jnp.float32)
        low = rest - middle
        block = jnp.concatenate(
            [high, middle, low, jnp.zeros((STATS - 6, 2 * HEAD_SIZE), jnp.float32)], 0
        ).astype(jnp.bfloat16)
        for half in range(2):
            out_ref[peer * 2 + half, 128 : 128 + STATS, :] = block


def chosen_attention(meta, ids, queries, kv_rows):
    whole = lambda shape: pl.BlockSpec(shape, lambda i, *_: (0,) * len(shape))
    return pl.pallas_call(
        chosen_kernel,
        grid_spec=pltpu.PrefetchScalarGridSpec(
            num_scalar_prefetch=2,
            grid=(1,),
            in_specs=[whole((2048, HEAD_SIZE)), whole((4096, 2 * HEAD_SIZE))],
            out_specs=whole((8, 128 + STATS, 2 * HEAD_SIZE)),
            scratch_shapes=[
                pltpu.VMEM((4, HEAD_SIZE, HEAD_SIZE), jnp.float32),
                pltpu.VMEM((4, 1, HEAD_SIZE), jnp.float32),
                pltpu.VMEM((4, 1, HEAD_SIZE), jnp.float32),
                pltpu.VMEM((16, HEAD_SIZE), jnp.float32),
            ],
        ),
        out_shape=jax.ShapeDtypeStruct((8, 128 + STATS, 2 * HEAD_SIZE), jnp.bfloat16),
        name="chosen_attention",
    )(meta, ids, queries, kv_rows)


def shards(
    tokens,
    query_weight,
    key_matrix,
    value_matrix,
    gate_weight,
    key_pool_weight,
    value_pool_weight,
    out_weight,
    chosen,
):
    z, y = lax.axis_index("z"), lax.axis_index("y")
    x, c = lax.axis_index("x"), lax.axis_index("c")
    own = z * 4 + y
    start = own * SPAN
    group = x * 2 + c
    f32, bf16 = jnp.float32, jnp.bfloat16

    cosines, sines = rotary_tables(own, np.arange(SPAN))
    key_projected = jnp.dot(tokens, key_matrix, preferred_element_type=f32)
    value_projected = jnp.dot(tokens, value_matrix, preferred_element_type=f32)
    keys = rotate(key_projected, cosines, sines).astype(bf16)
    kv_rows = jnp.concatenate([keys, value_projected.astype(bf16)], -1)
    all_kv = lax.all_gather(kv_rows, "z", axis=0, tiled=True)

    other_weight = lax.ppermute(out_weight, "c", [(0, 1), (1, 0)])

    query_proj = jnp.dot(tokens, query_weight, preferred_element_type=f32)
    query_proj = query_proj.reshape(SPAN, 2, HEAD_SIZE)
    queries = rotate(query_proj, cosines[:, None, :], sines[:, None, :]).astype(bf16)
    by_block = queries.reshape(4, BLOCK, 2, HEAD_SIZE).transpose(0, 2, 1, 3)
    picks = jnp.pad(chosen.astype(bf16).reshape(1, 128), ((0, 15), (0, 0)))
    sent = jnp.concatenate([by_block.reshape(512, HEAD_SIZE), picks], 0)
    near = lax.all_gather(sent, "y", axis=0, tiled=False)
    near_queries = near[:, :512].reshape(2048, HEAD_SIZE)
    near_chosen = near[:, 512].reshape(16, 32).astype(jnp.int32)

    mine = ((near_chosen // 4) % 4 == y).astype(jnp.int32)
    local = (near_chosen // 16) * 4 + near_chosen % 4
    before = (np.arange(32)[:, None] < np.arange(32)[None, :]).astype(np.int32)
    rank = jnp.sum(mine[:, :, None] * before[None], axis=1)
    place = (rank[:, :, None] == np.arange(32)[None, None, :]).astype(jnp.int32)
    ids = jnp.sum(mine[:, :, None] * place * (local[:, :, None] + 1), axis=1) - 1
    steps = (jnp.max(jnp.sum(mine, axis=1).reshape(4, 4), axis=1) + PER_STEP - 1) // PER_STEP
    meta = jnp.concatenate([jnp.stack([z, y]).astype(jnp.int32), steps.astype(jnp.int32)])

    key_mix = lax.dynamic_slice_in_dim(key_pool_weight, group, 1, 1)
    value_mix = lax.dynamic_slice_in_dim(value_pool_weight, group, 1, 1)
    pooled_here = SPAN // POOL_STRIDE
    pooled_k = jnp.sum(
        key_projected.reshape(pooled_here, POOL_STRIDE, HEAD_SIZE) * key_mix[None], axis=1
    )
    pooled_v = jnp.sum(
        value_projected.reshape(pooled_here, POOL_STRIDE, HEAD_SIZE) * value_mix[None], axis=1
    )
    ends = np.arange(pooled_here) * POOL_STRIDE + POOL_STRIDE - 1
    pooled_k = rotate(pooled_k, cosines[POOL_STRIDE - 1 :: POOL_STRIDE], sines[POOL_STRIDE - 1 :: POOL_STRIDE])
    pooled = jnp.concatenate([pooled_k.astype(bf16), pooled_v.astype(bf16)], -1)
    pooled = lax.all_gather(pooled, "y", axis=0, tiled=True)
    pooled = lax.all_gather(pooled, "z", axis=0, tiled=True)
    all_keys, all_values = pooled[:, :HEAD_SIZE], pooled[:, HEAD_SIZE:]

    positions = start + jnp.arange(SPAN, dtype=jnp.int32)
    pooled_total = all_keys.shape[0]
    pooled_ends = POOL_STRIDE * jnp.arange(pooled_total, dtype=jnp.int32) + POOL_STRIDE - 1
    visible = (pooled_ends[None, :] <= positions[:, None]) | (
        jnp.arange(pooled_total)[None, :] == 0
    )
    scores = jnp.einsum("qjd,nd->jqn", queries, all_keys, preferred_element_type=f32) * SCALE
    masked = jnp.where(visible, scores, NEGATIVE)
    peak = jnp.max(masked, axis=-1, keepdims=True)
    exponent = jnp.where(visible, jnp.exp(masked - peak), 0.0)
    weights = (exponent / jnp.sum(exponent, axis=-1, keepdims=True)).astype(bf16)
    pooled_out = jnp.einsum("jqn,nd->qjd", weights, all_values, preferred_element_type=f32)
    pooled_out = pooled_out.reshape(4, 2, 32, 2 * HEAD_SIZE)
    pooled_own = lax.dynamic_index_in_dim(pooled_out, c, 1, keepdims=False)
    pooled_send = lax.dynamic_index_in_dim(pooled_out, 1 - c, 1, keepdims=False)
    pooled_got = lax.ppermute(pooled_send, "c", [(0, 1), (1, 0)])

    own_tokens = lax.dynamic_index_in_dim(
        tokens.reshape(4, 2, 32, -1), c, 1, keepdims=False
    ).reshape(128, -1)
    gate_cols = lax.dynamic_slice_in_dim(gate_weight, x * 4, 4, 2)
    gates = jax.nn.sigmoid(
        jnp.einsum("td,bdh->bth", own_tokens, gate_cols, preferred_element_type=f32)
    )
    gates = gates.reshape(2, 128, 2, 2)

    partial = chosen_attention(meta, ids.reshape(-1), near_queries, all_kv)
    got = lax.all_to_all(partial, ("y", "c"), 0, 0, tiled=True)
    got = got.reshape(4, 2, 128 + STATS, 2 * HEAD_SIZE)
    stats = got[:, :, 128:134].astype(f32)
    lse = stats[:, :, 0:2] + stats[:, :, 2:4] + stats[:, :, 4:6]
    lse = lse.reshape(4, 2, 4, 2, BLOCK)
    top = jnp.max(lse, axis=0)
    parts = jnp.exp(lse - top[None])
    sums = jnp.sum(parts, axis=0)
    log_all = top + jnp.log(sums)
    log_own = lax.dynamic_index_in_dim(log_all, c, 0, keepdims=False)
    log_sums = log_own.transpose(0, 2, 1).reshape(SPAN, 2)
    share = parts / sums[None]
    share = lax.dynamic_index_in_dim(
        share.reshape(4, 2, 4, 2, 2, 32), c, 4, keepdims=False
    )
    share = share.transpose(0, 1, 2, 4, 3).reshape(4, 2, 128, 2)
    rows = got[:, :, :128].astype(f32).reshape(4, 2, 128, 2, HEAD_SIZE)
    sel_out = jnp.sum(rows * share[..., None], axis=0)

    def attended_of(which, pooled_rows):
        sel = lax.dynamic_index_in_dim(sel_out, which, 0, keepdims=False)
        gate = lax.dynamic_index_in_dim(gates, which, 2, keepdims=False)
        mix = (
            gate[0][:, :, None] * pooled_rows.reshape(128, 2, HEAD_SIZE)
            + gate[1][:, :, None] * sel
        )
        return mix.astype(bf16).reshape(128, 2 * HEAD_SIZE)

    mine_rows = attended_of(c, pooled_own)
    other_rows = attended_of(1 - c, pooled_got)
    shares = jnp.dot(mine_rows, out_weight, preferred_element_type=f32) + jnp.dot(
        other_rows, other_weight, preferred_element_type=f32
    )
    shares = shares.astype(bf16).reshape(4, 32, -1)
    pieces = lax.all_to_all(shares, "x", 0, 0, tiled=True)
    mixed = jnp.sum(pieces.astype(f32), axis=0).astype(bf16)
    return (mixed, log_sums)


def solution(mesh):
    split = Mesh(mesh.devices.reshape(16, 4, 4, 2), ("z", "y", "x", "c"))
    tp = ("x", "c")
    placed = (
        P(KV, None),
        P(None, tp),
        P(None, tp),
        P(None, tp),
        P(),
        P(),
        P(),
        P(tp, None),
        P(KV, None),
    )
    return jax.shard_map(
        shards,
        mesh=split,
        in_specs=placed,
        out_specs=(P(KV + tp, None), P(KV, tp)),
        check_vma=False,
    )
```

time: 195 us -> 156 us (0.80)
  blocking collectives: 97.3 us -> 57.9 us
  waiting for transfers between devices: 33 us -> 15.7 us
  starting transfers between devices: 5.13 us -> 21.4 us
  Pallas kernels: 0 us -> 15 us
  local copies, waits for them, and re-layouts: 18.8 us -> 12.5 us
  other arithmetic: 10.4 us -> 6.08 us
  matrix products: 15.8 us -> 11.8 us
    all_gather x2 -> x3, blocking collectives: 97.3 us -> 57.9 us  [the longest x1 34.8 us: shards(): pooled = lax.all_gather(pooled, 'z', axis=0, tiled=True)]
    all_gather x1, waiting for transfers between devices: 18.7 us -> 0.01 us  [shards(): all_kv = lax.all_gather(kv_rows, 'z', axis=0, tiled=True)]
    pallas_call x0 -> x1, Pallas kernels: none -> 15 us  [chosen_attention(): pl.pallas_call(chosen_kernel, grid_spec=pltpu.PrefetchScalarGridSpec(num_...]
    gather x3 -> x0, local copies, waits for them, and re-layouts: 12.5 us -> none  [the longest x1 6.2 us: shards(): taken = blocks[jnp.arange(owner_count, dtype=jnp.int32)[:, None], request]]
    ppermute x0 -> x2, starting transfers between devices: none -> 12 us  [the longest x1 10.1 us: shards(): pooled_got = lax.ppermute(pooled_send, 'c', [(0, 1), (1, 0)])]
    dot_general x11 -> x7, matrix products: 15.8 us -> 9.4 us  [the longest x1 2.33 us: shards(): jnp.dot(other_rows, other_weight, preferred_element_type=f32)]
    mul x5 -> x14, local copies, waits for them, and re-layouts: 0.94 us -> 6.77 us  [the longest x3 4.09 us: shards(): sel_out = jnp.sum(rows * share[..., None], axis=0)]
    all_to_all x1 -> x2, starting transfers between devices: 5.09 us -> 9.38 us  [the longest x1 5.25 us: shards(): got = lax.all_to_all(partial, ('y', 'c'), 0, 0, tiled=True)]
  transfers between devices with their start and end apart: 2 -> 5, of which waited for: 2 -> 2; matrix products, arithmetic and copies ran while one was open for 7% -> 14% of each run, Pallas kernels for 0% -> 10%
where the time goes in v1:
time: 156 us; the launch traced here: 155 us
  blocking collectives  57.9 us (37%)
  starting transfers between devices  21.4 us (14%)
  waiting for transfers between devices  15.7 us (10%)
  Pallas kernels  15 us (10%)
  between operations  14.4 us (9%)
  local copies, waits for them, and re-layouts  12.5 us (8%)
  matrix products  11.8 us (8%)
  other arithmetic  6.08 us (4%)
    all_gather x1, blocking collectives, shards(): pooled = lax.all_gather(pooled, 'z', axis=0, tiled=True)  34.8 us
    pallas_call x1, Pallas kernels, chosen_attention(): pl.pallas_call(chosen_kernel, grid_spec=pltpu.PrefetchScalarGridSpec(num_...  15 us
    all_gather x1, blocking collectives, shards(): near = lax.all_gather(sent, 'y', axis=0, tiled=False)  12.7 us
    all_gather x1, blocking collectives, shards(): pooled = lax.all_gather(pooled, 'y', axis=0, tiled=True)  10.4 us
    ppermute x1, starting transfers between devices, shards(): pooled_got = lax.ppermute(pooled_send, 'c', [(0, 1), (1, 0)])  10.1 us
    all_to_all x1, waiting for transfers between devices, shards(): got = lax.all_to_all(partial, ('y', 'c'), 0, 0, tiled=True)  8.45 us
    all_to_all x1, waiting for transfers between devices, shards(): pieces = lax.all_to_all(shares, 'x', 0, 0, tiled=True)  7.26 us
    all_to_all x1, starting transfers between devices, shards(): got = lax.all_to_all(partial, ('y', 'c'), 0, 0, tiled=True)  5.25 us
  transfers between devices with their start and end apart: 5, of which 2 were waited for; matrix products, arithmetic and copies ran while one was open for 14% of the time, Pallas kernels for 10%

profile of v1, /device:TPU:1, one launch (start us, length us, event | category | flops | bytes accessed | tf_op | source)
XLA Modules:
  0.0 154.9 jit_solution(7405402389815107691)
XLA Ops:
  7.3 1.3 copy-done
  8.6 1.5 fusion.50
  10.1 0.7 fusion.37
  10.8 0.4 multiply_reduce_fusion.4
  11.3 0.7 fusion.38
  12.1 0.8 pad_maximum_fusion.2
  12.9 0.5 fusion.52
  13.5 0.1 copy.72
  13.6 0.1 copy.73
  14.0 10.4 %all_gather.15 = bf16[64,256]{1,0:T(8,128)(2,1)S(1)} all-gather(bf16[16,256]{1,0:T(8,128)(2,1)S(1)} %pad_maximum_fusion.8), channel_id=1, replica_groups=mesh['z'=16,'y'=4,'x'=4,'c'=2] {'y'}, dimensions={0}, use_global_device_ids=true | all-gather | bytes 40960 | tf_op jit(solution)/shard_map/all_gather | solution.py:213
  24.4 0.3 compare_or_fusion
  24.8 34.8 %all_gather.16 = bf16[1024,256]{1,0:T(8,128)(2,1)S(1)} all-gather(bf16[64,256]{1,0:T(8,128)(2,1)S(1)} %all_gather.15), channel_id=1, replica_groups=mesh['z'=16,'y'=4,'x'=4,'c'=2] {'z'}, dimensions={0}, use_global_device_ids=true | all-gather | bytes 557056 | tf_op jit(solution)/shard_map/all_gather | solution.py:214
  59.7 2.4 %fusion.51 = (f32[2,256]{1,0:T(2,128)S(1)}, f32[2,256,1024]{1,2,0:T(8,128)}) fusion(pred[256,1024]{0,1:T(8,128)(4,1)S(1)} %compare_or_fusion, bf16[1024,256]{1,0:T(8,128)(2,1)S(1)} %all_gather.16, bf16[256,2,64]{2,0,1:T(8,128)(2,1)S(1)} %get-tuple-element.7, bf16[256,2,64]{2,0,1:T(8,128)(2,1)S(1)} %get-tuple-element.6), kind=kOutput, calls=%fused_computation.127 | convolution fusion | flops 137102336 | bytes 3016704 | tf_op jit(solution)/shard_map/sub | solution.py:226
  62.1 1.9 %convolution_bitcast_fusion = f32[256,2,128]{0,2,1:T(8,128)S(1)} fusion(f32[2,256,1024]{1,2,0:T(8,128)} %get-tuple-element.30, f32[2,256]{1,0:T(2,128)S(1)} %get-tuple-element.29, bf16[1024,256]{1,0:T(8,128)(2,1)S(1)} %all_gather.16), kind=kOutput, calls=%fused_computation.7 | convolution fusion | flops 135266304 | bytes 2623488 | tf_op jit(solution)/shard_map/jqn,nd->qjd/dot_general | solution.py:228
  64.0 0.1 copy.52
  64.2 0.2 reshape.198
  64.4 0.7 dynamic-slice_bitcast_fusion
  65.1 10.1 %collective-permute-start = (f32[4,32,256]{2,1,0:T(8,128)}, f32[4,32,256]{2,1,0:T(8,128)}, u32[]{:S(2)}, u32[]{:S(2)}) collective-permute-start(f32[4,32,256]{2,1,0:T(8,128)} %get-tuple-element.12), channel_id=1, source_target_pairs={{0,1},{1,0},{2,3},{3,2},{4,5},{5,4},{6,7},{7,6},{8,9},{9,8},{10,11... | collective-permute-start | bytes 393224 | tf_op jit(solution)/shard_map/ppermute | solution.py:232
  75.2 1.9 %collective-permute-start.1 = (bf16[256,2048]{1,0:T(8,128)(2,1)}, bf16[256,2048]{1,0:T(8,128)(2,1)}, u32[]{:S(2)}, u32[]{:S(2)}) collective-permute-start(bf16[256,2048]{1,0:T(8,128)(2,1)} %param.22), channel_id=1, source_target_pairs={{0,1},{1,0},{2,3},{3,2},{4,5},{5,4},{6,7},{7,6},{8,9},{9,8},{10,11... | collective-permute-start | bytes 3145736 | tf_op jit(solution)/shard_map/ppermute | solution.py:180
  77.4 12.7 %all-gather = bf16[2112,128]{1,0:T(8,128)(2,1)S(1)} all-gather(bf16[528,128]{1,0:T(8,128)(2,1)S(1)} %fusion.11), channel_id=2, replica_groups=mesh['z'=16,'y'=4,'x'=4,'c'=2] {'y'}, dimensions={0}, use_global_device_ids=true | all-gather | bytes 675840 | tf_op jit(solution)/shard_map/all_gather | solution.py:188
  90.1 0.8 slice.95
  91.0 0.1 fusion.47
  91.2 0.1 multiply_reduce_fusion.2
  91.3 0.3 multiply_reduce_fusion.1
  91.6 0.7 sub.84.ids_ref
  92.4 0.1 reduce_max.28
  92.5 0.7 pad_add_fusion.meta_ref
  93.2 15.0 %chosen_attention.1 = bf16[8,144,256]{2,1,0:T(8,128)(2,1)} custom-call(s32[6]{0:T(128)} %pad_add_fusion.meta_ref, s32[512]{0:T(512)} %sub.84.ids_ref, bf16[2048,128]{1,0:T(8,128)(2,1)} %bitcast.132, bf16[4096,256]{1,0:T(8,128)(2,1)} %all-gather.3.cloned.1.call-done.kv_ref), custom_call_target="tpu_custom_call" | custom-call | tf_op jit(solution)/shard_map/chosen_attention/pallas_call | solution.py:136
  108.2 5.2 %all-to-all-start = ((bf16[8,144,256]{2,1,0:T(8,128)(2,1)}), bf16[8,144,256]{2,1,0:T(8,128)(2,1)S(1)}, u32[]{:S(2)}, u32[]{:S(2)}) async-start(bf16[8,144,256]{2,1,0:T(8,128)(2,1)} %chosen_attention.1), calls=%async_computation | async-start | bytes 1179648 | tf_op jit(solution)/shard_map/all_to_all | solution.py:244
  113.4 1.1 fusion.5
  115.0 8.5 %all-to-all-done = bf16[8,144,256]{2,1,0:T(8,128)(2,1)S(1)} async-done(((bf16[8,144,256]{2,1,0:T(8,128)(2,1)}), bf16[8,144,256]{2,1,0:T(8,128)(2,1)S(1)}, u32[]{:S(2)}, u32[]{:S(2)}) %all-to-all-start) | async-done | bytes 589856 | tf_op jit(solution)/shard_map/all_to_all | solution.py:244
  123.5 0.1 reshape.205
  124.0 1.1 copy.70
  125.1 2.2 %mul.286 = f32[4,2,128,2,128]{4,3,2,1,0:T(2,128)S(1)} broadcast(f32[4,2,128,2]{3,2,1,0:T(8,128)} %bitcast.130), dimensions={0,1,2,3} | broadcast | bytes 1056768 | tf_op jit(solution)/shard_map/mul | solution.py:261
  127.3 0.8 mul.287
  128.1 1.2 multiply_reduce_fusion
  129.3 0.1 reduce_sum.94
  129.5 0.2 mul.236
  129.7 0.2 mul.271
  129.9 0.2 mul.291
  130.1 0.2 mul.295
  130.3 0.9 fusion.13
  131.3 1.5 fusion.53
  132.8 2.3 %fusion.1 = bf16[128,2048]{1,0:T(8,128)(2,1)} fusion(f32[128,2048]{1,0:T(8,128)S(1)} %fusion.53, bf16[128,256]{1,0:T(8,128)(2,1)S(1)} %fusion.13, bf16[256,2048]{1,0:T(8,128)(2,1)} %collective-permute-done.1), kind=kOutput, calls=%fused_computation.2 | convolution fusion | flops 134742016 | bytes 2686976 | tf_op jit(solution)/shard_map/dot_general | solution.py:274
  135.2 4.1 %all-to-all-start.1 = ((bf16[4,32,2048]{2,1,0:T(8,128)(2,1)}), bf16[4,32,2048]{2,1,0:T(8,128)(2,1)S(1)}, u32[]{:S(2)}, u32[]{:S(2)}) async-start(bf16[4,32,2048]{2,1,0:T(8,128)(2,1)} %bitcast.36), calls=%async_computation.1 | async-start | bytes 1048576 | tf_op jit(solution)/shard_map/all_to_all | solution.py:278
  139.4 0.7 reshape.208
  140.1 7.3 %all-to-all-done.1 = bf16[4,32,2048]{2,1,0:T(8,128)(2,1)S(1)} async-done(((bf16[4,32,2048]{2,1,0:T(8,128)(2,1)}), bf16[4,32,2048]{2,1,0:T(8,128)(2,1)S(1)}, u32[]{:S(2)}, u32[]{:S(2)}) %all-to-all-start.1) | async-done | bytes 524320 | tf_op jit(solution)/shard_map/all_to_all | solution.py:278
  147.3 0.7 reduce_sum.95
  (64 shorter events, 2.1 us)
Async XLA Ops:
  7.2 1.4 copy-start
  7.2 4.8 %copy-start.4 = (f32[256,64]{1,0:T(8,128)S(1)}, f32[256,64]{1,0:T(8,128)}, u32[]{:S(2)}) copy-start(f32[256,64]{1,0:T(8,128)} %constant.155.clone) | copy-start | bytes 196612
  7.2 4.8 %copy-start.5 = (f32[256,64]{1,0:T(8,128)S(1)}, f32[256,64]{1,0:T(8,128)}, u32[]{:S(2)}) copy-start(f32[256,64]{1,0:T(8,128)} %constant.156.clone) | copy-start | bytes 196612
  7.2 3.6 %copy-start.3 = (bf16[2048,128]{1,0:T(8,128)(2,1)S(1)}, bf16[2048,128]{1,0:T(8,128)(2,1)}, u32[]{:S(2)}) copy-start(bf16[2048,128]{1,0:T(8,128)(2,1)} %param.17) | copy-start | bytes 1572868
  7.2 85.9 %all-gather.3.cloned.1.call-start = ((), (), s32[]{:S(2)}) async-start(), calls=%async_computation.2 | async-start | bytes 2228224 | tf_op jit(solution)/shard_map/all_gather | solution.py:178
  8.6 4.3 %copy-start.2 = (bf16[2048,256]{1,0:T(8,128)(2,1)S(1)}, bf16[2048,256]{1,0:T(8,128)(2,1)}, u32[]{:S(2)}) copy-start(bf16[2048,256]{1,0:T(8,128)(2,1)} %param.16) | copy-start | bytes 3145732
  64.0 13.2 %copy-start.7 = (s32[4,32]{1,0:T(4,128)S(1)}, s32[4,32]{1,0:T(4,128)}, u32[]{:S(2)}) copy-start(s32[4,32]{1,0:T(4,128)} %param.23) | copy-start | bytes 1540
  64.0 27.2 %copy-start.6 = (s32[32,32]{1,0:T(8,128)S(1)}, s32[32,32]{1,0:T(8,128)}, u32[]{:S(2)}) copy-start(s32[32,32]{1,0:T(8,128)} %constant.164) | copy-start | bytes 12292
  65.1 64.9 %collective-permute-start = (f32[4,32,256]{2,1,0:T(8,128)}, f32[4,32,256]{2,1,0:T(8,128)}, u32[]{:S(2)}, u32[]{:S(2)}) collective-permute-start(f32[4,32,256]{2,1,0:T(8,128)} %get-tuple-element.12), channel_id=1, source_target_pairs={{0,1},{1,0},{2,3},{3,2},{4,5},{5,4},{6,7},{7,6},{8,9},{9,8},{10,11... | collective-permute-start | bytes 393224 | tf_op jit(solution)/shard_map/ppermute | solution.py:232
  75.2 57.7 %collective-permute-start.1 = (bf16[256,2048]{1,0:T(8,128)(2,1)}, bf16[256,2048]{1,0:T(8,128)(2,1)}, u32[]{:S(2)}, u32[]{:S(2)}) collective-permute-start(bf16[256,2048]{1,0:T(8,128)(2,1)} %param.22), channel_id=1, source_target_pairs={{0,1},{1,0},{2,3},{3,2},{4,5},{5,4},{6,7},{7,6},{8,9},{9,8},{10,11... | collective-permute-start | bytes 3145736 | tf_op jit(solution)/shard_map/ppermute | solution.py:180
  108.2 15.3 %all-to-all-start = ((bf16[8,144,256]{2,1,0:T(8,128)(2,1)}), bf16[8,144,256]{2,1,0:T(8,128)(2,1)S(1)}, u32[]{:S(2)}, u32[]{:S(2)}) async-start(bf16[8,144,256]{2,1,0:T(8,128)(2,1)} %chosen_attention.1), calls=%async_computation | async-start | bytes 1179648 | tf_op jit(solution)/shard_map/all_to_all | solution.py:244
  123.5 1.6 %copy-start.1 = (bf16[8,144,256]{2,1,0:T(8,128)(2,1)}, bf16[8,144,256]{2,1,0:T(8,128)(2,1)S(1)}, u32[]{:S(2)}) copy-start(bf16[8,144,256]{2,1,0:T(8,128)(2,1)S(1)} %all-to-all-done) | copy-start | bytes 1769476
  135.2 12.2 %all-to-all-start.1 = ((bf16[4,32,2048]{2,1,0:T(8,128)(2,1)}), bf16[4,32,2048]{2,1,0:T(8,128)(2,1)S(1)}, u32[]{:S(2)}, u32[]{:S(2)}) async-start(bf16[4,32,2048]{2,1,0:T(8,128)(2,1)} %bitcast.36), calls=%async_computation.1 | async-start | bytes 1048576 | tf_op jit(solution)/shard_map/all_to_all | solution.py:278
Sparse Core Ops, SparseCore 0:
  13.0 69.8 all-gather.2

commit v2 on v1

v2 whole, which is shorter than its diff:
```python
import jax
import jax.numpy as jnp
import numpy as np
from jax import lax
from jax.experimental import pallas as pl
from jax.experimental.pallas import tpu as pltpu
from jax.sharding import Mesh
from jax.sharding import PartitionSpec as P

HEAD_SIZE = 128
BLOCK = 64
POOL_STRIDE = 16
THETA = 10000.0
NEGATIVE = -1e30
FLOOR = -1e29
KV = ("z", "y")
SPAN = 256
STATS = 16
PER_STEP = 8
POOLED = 16
RING = 16
LIST = 32
SCALE = HEAD_SIZE**-0.5


def rotary_tables(start, offsets):
    half = HEAD_SIZE // 2
    inverse = THETA ** (-np.arange(half, dtype=np.float64) / half)
    local = np.asarray(offsets, np.float64)[:, None] * inverse[None, :]
    cos_l = jnp.asarray(np.cos(local), jnp.float32)
    sin_l = jnp.asarray(np.sin(local), jnp.float32)
    starts = np.arange(64, dtype=np.float64)[:, None] * SPAN * inverse[None, :]
    cos_s = lax.dynamic_slice_in_dim(jnp.asarray(np.cos(starts), jnp.float32), start, 1, 0)
    sin_s = lax.dynamic_slice_in_dim(jnp.asarray(np.sin(starts), jnp.float32), start, 1, 0)
    return cos_l * cos_s - sin_l * sin_s, sin_l * cos_s + cos_l * sin_s


def rotate(value, cosines, sines):
    half = HEAD_SIZE // 2
    front, back = value[..., :half], value[..., half:]
    return jnp.concatenate([front * cosines - back * sines, back * cosines + front * sines], -1)


def split_three(value):
    high = value.astype(jnp.bfloat16).astype(jnp.float32)
    rest = value - high
    middle = rest.astype(jnp.bfloat16).astype(jnp.float32)
    return [high, middle, rest - middle]


def attend_kernel(meta_ref, ids_ref, bias_ref, q_ref, *refs):
    chunk_refs = refs[:RING]
    out_ref, kv_ref, pool_ref, acc_ref, m_ref, l_ref, lse_ref = refs[RING:]
    z = meta_ref[0]
    y = meta_ref[1]
    for o in range(RING):
        kv_ref[o * SPAN : (o + 1) * SPAN, :] = chunk_refs[o][:SPAN, :]
        pool_ref[o * POOLED : (o + 1) * POOLED, :] = chunk_refs[o][SPAN:, :]
    row = lax.broadcasted_iota(jnp.int32, (BLOCK, HEAD_SIZE), 0)
    lane = lax.broadcasted_iota(jnp.int32, (1, HEAD_SIZE), 1)
    lane = jnp.where(lane >= BLOCK, lane - BLOCK, lane)

    def store(peer, qb, first, normal):
        out = jnp.transpose(normal).astype(jnp.bfloat16)
        for half in range(2):
            for head in range(2):
                at = head * BLOCK + half * 32
                out_ref[
                    peer * 2 + half,
                    first + qb * 32 : first + (qb + 1) * 32,
                    head * HEAD_SIZE : (head + 1) * HEAD_SIZE,
                ] = out[at : at + 32]

    pool_row = lax.broadcasted_iota(jnp.int32, (SPAN, 1), 0)
    offset = pool_row // POOLED
    pool_at = ((z - offset) * 4 + y) * POOLED + pool_row % POOLED
    pool_end = pool_at * POOL_STRIDE + POOL_STRIDE - 1
    pool_end = jnp.where(offset > z, 1 << 30, jnp.where(pool_at == 0, 0, pool_end))
    for peer in range(4):
        for qb in range(4):
            g = peer * 4 + qb
            qpos = (z * 4 + peer) * SPAN + qb * BLOCK + lane
            s = lax.dot_general(
                pool_ref[:, :HEAD_SIZE],
                q_ref[g * 128 : (g + 1) * 128, :],
                (((1,), (1,)), ((), ())),
                preferred_element_type=jnp.float32,
            )
            s = jnp.where(pool_end <= qpos, s * SCALE, NEGATIVE)
            m = jnp.maximum(jnp.max(s, axis=0, keepdims=True), FLOOR)
            p = jnp.exp(s - m)
            total = jnp.sum(p, axis=0, keepdims=True)
            acc = lax.dot_general(
                pool_ref[:, HEAD_SIZE:],
                p.astype(jnp.bfloat16),
                (((0,), (0,)), ((), ())),
                preferred_element_type=jnp.float32,
            )
            some = total > 0.0
            total = jnp.where(some, total, 1.0)
            store(peer, qb, 128, acc / total)
            lse_ref[16 + g : 17 + g, :] = jnp.where(some, m + jnp.log(total), FLOOR)

    for peer in range(4):
        for qb in range(4):
            acc_ref[qb] = jnp.zeros((HEAD_SIZE, HEAD_SIZE), jnp.float32)
            m_ref[qb] = jnp.full((1, HEAD_SIZE), FLOOR, jnp.float32)
            l_ref[qb] = jnp.zeros((1, HEAD_SIZE), jnp.float32)

        def group(k, carry, peer=peer):
            for qb in range(4):
                g = peer * 4 + qb
                qpos = (z * 4 + peer) * SPAN + qb * BLOCK + lane
                keys, values, bases, biases = [], [], [], []
                for e in range(PER_STEP):
                    at = g * LIST + k * PER_STEP + e
                    idx = ids_ref[at]
                    none = idx < 0
                    safe = jnp.where(none, 0, idx)
                    first = pl.multiple_of(safe * BLOCK, BLOCK)
                    keys.append(kv_ref[pl.ds(first, BLOCK), :HEAD_SIZE])
                    values.append(kv_ref[pl.ds(first, BLOCK), HEAD_SIZE:])
                    base = ((z - safe // 4) * 4 + y) * SPAN + (safe % 4) * BLOCK
                    bases.append(jnp.where(none, 1 << 30, base))
                    biases.append(bias_ref[at])
                kg = jnp.concatenate(keys, 0)
                vg = jnp.concatenate(values, 0)
                s = lax.dot_general(
                    kg,
                    q_ref[g * 128 : (g + 1) * 128, :],
                    (((1,), (1,)), ((), ())),
                    preferred_element_type=jnp.float32,
                )
                slabs = []
                for e in range(PER_STEP):
                    slab = s[e * BLOCK : (e + 1) * BLOCK] * SCALE + biases[e]
                    seen = row <= (qpos - bases[e])
                    slabs.append(jnp.where(seen, slab, NEGATIVE))
                s = jnp.concatenate(slabs, 0)
                m_old = m_ref[qb]
                m_new = jnp.maximum(m_old, jnp.max(s, axis=0, keepdims=True))
                alpha = jnp.exp(m_old - m_new)
                p = jnp.exp(s - m_new)
                l_ref[qb] = l_ref[qb] * alpha + jnp.sum(p, axis=0, keepdims=True)
                m_ref[qb] = m_new
                pv = lax.dot_general(
                    vg,
                    p.astype(jnp.bfloat16),
                    (((0,), (0,)), ((), ())),
                    preferred_element_type=jnp.float32,
                )
                acc_ref[qb] = acc_ref[qb] * alpha + pv
            return carry

        lax.fori_loop(0, meta_ref[2 + peer], group, 0)
        for qb in range(4):
            total = l_ref[qb]
            some = total > 0.0
            total = jnp.where(some, total, 1.0)
            store(peer, qb, 0, acc_ref[qb] / total)
            g = peer * 4 + qb
            lse_ref[g : g + 1, :] = jnp.where(some, m_ref[qb] + jnp.log(total), FLOOR)

    for peer in range(4):
        rows = []
        for branch in range(2):
            at = branch * 16 + peer * 4
            lse = lse_ref[at : at + 4, :]
            wide = jnp.concatenate(
                [
                    jnp.concatenate([lse[0:1], lse[1:2]], 1),
                    jnp.concatenate([lse[2:3], lse[3:4]], 1),
                ],
                0,
            )
            rows += split_three(wide)
        rows.append(jnp.zeros((STATS - 12, 2 * HEAD_SIZE), jnp.float32))
        block = jnp.concatenate(rows, 0).astype(jnp.bfloat16)
        for half in range(2):
            out_ref[peer * 2 + half, SPAN : SPAN + STATS, :] = block


def attend(meta, ids, bias, queries, chunks):
    whole = lambda shape: pl.BlockSpec(shape, lambda i, *_: (0,) * len(shape))
    return pl.pallas_call(
        attend_kernel,
        grid_spec=pltpu.PrefetchScalarGridSpec(
            num_scalar_prefetch=3,
            grid=(1,),
            in_specs=[whole((2048, HEAD_SIZE))]
            + [whole((SPAN + POOLED, 2 * HEAD_SIZE))] * RING,
            out_specs=whole((8, SPAN + STATS, 2 * HEAD_SIZE)),
            scratch_shapes=[
                pltpu.VMEM((RING * SPAN, 2 * HEAD_SIZE), jnp.bfloat16),
                pltpu.VMEM((RING * POOLED, 2 * HEAD_SIZE), jnp.bfloat16),
                pltpu.VMEM((4, HEAD_SIZE, HEAD_SIZE), jnp.float32),
                pltpu.VMEM((4, 1, HEAD_SIZE), jnp.float32),
                pltpu.VMEM((4, 1, HEAD_SIZE), jnp.float32),
                pltpu.VMEM((32, HEAD_SIZE), jnp.float32),
            ],
        ),
        out_shape=jax.ShapeDtypeStruct((8, SPAN + STATS, 2 * HEAD_SIZE), jnp.bfloat16),
        name="attend",
    )(meta, ids, bias, queries, *chunks)


def merge_kernel(meta_ref, got_ref, gate_ref, own_ref, other_ref, out_ref, log_ref, t_ref, att_ref):
    c = meta_ref[0]
    for branch in range(2):
        pieces = []
        for core in range(2):
            lses = []
            for peer in range(4):
                block = got_ref[peer * 2 + core, SPAN : SPAN + STATS, :].astype(jnp.float32)
                at = branch * 6
                lses.append(block[at : at + 2] + block[at + 2 : at + 4] + block[at + 4 : at + 6])
            top = jnp.maximum(jnp.maximum(lses[0], lses[1]), jnp.maximum(lses[2], lses[3]))
            parts = [jnp.exp(v - top) for v in lses]
            total = (parts[0] + parts[1]) + (parts[2] + parts[3])
            if branch == 0:
                log_ref[core] = top + jnp.log(total)
            for v in parts:
                share = v / total
                pieces.append(share[:, :HEAD_SIZE])
                pieces.append(share[:, HEAD_SIZE:])
        t_ref[branch] = jnp.transpose(jnp.concatenate(pieces, 0))
    for core in range(2):
        for qb in range(4):
            for head in range(2):
                cols = slice(head * HEAD_SIZE, (head + 1) * HEAD_SIZE)
                total = jnp.zeros((32, HEAD_SIZE), jnp.float32)
                for branch in range(2):
                    share = t_ref[branch, pl.ds(head * BLOCK + c * 32, 32), :]
                    part = jnp.zeros((32, HEAD_SIZE), jnp.float32)
                    for peer in range(4):
                        col = (core * 4 + peer) * 4 + (qb % 2) * 2 + qb // 2
                        first = branch * 128 + qb * 32
                        value = got_ref[peer * 2 + core, first : first + 32, cols]
                        part = part + value.astype(jnp.float32) * share[:, col : col + 1]
                    g = (1 - branch) * 4 + core * 2 + head
                    total = total + part * gate_ref[qb * 32 : (qb + 1) * 32, g : g + 1]
                att_ref[core, qb * 32 : (qb + 1) * 32, cols] = total.astype(jnp.bfloat16)
    shares = jnp.dot(att_ref[c], own_ref[...], preferred_element_type=jnp.float32)
    shares = shares + jnp.dot(att_ref[1 - c], other_ref[...], preferred_element_type=jnp.float32)
    out_ref[...] = shares.astype(jnp.bfloat16)


def merge(meta, got, gates, own_weight, other_weight):
    whole = lambda shape: pl.BlockSpec(shape, lambda i, *_: (0,) * len(shape))
    width = own_weight.shape[1]
    return pl.pallas_call(
        merge_kernel,
        grid_spec=pltpu.PrefetchScalarGridSpec(
            num_scalar_prefetch=1,
            grid=(1,),
            in_specs=[
                whole((8, SPAN + STATS, 2 * HEAD_SIZE)),
                whole((128, 8)),
                whole((2 * HEAD_SIZE, width)),
                whole((2 * HEAD_SIZE, width)),
            ],
            out_specs=[whole((128, width)), whole((2, 2, 2 * HEAD_SIZE))],
            scratch_shapes=[
                pltpu.VMEM((2, HEAD_SIZE, 32), jnp.float32),
                pltpu.VMEM((2, 128, 2 * HEAD_SIZE), jnp.bfloat16),
            ],
        ),
        out_shape=[
            jax.ShapeDtypeStruct((128, width), jnp.bfloat16),
            jax.ShapeDtypeStruct((2, 2, 2 * HEAD_SIZE), jnp.float32),
        ],
        name="merge",
    )(meta, got, gates, own_weight, other_weight)


def shards(
    tokens,
    query_weight,
    key_matrix,
    value_matrix,
    gate_weight,
    key_pool_weight,
    value_pool_weight,
    out_weight,
    chosen,
):
    z, y = lax.axis_index("z"), lax.axis_index("y")
    x, c = lax.axis_index("x"), lax.axis_index("c")
    own = z * 4 + y
    group = x * 2 + c
    f32, bf16 = jnp.float32, jnp.bfloat16

    cosines, sines = rotary_tables(own, np.arange(SPAN))
    key_projected = jnp.dot(tokens, key_matrix, preferred_element_type=f32)
    value_projected = jnp.dot(tokens, value_matrix, preferred_element_type=f32)
    keys = rotate(key_projected, cosines, sines).astype(bf16)
    key_mix = lax.dynamic_slice_in_dim(key_pool_weight, group, 1, 1)
    value_mix = lax.dynamic_slice_in_dim(value_pool_weight, group, 1, 1)
    pooled_k = jnp.sum(key_projected.reshape(POOLED, POOL_STRIDE, HEAD_SIZE) * key_mix[None], axis=1)
    pooled_v = jnp.sum(
        value_projected.reshape(POOLED, POOL_STRIDE, HEAD_SIZE) * value_mix[None], axis=1
    )
    last = slice(POOL_STRIDE - 1, None, POOL_STRIDE)
    pooled_k = rotate(pooled_k, cosines[last], sines[last])
    chunk = jnp.concatenate(
        [
            jnp.concatenate([keys, value_projected.astype(bf16)], -1),
            jnp.concatenate([pooled_k.astype(bf16), pooled_v.astype(bf16)], -1),
        ],
        0,
    )
    ring_up = [(i, (i + 1) % RING) for i in range(RING)]
    ring_down = [(i, (i - 1) % RING) for i in range(RING)]
    chunks = [None] * RING
    chunks[0] = chunk
    up = down = chunk
    for k in range(1, RING // 2 + 1):
        up = lax.ppermute(up, "z", ring_up)
        chunks[k] = up
        if k < RING // 2:
            down = lax.ppermute(down, "z", ring_down)
            chunks[RING - k] = down

    other_weight = lax.ppermute(out_weight, "c", [(0, 1), (1, 0)])

    query_proj = jnp.dot(tokens, query_weight, preferred_element_type=f32)
    query_proj = query_proj.reshape(SPAN, 2, HEAD_SIZE)
    queries = rotate(query_proj, cosines[:, None, :], sines[:, None, :]).astype(bf16)
    by_block = queries.reshape(4, BLOCK, 2, HEAD_SIZE).transpose(0, 2, 1, 3)
    picks = jnp.pad(chosen.astype(bf16).reshape(1, 128), ((0, 15), (0, 0)))
    sent = jnp.concatenate([by_block.reshape(512, HEAD_SIZE), picks], 0)
    near = lax.all_gather(sent, "y", axis=0, tiled=False)
    near_queries = near[:, :512].reshape(2048, HEAD_SIZE)
    near_chosen = near[:, 512].reshape(16, 32).astype(jnp.int32)

    mine = (near_chosen // 4) % 4 == y
    slot = ((z - near_chosen // 16) % RING) * 4 + near_chosen % 4
    slot = jnp.where(mine, slot, -1)
    counts = jnp.sum((slot[:, :, None] == np.arange(BLOCK)[None, None, :]).astype(jnp.int32), axis=1)
    present = counts > 0
    earlier = (np.arange(BLOCK)[:, None] < np.arange(BLOCK)[None, :]).astype(np.float32)
    rank = jnp.dot(present.astype(f32), earlier).astype(jnp.int32)
    hit = present[:, :, None] & (rank[:, :, None] == np.arange(LIST)[None, None, :])
    ids = jnp.sum(jnp.where(hit, np.arange(1, BLOCK + 1)[None, :, None], 0), axis=1) - 1
    times = jnp.sum(jnp.where(hit, counts[:, :, None], 0), axis=1)
    bias = jnp.log(jnp.maximum(times, 1).astype(f32))
    lengths = jnp.sum(present.astype(jnp.int32), axis=1)
    steps = (jnp.max(lengths.reshape(4, 4), axis=1) + PER_STEP - 1) // PER_STEP
    meta = jnp.concatenate([jnp.stack([z, y]).astype(jnp.int32), steps.astype(jnp.int32)])

    own_tokens = lax.dynamic_index_in_dim(
        tokens.reshape(4, 2, 32, -1), c, 1, keepdims=False
    ).reshape(128, -1)
    gate_cols = lax.dynamic_slice_in_dim(gate_weight, x * 4, 4, 2)
    gates = jax.nn.sigmoid(
        jnp.einsum("td,bdh->tbh", own_tokens, gate_cols, preferred_element_type=f32)
    ).reshape(128, 8)

    partial = attend(meta, ids.reshape(-1), bias.reshape(-1), near_queries, chunks)
    got = lax.all_to_all(partial, ("y", "c"), 0, 0, tiled=True)
    shares, log_all = merge(
        c.astype(jnp.int32).reshape(1), got, gates, out_weight, other_weight
    )
    log_own = lax.dynamic_index_in_dim(log_all, c, 0, keepdims=False)
    log_sums = log_own.reshape(4, 2, BLOCK).transpose(0, 2, 1).reshape(SPAN, 2)
    pieces = lax.all_to_all(shares.reshape(4, 32, -1), "x", 0, 0, tiled=True)
    mixed = jnp.sum(pieces.astype(f32), axis=0).astype(bf16)
    return (mixed, log_sums)


def solution(mesh):
    split = Mesh(mesh.devices.reshape(16, 4, 4, 2), ("z", "y", "x", "c"))
    tp = ("x", "c")
    placed = (
        P(KV, None),
        P(None, tp),
        P(None, tp),
        P(None, tp),
        P(),
        P(),
        P(),
        P(tp, None),
        P(KV, None),
    )
    return jax.shard_map(
        shards,
        mesh=split,
        in_specs=placed,
        out_specs=(P(KV + tp, None), P(KV, tp)),
        check_vma=False,
    )
```

time: 156 us -> 145 us (0.929)
  starting transfers between devices: 21.4 us -> 75.7 us
  blocking collectives: 57.9 us -> 11.2 us
  between operations: 14.4 us -> 1.15 us
  waiting for transfers between devices: 15.7 us -> 24.5 us
  matrix products: 11.8 us -> 4.79 us
  local copies, waits for them, and re-layouts: 12.5 us -> 9.54 us
  other arithmetic: 6.08 us -> 3.68 us
    ppermute x1 -> x15, starting transfers between devices: 10.1 us -> 56.6 us  [the longest x7 38.8 us: shards(): down = lax.ppermute(down, 'z', ring_down)]
    all_gather x2 -> x0, blocking collectives: 45.2 us -> none  [the longest x1 34.8 us: shards(): pooled = lax.all_gather(pooled, 'z', axis=0, tiled=True)]
    all_to_all x1, starting transfers between devices: 5.25 us -> 12.3 us  [shards(): got = lax.all_to_all(partial, ('y', 'c'), 0, 0, tiled=True)]
    dot_general x4 -> x2, matrix products: 6.9 us -> 1.23 us  [the longest x1 1.1 us: shards(): jnp.einsum('td,bdh->tbh', own_tokens, gate_cols, preferred_element_type=f32)]
    all_to_all x1, waiting for transfers between devices: 8.45 us -> 13.8 us  [shards(): got = lax.all_to_all(partial, ('y', 'c'), 0, 0, tiled=True)]
    mul x13 -> x1, local copies, waits for them, and re-layouts: 6.06 us -> 1.32 us  [shards(): key_projected.reshape(POOLED, POOL_STRIDE, HEAD_SIZE) * key_mix[None]]
    ppermute x1 -> x15, waiting for transfers between devices: 0.01 us -> 4.14 us  [the longest x8 3.85 us: shards(): up = lax.ppermute(up, 'z', ring_up)]
    sub x1 -> x0, matrix products: 2.41 us -> none  [shards(): exponent = jnp.where(visible, jnp.exp(masked - peak), 0.0)]
  transfers between devices with their start and end apart: 5 -> 18, of which waited for: 2 -> 5; matrix products, arithmetic and copies ran while one was open for 14% -> 6% of each run, Pallas kernels for 10% -> 7%
where the time goes in v2:
time: 145 us; the launch traced here: 144 us
  starting transfers between devices  75.7 us (52%)
  waiting for transfers between devices  24.5 us (17%)
  Pallas kernels  13.7 us (9%)
  blocking collectives  11.2 us (8%)
  local copies, waits for them, and re-layouts  9.54 us (7%)
  matrix products  4.79 us (3%)
  other arithmetic  3.68 us (3%)
    ppermute x7, starting transfers between devices, shards(): down = lax.ppermute(down, 'z', ring_down)  38.8 us
    ppermute x8, starting transfers between devices, shards(): up = lax.ppermute(up, 'z', ring_up)  17.8 us
    all_to_all x1, waiting for transfers between devices, shards(): got = lax.all_to_all(partial, ('y', 'c'), 0, 0, tiled=True)  13.8 us
    all_to_all x1, starting transfers between devices, shards(): got = lax.all_to_all(partial, ('y', 'c'), 0, 0, tiled=True)  12.3 us
    all_gather x1, blocking collectives, shards(): near = lax.all_gather(sent, 'y', axis=0, tiled=False)  11.2 us
    pallas_call x1, Pallas kernels, attend(): pl.pallas_call(attend_kernel, grid_spec=pltpu.PrefetchScalarGridSpec(num_...  9.4 us
    all_to_all x1, waiting for transfers between devices, shards(): pieces = lax.all_to_all(shares.reshape(4, 32, -1), 'x', 0, 0, tiled=True)  6.59 us
    pallas_call x1, Pallas kernels, merge(): pl.pallas_call(merge_kernel, grid_spec=pltpu.PrefetchScalarGridSpec(num_s...  4.27 us
  transfers between devices with their start and end apart: 18, of which 5 were waited for; matrix products, arithmetic and copies ran while one was open for 6% of the time, Pallas kernels for 7%

profile of v2, /device:TPU:1, one launch (start us, length us, event | category | flops | bytes accessed | tf_op | source)
XLA Modules:
  0.0 144.3 jit_solution(7763219400571755615)
XLA Ops:
  0.7 1.3 fusion.21
  2.0 1.5 %multiply_reduce_fusion.1 = (f32[16,128]{1,0:T(8,128)S(1)}, f32[256,128]{1,0:T(8,128)S(1)}) fusion(f32[16]{0:T(128)S(1)} %get-tuple-element.22, bf16[256,2048]{1,0:T(8,128)(2,1)S(1)} %copy-done, bf16[2048,128]{1,0:T(8,128)(2,1)} %param.19), kind=kOutput, calls=%fused_computation.17 | convolution fusion | flops 134281216 | bytes 1712192 | tf_op jit(solution)/shard_map/dot_general | solution.py:294
  3.5 0.7 fusion.19
  4.4 0.6 slice.39
  5.0 1.6 %multiply_reduce_fusion = (bf16[16,128]{1,0:T(8,128)(2,1)S(1)}, bf16[256,128]{1,0:T(8,128)(2,1)S(1)}) fusion(f32[16]{0:T(128)} %get-tuple-element.23, bf16[256,2048]{1,0:T(8,128)(2,1)S(1)} %copy-done, bf16[2048,128]{1,0:T(8,128)(2,1)} %param.20), kind=kOutput, calls=%fused_computation.16 | convolution fusion | flops 134313984 | bytes 1642560 | tf_op jit(solution)/shard_map/dot_general | solution.py:295
  6.6 0.8 maximum_maximum_fusion.refs_0_
  7.4 4.4 %collective-permute-start = (bf16[272,256]{1,0:T(8,128)(2,1)}, bf16[272,256]{1,0:T(8,128)(2,1)}, u32[]{:S(2)}, u32[]{:S(2)}) collective-permute-start(bf16[272,256]{1,0:T(8,128)(2,1)} %maximum_maximum_fusion.refs_0_), channel_id=1, source_target_pairs={{0,32},{32,64},{64,96},{96,128},{128,160},{160,192},{192,224},{224... | collective-permute-start | bytes 417800 | tf_op jit(solution)/shard_map/ppermute | solution.py:318
  11.8 9.5 %collective-permute-start.8 = (bf16[272,256]{1,0:T(8,128)(2,1)}, bf16[272,256]{1,0:T(8,128)(2,1)}, u32[]{:S(2)}, u32[]{:S(2)}) collective-permute-start(bf16[272,256]{1,0:T(8,128)(2,1)} %maximum_maximum_fusion.refs_0_), channel_id=1, source_target_pairs={{0,480},{32,0},{64,32},{96,64},{128,96},{160,128},{192,160},{224,1... | collective-permute-start | bytes 417800 | tf_op jit(solution)/shard_map/ppermute | solution.py:321
  21.3 2.9 %collective-permute-start.15 = (bf16[256,2048]{1,0:T(8,128)(2,1)S(1)}, bf16[256,2048]{1,0:T(8,128)(2,1)}, u32[]{:S(2)}, u32[]{:S(2)}) collective-permute-start(bf16[256,2048]{1,0:T(8,128)(2,1)S(1)} %copy-done.3), channel_id=1, source_target_pairs={{0,1},{1,0},{2,3},{3,2},{4,5},{5,4},{6,7},{7,6},{8,9},{9,8},{10,11... | collective-permute-start | bytes 3145736 | tf_op jit(solution)/shard_map/ppermute | solution.py:324
  24.3 0.5 fusion.23
  25.2 0.2 maximum_bitcast_fusion
  25.4 0.2 copy.56
  25.7 1.9 %collective-permute-start.1 = (bf16[272,256]{1,0:T(8,128)(2,1)}, bf16[272,256]{1,0:T(8,128)(2,1)S(1)}, u32[]{:S(2)}, u32[]{:S(2)}) collective-permute-start(bf16[272,256]{1,0:T(8,128)(2,1)} %collective-permute-done.refs_1_), channel_id=1, source_target_pairs={{0,32},{32,64},{64,96},{96,128},{128,160},{160,192},{192,224},{224... | collective-permute-start | bytes 417800 | tf_op jit(solution)/shard_map/ppermute | solution.py:318
  27.6 11.2 %all-gather = bf16[2112,128]{1,0:T(8,128)(2,1)S(1)} all-gather(bf16[528,128]{1,0:T(8,128)(2,1)S(1)} %fusion.5), channel_id=2, replica_groups=mesh['z'=16,'y'=4,'x'=4,'c'=2] {'y'}, dimensions={0}, use_global_device_ids=true | all-gather | bytes 675840 | tf_op jit(solution)/shard_map/all_gather | solution.py:332
  38.9 4.8 %collective-permute-start.9 = (bf16[272,256]{1,0:T(8,128)(2,1)}, bf16[272,256]{1,0:T(8,128)(2,1)S(1)}, u32[]{:S(2)}, u32[]{:S(2)}) collective-permute-start(bf16[272,256]{1,0:T(8,128)(2,1)} %collective-permute-done.8.refs_15_), channel_id=1, source_target_pairs={{0,480},{32,0},{64,32},{96,64},{128,96},{160,128},{192,160},{224,1... | collective-permute-start | bytes 417800 | tf_op jit(solution)/shard_map/ppermute | solution.py:321
  43.8 1.9 %collective-permute-start.2 = (bf16[272,256]{1,0:T(8,128)(2,1)S(1)}, bf16[272,256]{1,0:T(8,128)(2,1)S(1)}, u32[]{:S(2)}, u32[]{:S(2)}) collective-permute-start(bf16[272,256]{1,0:T(8,128)(2,1)S(1)} %collective-permute-done.1.refs_2_), channel_id=1, source_target_pairs={{0,32},{32,64},{64,96},{96,128},{128,160},{160,192},{192,224},{224... | collective-permute-start | bytes 417800 | tf_op jit(solution)/shard_map/ppermute | solution.py:318
  45.7 0.1 convert_reduce_fusion
  45.9 0.2 collective-permute-done.9.refs_14_
  46.1 4.9 %collective-permute-start.10 = (bf16[272,256]{1,0:T(8,128)(2,1)S(1)}, bf16[272,256]{1,0:T(8,128)(2,1)S(1)}, u32[]{:S(2)}, u32[]{:S(2)}) collective-permute-start(bf16[272,256]{1,0:T(8,128)(2,1)S(1)} %collective-permute-done.9.refs_14_), channel_id=1, source_target_pairs={{0,480},{32,0},{64,32},{96,64},{128,96},{160,128},{192,160},{224,1... | collective-permute-start | bytes 417800 | tf_op jit(solution)/shard_map/ppermute | solution.py:321
  51.0 1.9 %collective-permute-start.3 = (bf16[272,256]{1,0:T(8,128)(2,1)S(1)}, bf16[272,256]{1,0:T(8,128)(2,1)S(1)}, u32[]{:S(2)}, u32[]{:S(2)}) collective-permute-start(bf16[272,256]{1,0:T(8,128)(2,1)S(1)} %collective-permute-done.2.refs_3_), channel_id=1, source_target_pairs={{0,32},{32,64},{64,96},{96,128},{128,160},{160,192},{192,224},{224... | collective-permute-start | bytes 417800 | tf_op jit(solution)/shard_map/ppermute | solution.py:318
  53.0 4.9 %collective-permute-start.11 = (bf16[272,256]{1,0:T(8,128)(2,1)S(1)}, bf16[272,256]{1,0:T(8,128)(2,1)S(1)}, u32[]{:S(2)}, u32[]{:S(2)}) collective-permute-start(bf16[272,256]{1,0:T(8,128)(2,1)S(1)} %collective-permute-done.10.refs_13_), channel_id=1, source_target_pairs={{0,480},{32,0},{64,32},{96,64},{128,96},{160,128},{192,160},{224,1... | collective-permute-start | bytes 417800 | tf_op jit(solution)/shard_map/ppermute | solution.py:321
  58.0 1.9 %collective-permute-start.4 = (bf16[272,256]{1,0:T(8,128)(2,1)S(1)}, bf16[272,256]{1,0:T(8,128)(2,1)}, u32[]{:S(2)}, u32[]{:S(2)}) collective-permute-start(bf16[272,256]{1,0:T(8,128)(2,1)S(1)} %collective-permute-done.3.refs_4_), channel_id=1, source_target_pairs={{0,32},{32,64},{64,96},{96,128},{128,160},{160,192},{192,224},{224... | collective-permute-start | bytes 417800 | tf_op jit(solution)/shard_map/ppermute | solution.py:318
  59.9 0.1 convolution_convert_fusion
  60.3 0.6 select_reduce_fusion
  60.9 4.6 %collective-permute-start.12 = (bf16[272,256]{1,0:T(8,128)(2,1)S(1)}, bf16[272,256]{1,0:T(8,128)(2,1)S(1)}, u32[]{:S(2)}, u32[]{:S(2)}) collective-permute-start(bf16[272,256]{1,0:T(8,128)(2,1)S(1)} %collective-permute-done.11.refs_12_), channel_id=1, source_target_pairs={{0,480},{32,0},{64,32},{96,64},{128,96},{160,128},{192,160},{224,1... | collective-permute-start | bytes 417800 | tf_op jit(solution)/shard_map/ppermute | solution.py:321
  65.5 1.9 %collective-permute-start.5 = (bf16[272,256]{1,0:T(8,128)(2,1)}, bf16[272,256]{1,0:T(8,128)(2,1)S(1)}, u32[]{:S(2)}, u32[]{:S(2)}) collective-permute-start(bf16[272,256]{1,0:T(8,128)(2,1)} %collective-permute-done.4.refs_5_), channel_id=1, source_target_pairs={{0,32},{32,64},{64,96},{96,128},{128,160},{160,192},{192,224},{224... | collective-permute-start | bytes 417800 | tf_op jit(solution)/shard_map/ppermute | solution.py:318
  67.5 0.6 copy-done.10
  68.1 5.0 %collective-permute-start.13 = (bf16[272,256]{1,0:T(8,128)(2,1)S(1)}, bf16[272,256]{1,0:T(8,128)(2,1)}, u32[]{:S(2)}, u32[]{:S(2)}) collective-permute-start(bf16[272,256]{1,0:T(8,128)(2,1)S(1)} %collective-permute-done.12.refs_11_), channel_id=1, source_target_pairs={{0,480},{32,0},{64,32},{96,64},{128,96},{160,128},{192,160},{224,1... | collective-permute-start | bytes 417800 | tf_op jit(solution)/shard_map/ppermute | solution.py:321
  73.1 1.9 %collective-permute-start.6 = (bf16[272,256]{1,0:T(8,128)(2,1)S(1)}, bf16[272,256]{1,0:T(8,128)(2,1)}, u32[]{:S(2)}, u32[]{:S(2)}) collective-permute-start(bf16[272,256]{1,0:T(8,128)(2,1)S(1)} %collective-permute-done.5.refs_6_), channel_id=1, source_target_pairs={{0,32},{32,64},{64,96},{96,128},{128,160},{160,192},{192,224},{224... | collective-permute-start | bytes 417800 | tf_op jit(solution)/shard_map/ppermute | solution.py:318
  75.1 5.1 %collective-permute-start.14 = (bf16[272,256]{1,0:T(8,128)(2,1)}, bf16[272,256]{1,0:T(8,128)(2,1)}, u32[]{:S(2)}, u32[]{:S(2)}) collective-permute-start(bf16[272,256]{1,0:T(8,128)(2,1)} %collective-permute-done.13.refs_10_), channel_id=1, source_target_pairs={{0,480},{32,0},{64,32},{96,64},{128,96},{160,128},{192,160},{224,1... | collective-permute-start | bytes 417800 | tf_op jit(solution)/shard_map/ppermute | solution.py:321
  80.3 1.9 %collective-permute-start.7 = (bf16[272,256]{1,0:T(8,128)(2,1)}, bf16[272,256]{1,0:T(8,128)(2,1)}, u32[]{:S(2)}, u32[]{:S(2)}) collective-permute-start(bf16[272,256]{1,0:T(8,128)(2,1)} %collective-permute-done.6.refs_7_), channel_id=1, source_target_pairs={{0,32},{32,64},{64,96},{96,128},{128,160},{160,192},{192,224},{224... | collective-permute-start | bytes 417800 | tf_op jit(solution)/shard_map/ppermute | solution.py:318
  82.2 0.8 slice.43
  83.1 0.7 log.8.bias_ref
  83.7 0.7 sub.56.ids_ref
  84.4 0.7 pad_add_fusion.meta_ref
  85.0 3.8 %collective-permute-done.7.refs_8_ = bf16[272,256]{1,0:T(8,128)(2,1)} collective-permute-done((bf16[272,256]{1,0:T(8,128)(2,1)}, bf16[272,256]{1,0:T(8,128)(2,1)}, u32[]{:S(2)}, u32[]{:S(2)}) %collective-permute-start.7) | collective-permute-done | bytes 139296 | tf_op jit(solution)/shard_map/ppermute | solution.py:318
  88.8 9.4 %attend.1 = bf16[8,272,256]{2,1,0:T(8,128)(2,1)} custom-call(s32[6]{0:T(128)} %pad_add_fusion.meta_ref, s32[512]{0:T(512)} %sub.56.ids_ref, f32[512]{0:T(512)} %log.8.bias_ref, bf16[2048,128]{1,0:T(8,128)(2,1)} %bitcast.49, bf16[272,256]{1,0:T(8,128)(2,1)} %maximum_maximum_fusion.refs_0_, bf16[272,256]{1,0:T(8,128)(2,1)} %collective-permute-done.refs_1_, ...), custom_call_target="tpu_custom_call" | custom-call | tf_op jit(solution)/shard_map/attend/pallas_call | solution.py:185
  98.2 12.3 %all-to-all-start = ((bf16[8,272,256]{2,1,0:T(8,128)(2,1)}), bf16[8,272,256]{2,1,0:T(8,128)(2,1)S(1)}, u32[]{:S(2)}, u32[]{:S(2)}) async-start(bf16[8,272,256]{2,1,0:T(8,128)(2,1)} %attend.1), calls=%async_computation | async-start | bytes 2228224 | tf_op jit(solution)/shard_map/all_to_all | solution.py:360
  110.5 1.1 fusion.2
  111.6 0.7 copy.61.gate_ref
  112.4 13.8 %all-to-all-done.got_ref = bf16[8,272,256]{2,1,0:T(8,128)(2,1)S(1)} async-done(((bf16[8,272,256]{2,1,0:T(8,128)(2,1)}), bf16[8,272,256]{2,1,0:T(8,128)(2,1)S(1)}, u32[]{:S(2)}, u32[]{:S(2)}) %all-to-all-start) | async-done | bytes 1114144 | tf_op jit(solution)/shard_map/all_to_all | solution.py:360
  126.2 1.0 copy-done.1
  127.2 4.3 %merge.1 = (bf16[128,2048]{1,0:T(8,128)(2,1)}, f32[2,2,256]{2,1,0:T(2,128)}) custom-call(s32[1]{0:T(128)} %bitcast.1.meta_ref, bf16[8,272,256]{2,1,0:T(8,128)(2,1)} %copy-done.1, f32[128,8]{1,0:T(8,128)} %copy.61.gate_ref, bf16[256,2048]{1,0:T(8,128)(2,1)} %own_ref.1, bf16[256,2048]{1,0:T(8,128)(2,1)} %collective-permute-done.15.other_ref), custom_call_target="tpu_custom_call" | custom-call | tf_op jit(solution)/shard_map/merge/pallas_call | solution.py:251
  131.5 4.0 %all-to-all-start.1 = ((bf16[4,32,2048]{2,1,0:T(8,128)(2,1)}), bf16[4,32,2048]{2,1,0:T(8,128)(2,1)S(1)}, u32[]{:S(2)}, u32[]{:S(2)}) async-start(bf16[4,32,2048]{2,1,0:T(8,128)(2,1)} %bitcast.53), calls=%async_computation.1 | async-start | bytes 1048576 | tf_op jit(solution)/shard_map/all_to_all | solution.py:366
  135.5 0.7 constant_dynamic-slice_fusion
  136.3 0.7 reshape.155
  136.9 6.6 %all-to-all-done.1 = bf16[4,32,2048]{2,1,0:T(8,128)(2,1)S(1)} async-done(((bf16[4,32,2048]{2,1,0:T(8,128)(2,1)}), bf16[4,32,2048]{2,1,0:T(8,128)(2,1)S(1)}, u32[]{:S(2)}, u32[]{:S(2)}) %all-to-all-start.1) | async-done | bytes 524320 | tf_op jit(solution)/shard_map/all_to_all | solution.py:366
  143.5 0.7 reduce_sum.72
  (71 shorter events, 1.6 us)
Async XLA Ops:
  0.6 1.4 copy-start
  0.6 3.6 %copy-start.12 = (f32[256,64]{1,0:T(8,128)S(1)}, f32[256,64]{1,0:T(8,128)}, u32[]{:S(2)}) copy-start(f32[256,64]{1,0:T(8,128)} %constant.129.clone) | copy-start | bytes 196612
  0.7 3.5 %copy-start.13 = (f32[256,64]{1,0:T(8,128)S(1)}, f32[256,64]{1,0:T(8,128)}, u32[]{:S(2)}) copy-start(f32[256,64]{1,0:T(8,128)} %constant.142) | copy-start | bytes 196612
  4.3 16.9 %copy-start.3 = (bf16[256,2048]{1,0:T(8,128)(2,1)S(1)}, bf16[256,2048]{1,0:T(8,128)(2,1)}, u32[]{:S(2)}) copy-start(bf16[256,2048]{1,0:T(8,128)(2,1)} %own_ref.1) | copy-start | bytes 3145732
  5.0 1.6 %copy-start.14 = (f32[16,64]{1,0:T(8,128)S(1)}, f32[16,64]{1,0:T(8,128)}, u32[]{:S(2)}) copy-start(f32[16,64]{1,0:T(8,128)} %slice.39) | copy-start | bytes 12292
  5.0 19.3 %copy-start.2 = (bf16[2048,256]{1,0:T(8,128)(2,1)S(1)}, bf16[2048,256]{1,0:T(8,128)(2,1)}, u32[]{:S(2)}) copy-start(bf16[2048,256]{1,0:T(8,128)(2,1)} %param.18) | copy-start | bytes 3145732
  7.4 18.3 %collective-permute-start = (bf16[272,256]{1,0:T(8,128)(2,1)}, bf16[272,256]{1,0:T(8,128)(2,1)}, u32[]{:S(2)}, u32[]{:S(2)}) collective-permute-start(bf16[272,256]{1,0:T(8,128)(2,1)} %maximum_maximum_fusion.refs_0_), channel_id=1, source_target_pairs={{0,32},{32,64},{64,96},{96,128},{128,160},{160,192},{192,224},{224... | collective-permute-start | bytes 417800 | tf_op jit(solution)/shard_map/ppermute | solution.py:318
  11.8 27.2 %collective-permute-start.8 = (bf16[272,256]{1,0:T(8,128)(2,1)}, bf16[272,256]{1,0:T(8,128)(2,1)}, u32[]{:S(2)}, u32[]{:S(2)}) collective-permute-start(bf16[272,256]{1,0:T(8,128)(2,1)} %maximum_maximum_fusion.refs_0_), channel_id=1, source_target_pairs={{0,480},{32,0},{64,32},{96,64},{128,96},{160,128},{192,160},{224,1... | collective-permute-start | bytes 417800 | tf_op jit(solution)/shard_map/ppermute | solution.py:321
  21.3 91.1 %collective-permute-start.15 = (bf16[256,2048]{1,0:T(8,128)(2,1)S(1)}, bf16[256,2048]{1,0:T(8,128)(2,1)}, u32[]{:S(2)}, u32[]{:S(2)}) collective-permute-start(bf16[256,2048]{1,0:T(8,128)(2,1)S(1)} %copy-done.3), channel_id=1, source_target_pairs={{0,1},{1,0},{2,3},{3,2},{4,5},{5,4},{6,7},{7,6},{8,9},{9,8},{10,11... | collective-permute-start | bytes 3145736 | tf_op jit(solution)/shard_map/ppermute | solution.py:324
  24.9 0.7 copy-start.16
  24.9 35.0 %copy-start.15 = (bf16[64,64]{1,0:T(8,128)(2,1)S(1)}, bf16[64,64]{1,0:T(8,128)(2,1)}, u32[]{:S(2)}) copy-start(bf16[64,64]{1,0:T(8,128)(2,1)} %constant.203) | copy-start | bytes 24580
  25.0 35.2 %copy-start.17 = (s32[64]{0:T(128)S(1)}, s32[64]{0:T(128)}, u32[]{:S(2)}) copy-start(s32[64]{0:T(128)} %constant.141) | copy-start | bytes 772
  25.7 18.0 %collective-permute-start.1 = (bf16[272,256]{1,0:T(8,128)(2,1)}, bf16[272,256]{1,0:T(8,128)(2,1)S(1)}, u32[]{:S(2)}, u32[]{:S(2)}) collective-permute-start(bf16[272,256]{1,0:T(8,128)(2,1)} %collective-permute-done.refs_1_), channel_id=1, source_target_pairs={{0,32},{32,64},{64,96},{96,128},{128,160},{160,192},{192,224},{224... | collective-permute-start | bytes 417800 | tf_op jit(solution)/shard_map/ppermute | solution.py:318
  38.9 7.2 %collective-permute-start.9 = (bf16[272,256]{1,0:T(8,128)(2,1)}, bf16[272,256]{1,0:T(8,128)(2,1)S(1)}, u32[]{:S(2)}, u32[]{:S(2)}) collective-permute-start(bf16[272,256]{1,0:T(8,128)(2,1)} %collective-permute-done.8.refs_15_), channel_id=1, source_target_pairs={{0,480},{32,0},{64,32},{96,64},{128,96},{160,128},{192,160},{224,1... | collective-permute-start | bytes 417800 | tf_op jit(solution)/shard_map/ppermute | solution.py:321
  43.8 45.0 %copy-start.4 = (bf16[272,256]{1,0:T(8,128)(2,1)}, bf16[272,256]{1,0:T(8,128)(2,1)S(1)}, u32[]{:S(2)}) copy-start(bf16[272,256]{1,0:T(8,128)(2,1)S(1)} %collective-permute-done.1.refs_2_) | copy-start | bytes 417796
  43.8 7.2 %collective-permute-start.2 = (bf16[272,256]{1,0:T(8,128)(2,1)S(1)}, bf16[272,256]{1,0:T(8,128)(2,1)S(1)}, u32[]{:S(2)}, u32[]{:S(2)}) collective-permute-start(bf16[272,256]{1,0:T(8,128)(2,1)S(1)} %collective-permute-done.1.refs_2_), channel_id=1, source_target_pairs={{0,32},{32,64},{64,96},{96,128},{128,160},{160,192},{192,224},{224... | collective-permute-start | bytes 417800 | tf_op jit(solution)/shard_map/ppermute | solution.py:318
  46.1 42.7 %copy-start.5 = (bf16[272,256]{1,0:T(8,128)(2,1)}, bf16[272,256]{1,0:T(8,128)(2,1)S(1)}, u32[]{:S(2)}) copy-start(bf16[272,256]{1,0:T(8,128)(2,1)S(1)} %collective-permute-done.9.refs_14_) | copy-start | bytes 417796
  46.1 7.0 %collective-permute-start.10 = (bf16[272,256]{1,0:T(8,128)(2,1)S(1)}, bf16[272,256]{1,0:T(8,128)(2,1)S(1)}, u32[]{:S(2)}, u32[]{:S(2)}) collective-permute-start(bf16[272,256]{1,0:T(8,128)(2,1)S(1)} %collective-permute-done.9.refs_14_), channel_id=1, source_target_pairs={{0,480},{32,0},{64,32},{96,64},{128,96},{160,128},{192,160},{224,1... | collective-permute-start | bytes 417800 | tf_op jit(solution)/shard_map/ppermute | solution.py:321
  51.0 37.8 %copy-start.6 = (bf16[272,256]{1,0:T(8,128)(2,1)}, bf16[272,256]{1,0:T(8,128)(2,1)S(1)}, u32[]{:S(2)}) copy-start(bf16[272,256]{1,0:T(8,128)(2,1)S(1)} %collective-permute-done.2.refs_3_) | copy-start | bytes 417796
  51.0 7.0 %collective-permute-start.3 = (bf16[272,256]{1,0:T(8,128)(2,1)S(1)}, bf16[272,256]{1,0:T(8,128)(2,1)S(1)}, u32[]{:S(2)}, u32[]{:S(2)}) collective-permute-start(bf16[272,256]{1,0:T(8,128)(2,1)S(1)} %collective-permute-done.2.refs_3_), channel_id=1, source_target_pairs={{0,32},{32,64},{64,96},{96,128},{128,160},{160,192},{192,224},{224... | collective-permute-start | bytes 417800 | tf_op jit(solution)/shard_map/ppermute | solution.py:318
  53.0 35.8 %copy-start.7 = (bf16[272,256]{1,0:T(8,128)(2,1)}, bf16[272,256]{1,0:T(8,128)(2,1)S(1)}, u32[]{:S(2)}) copy-start(bf16[272,256]{1,0:T(8,128)(2,1)S(1)} %collective-permute-done.10.refs_13_) | copy-start | bytes 417796
  53.0 7.8 %collective-permute-start.11 = (bf16[272,256]{1,0:T(8,128)(2,1)S(1)}, bf16[272,256]{1,0:T(8,128)(2,1)S(1)}, u32[]{:S(2)}, u32[]{:S(2)}) collective-permute-start(bf16[272,256]{1,0:T(8,128)(2,1)S(1)} %collective-permute-done.10.refs_13_), channel_id=1, source_target_pairs={{0,480},{32,0},{64,32},{96,64},{128,96},{160,128},{192,160},{224,1... | collective-permute-start | bytes 417800 | tf_op jit(solution)/shard_map/ppermute | solution.py:321
  58.0 30.8 %copy-start.8 = (bf16[272,256]{1,0:T(8,128)(2,1)}, bf16[272,256]{1,0:T(8,128)(2,1)S(1)}, u32[]{:S(2)}) copy-start(bf16[272,256]{1,0:T(8,128)(2,1)S(1)} %collective-permute-done.3.refs_4_) | copy-start | bytes 417796
  58.0 7.5 %collective-permute-start.4 = (bf16[272,256]{1,0:T(8,128)(2,1)S(1)}, bf16[272,256]{1,0:T(8,128)(2,1)}, u32[]{:S(2)}, u32[]{:S(2)}) collective-permute-start(bf16[272,256]{1,0:T(8,128)(2,1)S(1)} %collective-permute-done.3.refs_4_), channel_id=1, source_target_pairs={{0,32},{32,64},{64,96},{96,128},{128,160},{160,192},{192,224},{224... | collective-permute-start | bytes 417800 | tf_op jit(solution)/shard_map/ppermute | solution.py:318
  60.9 27.9 %copy-start.9 = (bf16[272,256]{1,0:T(8,128)(2,1)}, bf16[272,256]{1,0:T(8,128)(2,1)S(1)}, u32[]{:S(2)}) copy-start(bf16[272,256]{1,0:T(8,128)(2,1)S(1)} %collective-permute-done.11.refs_12_) | copy-start | bytes 417796
  60.9 6.6 %collective-permute-start.12 = (bf16[272,256]{1,0:T(8,128)(2,1)S(1)}, bf16[272,256]{1,0:T(8,128)(2,1)S(1)}, u32[]{:S(2)}, u32[]{:S(2)}) collective-permute-start(bf16[272,256]{1,0:T(8,128)(2,1)S(1)} %collective-permute-done.11.refs_12_), channel_id=1, source_target_pairs={{0,480},{32,0},{64,32},{96,64},{128,96},{160,128},{192,160},{224,1... | collective-permute-start | bytes 417800 | tf_op jit(solution)/shard_map/ppermute | solution.py:321
  65.5 7.6 %collective-permute-start.5 = (bf16[272,256]{1,0:T(8,128)(2,1)}, bf16[272,256]{1,0:T(8,128)(2,1)S(1)}, u32[]{:S(2)}, u32[]{:S(2)}) collective-permute-start(bf16[272,256]{1,0:T(8,128)(2,1)} %collective-permute-done.4.refs_5_), channel_id=1, source_target_pairs={{0,32},{32,64},{64,96},{96,128},{128,160},{160,192},{192,224},{224... | collective-permute-start | bytes 417800 | tf_op jit(solution)/shard_map/ppermute | solution.py:318
  67.5 0.6 copy-start.10
  68.1 7.0 %collective-permute-start.13 = (bf16[272,256]{1,0:T(8,128)(2,1)S(1)}, bf16[272,256]{1,0:T(8,128)(2,1)}, u32[]{:S(2)}, u32[]{:S(2)}) collective-permute-start(bf16[272,256]{1,0:T(8,128)(2,1)S(1)} %collective-permute-done.12.refs_11_), channel_id=1, source_target_pairs={{0,480},{32,0},{64,32},{96,64},{128,96},{160,128},{192,160},{224,1... | collective-permute-start | bytes 417800 | tf_op jit(solution)/shard_map/ppermute | solution.py:321
  73.1 2.0 %copy-start.11 = (bf16[272,256]{1,0:T(8,128)(2,1)}, bf16[272,256]{1,0:T(8,128)(2,1)S(1)}, u32[]{:S(2)}) copy-start(bf16[272,256]{1,0:T(8,128)(2,1)S(1)} %collective-permute-done.5.refs_6_) | copy-start | bytes 417796
  73.1 7.1 %collective-permute-start.6 = (bf16[272,256]{1,0:T(8,128)(2,1)S(1)}, bf16[272,256]{1,0:T(8,128)(2,1)}, u32[]{:S(2)}, u32[]{:S(2)}) collective-permute-start(bf16[272,256]{1,0:T(8,128)(2,1)S(1)} %collective-permute-done.5.refs_6_), channel_id=1, source_target_pairs={{0,32},{32,64},{64,96},{96,128},{128,160},{160,192},{192,224},{224... | collective-permute-start | bytes 417800 | tf_op jit(solution)/shard_map/ppermute | solution.py:318
  75.1 9.9 %collective-permute-start.14 = (bf16[272,256]{1,0:T(8,128)(2,1)}, bf16[272,256]{1,0:T(8,128)(2,1)}, u32[]{:S(2)}, u32[]{:S(2)}) collective-permute-start(bf16[272,256]{1,0:T(8,128)(2,1)} %collective-permute-done.13.refs_10_), channel_id=1, source_target_pairs={{0,480},{32,0},{64,32},{96,64},{128,96},{160,128},{192,160},{224,1... | collective-permute-start | bytes 417800 | tf_op jit(solution)/shard_map/ppermute | solution.py:321
  80.3 8.5 %collective-permute-start.7 = (bf16[272,256]{1,0:T(8,128)(2,1)}, bf16[272,256]{1,0:T(8,128)(2,1)}, u32[]{:S(2)}, u32[]{:S(2)}) collective-permute-start(bf16[272,256]{1,0:T(8,128)(2,1)} %collective-permute-done.6.refs_7_), channel_id=1, source_target_pairs={{0,32},{32,64},{64,96},{96,128},{128,160},{160,192},{192,224},{224... | collective-permute-start | bytes 417800 | tf_op jit(solution)/shard_map/ppermute | solution.py:318
  98.2 28.0 %all-to-all-start = ((bf16[8,272,256]{2,1,0:T(8,128)(2,1)}), bf16[8,272,256]{2,1,0:T(8,128)(2,1)S(1)}, u32[]{:S(2)}, u32[]{:S(2)}) async-start(bf16[8,272,256]{2,1,0:T(8,128)(2,1)} %attend.1), calls=%async_computation | async-start | bytes 2228224 | tf_op jit(solution)/shard_map/all_to_all | solution.py:360
  126.2 1.0 copy-start.1
  131.5 12.0 %all-to-all-start.1 = ((bf16[4,32,2048]{2,1,0:T(8,128)(2,1)}), bf16[4,32,2048]{2,1,0:T(8,128)(2,1)S(1)}, u32[]{:S(2)}, u32[]{:S(2)}) async-start(bf16[4,32,2048]{2,1,0:T(8,128)(2,1)} %bitcast.53), calls=%async_computation.1 | async-start | bytes 1048576 | tf_op jit(solution)/shard_map/all_to_all | solution.py:366

commit v3 on v2

--- a/solution.py
+++ b/solution.py
@@ -6,6 +6,7 @@
 from jax.experimental.pallas import tpu as pltpu
 from jax.sharding import Mesh
 from jax.sharding import PartitionSpec as P
+
 
 HEAD_SIZE = 128
 BLOCK = 64
@@ -16,7 +17,7 @@
 KV = ("z", "y")
 SPAN = 256
 STATS = 16
-PER_STEP = 8
+PER_STEP = 4
 POOLED = 16
 RING = 16
 LIST = 32
@@ -41,6 +42,89 @@
     return jnp.concatenate([front * cosines - back * sines, back * cosines + front * sines], -1)
 
 
+def project_kernel(
+    meta_ref, tok_ref, wk_ref, wv_ref, kmix_ref, vmix_ref, local_ref, span_ref, out_ref, k_ref, v_ref
+):
+    step = pl.program_id(0)
+
+    @pl.when(step == 0)
+    def _():
+        k_ref[...] = jnp.zeros_like(k_ref)
+        v_ref[...] = jnp.zeros_like(v_ref)
+
+    k_ref[...] += jnp.dot(tok_ref[...], wk_ref[...], preferred_element_type=jnp.float32)
+    v_ref[...] += jnp.dot(tok_ref[...], wv_ref[...], preferred_element_type=jnp.float32)
+
+    @pl.when(step == pl.num_programs(0) - 1)
+    def _():
+        own = meta_ref[0]
+        group = meta_ref[1]
+        cos_s = span_ref[0, pl.ds(own, 1), :]
+        sin_s = span_ref[1, pl.ds(own, 1), :]
+
+        def rotated(value, cos_l, sin_l):
+            cosines = cos_l * cos_s - sin_l * sin_s
+            sines = sin_l * cos_s + cos_l * sin_s
+            sign = lax.broadcasted_iota(jnp.int32, (1, HEAD_SIZE), 1) < HEAD_SIZE // 2
+            turned = pltpu.roll(value, HEAD_SIZE // 2, 1)
+            return value * cosines + jnp.where(sign, -turned, turned) * sines
+
+        def pooled(value, mix_ref):
+            lane = lax.broadcasted_iota(jnp.int32, (POOL_STRIDE, 8), 1)
+            mix = jnp.sum(jnp.where(lane == group, mix_ref[...], 0.0), axis=1, keepdims=True)
+            mixed = value.reshape(POOLED, POOL_STRIDE, HEAD_SIZE) * mix[None]
+            return jnp.sum(mixed, axis=1)
+
+        keys = k_ref[...]
+        values = v_ref[...]
+        out_ref[:SPAN, :HEAD_SIZE] = rotated(
+            keys, local_ref[0, :SPAN], local_ref[1, :SPAN]
+        ).astype(jnp.bfloat16)
+        out_ref[:SPAN, HEAD_SIZE:] = values.astype(jnp.bfloat16)
+        out_ref[SPAN:, :HEAD_SIZE] = rotated(
+            pooled(keys, kmix_ref), local_ref[0, SPAN:], local_ref[1, SPAN:]
+        ).astype(jnp.bfloat16)
+        out_ref[SPAN:, HEAD_SIZE:] = pooled(values, vmix_ref).astype(jnp.bfloat16)
+
+
+def project(meta, tokens, key_matrix, value_matrix, key_mix, value_mix):
+    half = HEAD_SIZE // 2
+    inverse = THETA ** (-np.arange(half, dtype=np.float64) / half)
+    inverse = np.concatenate([inverse, inverse])
+    offsets = np.concatenate(
+        [np.arange(SPAN), np.arange(POOLED) * POOL_STRIDE + POOL_STRIDE - 1]
+    ).astype(np.float64)
+    local = offsets[:, None] * inverse[None, :]
+    spans = np.arange(64, dtype=np.float64)[:, None] * SPAN * inverse[None, :]
+    local = jnp.asarray(np.stack([np.cos(local), np.sin(local)]), jnp.float32)
+    spans = jnp.asarray(np.stack([np.cos(spans), np.sin(spans)]), jnp.float32)
+    depth = 512
+    return pl.pallas_call(
+        project_kernel,
+        grid_spec=pltpu.PrefetchScalarGridSpec(
+            num_scalar_prefetch=1,
+            grid=(tokens.shape[1] // depth,),
+            in_specs=[
+                pl.BlockSpec((SPAN, depth), lambda i, *_: (0, i)),
+                pl.BlockSpec((depth, HEAD_SIZE), lambda i, *_: (i, 0)),
+                pl.BlockSpec((depth, HEAD_SIZE), lambda i, *_: (i, 0)),
+                pl.BlockSpec((POOL_STRIDE, 8), lambda i, *_: (0, 0)),
+                pl.BlockSpec((POOL_STRIDE, 8), lambda i, *_: (0, 0)),
+                pl.BlockSpec((2, SPAN + POOLED, HEAD_SIZE), lambda i, *_: (0, 0, 0)),
+                pl.BlockSpec((2, 64, HEAD_SIZE), lambda i, *_: (0, 0, 0)),
+            ],
+            out_specs=pl.BlockSpec((SPAN + POOLED, 2 * HEAD_SIZE), lambda i, *_: (0, 0)),
+            scratch_shapes=[
+                pltpu.VMEM((SPAN, HEAD_SIZE), jnp.float32),
+                pltpu.VMEM((SPAN, HEAD_SIZE), jnp.float32),
+            ],
+        ),
+        out_shape=jax.ShapeDtypeStruct((SPAN + POOLED, 2 * HEAD_SIZE), jnp.bfloat16),
+        compiler_params=pltpu.CompilerParams(vmem_limit_bytes=12 << 20),
+        name="project",
+    )(meta, tokens, key_matrix, value_matrix, key_mix, value_mix, local, spans)
+
+
 def split_three(value):
     high = value.astype(jnp.bfloat16).astype(jnp.float32)
     rest = value - high
@@ -48,11 +132,13 @@
     return [high, middle, rest - middle]
 
 
-def attend_kernel(meta_ref, ids_ref, bias_ref, q_ref, *refs):
-    chunk_refs = refs[:RING]
-    out_ref, kv_ref, pool_ref, acc_ref, m_ref, l_ref, lse_ref = refs[RING:]
+def attend_kernel(meta_ref, ids_ref, bias_ref, *refs):
+    q_refs = refs[:4]
+    chunk_refs = refs[4 : 4 + RING]
+    out_ref, kv_ref, pool_ref, acc_ref, m_ref, l_ref, lse_ref = refs[4 + RING :]
     z = meta_ref[0]
     y = meta_ref[1]
+    owners = [(y + peer) % 4 for peer in range(4)]
     for o in range(RING):
         kv_ref[o * SPAN : (o + 1) * SPAN, :] = chunk_refs[o][:SPAN, :]
         pool_ref[o * POOLED : (o + 1) * POOLED, :] = chunk_refs[o][SPAN:, :]
@@ -66,40 +152,51 @@
             for head in range(2):
                 at = head * BLOCK + half * 32
                 out_ref[
-                    peer * 2 + half,
+                    owners[peer] * 2 + half,
                     first + qb * 32 : first + (qb + 1) * 32,
                     head * HEAD_SIZE : (head + 1) * HEAD_SIZE,
                 ] = out[at : at + 32]
 
-    pool_row = lax.broadcasted_iota(jnp.int32, (SPAN, 1), 0)
-    offset = pool_row // POOLED
-    pool_at = ((z - offset) * 4 + y) * POOLED + pool_row % POOLED
+    col = lax.broadcasted_iota(jnp.int32, (1, RING * POOLED), 1)
+    offset = col // POOLED
+    pool_at = ((z - offset) * 4 + y) * POOLED + col % POOLED
     pool_end = pool_at * POOL_STRIDE + POOL_STRIDE - 1
     pool_end = jnp.where(offset > z, 1 << 30, jnp.where(pool_at == 0, 0, pool_end))
+    q_row = lax.broadcasted_iota(jnp.int32, (512, 1), 0)
+    q_row = (q_row // 128) * BLOCK + q_row % BLOCK
+    eye = lax.broadcasted_iota(jnp.int32, (128, 128), 0) == lax.broadcasted_iota(
+        jnp.int32, (128, 128), 1
+    )
     for peer in range(4):
+        s = lax.dot_general(
+            q_refs[peer][:512, :],
+            pool_ref[:, :HEAD_SIZE],
+            (((1,), (1,)), ((), ())),
+            preferred_element_type=jnp.float32,
+        )
+        s = jnp.where(pool_end <= (z * 4 + owners[peer]) * SPAN + q_row, s * SCALE, NEGATIVE)
+        m = jnp.maximum(jnp.max(s, axis=1, keepdims=True), FLOOR)
+        p = jnp.exp(s - m)
+        total = jnp.sum(p, axis=1, keepdims=True)
+        acc = jnp.dot(
+            p.astype(jnp.bfloat16), pool_ref[:, HEAD_SIZE:], preferred_element_type=jnp.float32
+        )
+        some = total > 0.0
+        total = jnp.where(some, total, 1.0)
+        lse = jnp.where(some, m + jnp.log(total), FLOOR)
+        out = (acc / total).astype(jnp.bfloat16)
         for qb in range(4):
-            g = peer * 4 + qb
-            qpos = (z * 4 + peer) * SPAN + qb * BLOCK + lane
-            s = lax.dot_general(
-                pool_ref[:, :HEAD_SIZE],
-                q_ref[g * 128 : (g + 1) * 128, :],
-                (((1,), (1,)), ((), ())),
-                preferred_element_type=jnp.float32,
-            )
-            s = jnp.where(pool_end <= qpos, s * SCALE, NEGATIVE)
-            m = jnp.maximum(jnp.max(s, axis=0, keepdims=True), FLOOR)
-            p = jnp.exp(s - m)
-            total = jnp.sum(p, axis=0, keepdims=True)
-            acc = lax.dot_general(
-                pool_ref[:, HEAD_SIZE:],
-                p.astype(jnp.bfloat16),
-                (((0,), (0,)), ((), ())),
-                preferred_element_type=jnp.float32,
-            )
-            some = total > 0.0
-            total = jnp.where(some, total, 1.0)
-            store(peer, qb, 128, acc / total)
-            lse_ref[16 + g : 17 + g, :] = jnp.where(some, m + jnp.log(total), FLOOR)
+            for head in range(2):
+                for half in range(2):
+                    at = qb * 128 + head * BLOCK + half * 32
+                    out_ref[
+                        owners[peer] * 2 + half,
+                        128 + qb * 32 : 128 + (qb + 1) * 32,
+                        head * HEAD_SIZE : (head + 1) * HEAD_SIZE,
+                    ] = out[at : at + 32]
+            spread = jnp.where(eye, lse[qb * 128 : (qb + 1) * 128], 0.0)
+            g = 16 + peer * 4 + qb
+            lse_ref[g : g + 1, :] = jnp.sum(spread, axis=0, keepdims=True)
 
     for peer in range(4):
         for qb in range(4):
@@ -110,11 +207,10 @@
         def group(k, carry, peer=peer):
             for qb in range(4):
                 g = peer * 4 + qb
-                qpos = (z * 4 + peer) * SPAN + qb * BLOCK + lane
+                qpos = (z * 4 + owners[peer]) * SPAN + qb * BLOCK + lane
                 keys, values, bases, biases = [], [], [], []
                 for e in range(PER_STEP):
-                    at = g * LIST + k * PER_STEP + e
-                    idx = ids_ref[at]
+                    idx = ids_ref[g, k * PER_STEP + e]
                     none = idx < 0
                     safe = jnp.where(none, 0, idx)
                     first = pl.multiple_of(safe * BLOCK, BLOCK)
@@ -122,12 +218,12 @@
                     values.append(kv_ref[pl.ds(first, BLOCK), HEAD_SIZE:])
                     base = ((z - safe // 4) * 4 + y) * SPAN + (safe % 4) * BLOCK
                     bases.append(jnp.where(none, 1 << 30, base))
-                    biases.append(bias_ref[at])
+                    biases.append(bias_ref[g, k * PER_STEP + e])
                 kg = jnp.concatenate(keys, 0)
                 vg = jnp.concatenate(values, 0)
                 s = lax.dot_general(
                     kg,
-                    q_ref[g * 128 : (g + 1) * 128, :],
+                    q_refs[peer][qb * 128 : (qb + 1) * 128, :],
                     (((1,), (1,)), ((), ())),
                     preferred_element_type=jnp.float32,
                 )
@@ -177,7 +273,7 @@
         rows.append(jnp.zeros((STATS - 12, 2 * HEAD_SIZE), jnp.float32))
         block = jnp.concatenate(rows, 0).astype(jnp.bfloat16)
         for half in range(2):
-            out_ref[peer * 2 + half, SPAN : SPAN + STATS, :] = block
+            out_ref[owners[peer] * 2 + half, SPAN : SPAN + STATS, :] = block
 
 
 def attend(meta, ids, bias, queries, chunks):
@@ -187,7 +283,7 @@
         grid_spec=pltpu.PrefetchScalarGridSpec(
             num_scalar_prefetch=3,
             grid=(1,),
-            in_specs=[whole((2048, HEAD_SIZE))]
+            in_specs=[whole((528, HEAD_SIZE))] * 4
             + [whole((SPAN + POOLED, 2 * HEAD_SIZE))] * RING,
             out_specs=whole((8, SPAN + STATS, 2 * HEAD_SIZE)),
             scratch_shapes=[
@@ -200,8 +296,9 @@
             ],
         ),
         out_shape=jax.ShapeDtypeStruct((8, SPAN + STATS, 2 * HEAD_SIZE), jnp.bfloat16),
+        compiler_params=pltpu.CompilerParams(vmem_limit_bytes=20 << 20),
         name="attend",
-    )(meta, ids, bias, queries, *chunks)
+    )(meta, ids, bias, *queries, *chunks)
 
 
 def merge_kernel(meta_ref, got_ref, gate_ref, own_ref, other_ref, out_ref, log_ref, t_ref, att_ref):
@@ -269,8 +366,29 @@
             jax.ShapeDtypeStruct((128, width), jnp.bfloat16),
             jax.ShapeDtypeStruct((2, 2, 2 * HEAD_SIZE), jnp.float32),
         ],
+        compiler_params=pltpu.CompilerParams(vmem_limit_bytes=12 << 20),
         name="merge",
     )(meta, got, gates, own_weight, other_weight)
+
+
+def block_lists(near, z, y):
+    f32 = jnp.float32
+    near_chosen = jnp.stack([v[512] for v in near]).reshape(16, 32).astype(jnp.int32)
+    mine = (near_chosen // 4) % 4 == y
+    slot = ((z - near_chosen // 16) % RING) * 4 + near_chosen % 4
+    slot = jnp.where(mine, slot, -1)
+    counts = jnp.sum((slot[:, :, None] == np.arange(BLOCK)[None, None, :]).astype(jnp.int32), axis=1)
+    present = counts > 0
+    earlier = (np.arange(BLOCK)[:, None] < np.arange(BLOCK)[None, :]).astype(np.float32)
+    rank = jnp.dot(present.astype(f32), earlier).astype(jnp.int32)
+    hit = present[:, :, None] & (rank[:, :, None] == np.arange(LIST)[None, None, :])
+    ids = jnp.sum(jnp.where(hit, np.arange(1, BLOCK + 1)[None, :, None], 0), axis=1) - 1
+    times = jnp.sum(jnp.where(hit, counts[:, :, None], 0), axis=1)
+    bias = jnp.log(jnp.maximum(times, 1).astype(f32))
+    lengths = jnp.sum(present.astype(jnp.int32), axis=1)
+    steps = (jnp.max(lengths.reshape(4, 4), axis=1) + PER_STEP - 1) // PER_STEP
+    meta = jnp.concatenate([jnp.stack([z, y]).astype(jnp.int32), steps.astype(jnp.int32)])
+    return meta, ids, bias
 
 
 def shards(
@@ -291,62 +409,35 @@
     f32, bf16 = jnp.float32, jnp.bfloat16
 
     cosines, sines = rotary_tables(own, np.arange(SPAN))
-    key_projected = jnp.dot(tokens, key_matrix, preferred_element_type=f32)
-    value_projected = jnp.dot(tokens, value_matrix, preferred_element_type=f32)
-    keys = rotate(key_projected, cosines, sines).astype(bf16)
-    key_mix = lax.dynamic_slice_in_dim(key_pool_weight, group, 1, 1)
-    value_mix = lax.dynamic_slice_in_dim(value_pool_weight, group, 1, 1)
-    pooled_k = jnp.sum(key_projected.reshape(POOLED, POOL_STRIDE, HEAD_SIZE) * key_mix[None], axis=1)
-    pooled_v = jnp.sum(
-        value_projected.reshape(POOLED, POOL_STRIDE, HEAD_SIZE) * value_mix[None], axis=1
-    )
-    last = slice(POOL_STRIDE - 1, None, POOL_STRIDE)
-    pooled_k = rotate(pooled_k, cosines[last], sines[last])
-    chunk = jnp.concatenate(
-        [
-            jnp.concatenate([keys, value_projected.astype(bf16)], -1),
-            jnp.concatenate([pooled_k.astype(bf16), pooled_v.astype(bf16)], -1),
-        ],
-        0,
-    )
+    place = jnp.stack([own, group]).astype(jnp.int32)
+    chunk = project(place, tokens, key_matrix, value_matrix, key_pool_weight, value_pool_weight)
+    query_proj = jnp.dot(tokens, query_weight, preferred_element_type=f32)
+    query_proj = query_proj.reshape(SPAN, 2, HEAD_SIZE)
+    queries = rotate(query_proj, cosines[:, None, :], sines[:, None, :]).astype(bf16)
+    by_block = queries.reshape(4, BLOCK, 2, HEAD_SIZE).transpose(0, 2, 1, 3)
+    picks = jnp.pad(chosen.astype(bf16).reshape(1, 128), ((0, 15), (0, 0)))
+    sent = jnp.concatenate([by_block.reshape(512, HEAD_SIZE), picks], 0)
+
     ring_up = [(i, (i + 1) % RING) for i in range(RING)]
     ring_down = [(i, (i - 1) % RING) for i in range(RING)]
     chunks = [None] * RING
     chunks[0] = chunk
     up = down = chunk
+    near = [sent]
+
     for k in range(1, RING // 2 + 1):
         up = lax.ppermute(up, "z", ring_up)
         chunks[k] = up
         if k < RING // 2:
             down = lax.ppermute(down, "z", ring_down)
             chunks[RING - k] = down
-
-    other_weight = lax.ppermute(out_weight, "c", [(0, 1), (1, 0)])
-
-    query_proj = jnp.dot(tokens, query_weight, preferred_element_type=f32)
-    query_proj = query_proj.reshape(SPAN, 2, HEAD_SIZE)
-    queries = rotate(query_proj, cosines[:, None, :], sines[:, None, :]).astype(bf16)
-    by_block = queries.reshape(4, BLOCK, 2, HEAD_SIZE).transpose(0, 2, 1, 3)
-    picks = jnp.pad(chosen.astype(bf16).reshape(1, 128), ((0, 15), (0, 0)))
-    sent = jnp.concatenate([by_block.reshape(512, HEAD_SIZE), picks], 0)
-    near = lax.all_gather(sent, "y", axis=0, tiled=False)
-    near_queries = near[:, :512].reshape(2048, HEAD_SIZE)
-    near_chosen = near[:, 512].reshape(16, 32).astype(jnp.int32)
-
-    mine = (near_chosen // 4) % 4 == y
-    slot = ((z - near_chosen // 16) % RING) * 4 + near_chosen % 4
-    slot = jnp.where(mine, slot, -1)
-    counts = jnp.sum((slot[:, :, None] == np.arange(BLOCK)[None, None, :]).astype(jnp.int32), axis=1)
-    present = counts > 0
-    earlier = (np.arange(BLOCK)[:, None] < np.arange(BLOCK)[None, :]).astype(np.float32)
-    rank = jnp.dot(present.astype(f32), earlier).astype(jnp.int32)
-    hit = present[:, :, None] & (rank[:, :, None] == np.arange(LIST)[None, None, :])
-    ids = jnp.sum(jnp.where(hit, np.arange(1, BLOCK + 1)[None, :, None], 0), axis=1) - 1
-    times = jnp.sum(jnp.where(hit, counts[:, :, None], 0), axis=1)
-    bias = jnp.log(jnp.maximum(times, 1).astype(f32))
-    lengths = jnp.sum(present.astype(jnp.int32), axis=1)
-    steps = (jnp.max(lengths.reshape(4, 4), axis=1) + PER_STEP - 1) // PER_STEP
-    meta = jnp.concatenate([jnp.stack([z, y]).astype(jnp.int32), steps.astype(jnp.int32)])
+        if 1 <= k <= 3:
+            pairs = [(i, (i - k) % 4) for i in range(4)]
+            near.append(lax.ppermute(sent, "y", pairs))
+        if k == 4:
+            other_weight = lax.ppermute(out_weight, "c", [(0, 1), (1, 0)])
+
+    meta, ids, bias = block_lists(near, z, y)
 
     own_tokens = lax.dynamic_index_in_dim(
         tokens.reshape(4, 2, 32, -1), c, 1, keepdims=False
@@ -356,7 +447,7 @@
         jnp.einsum("td,bdh->tbh", own_tokens, gate_cols, preferred_element_type=f32)
     ).reshape(128, 8)
 
-    partial = attend(meta, ids.reshape(-1), bias.reshape(-1), near_queries, chunks)
+    partial = attend(meta, ids, bias, near, chunks)
     got = lax.all_to_all(partial, ("y", "c"), 0, 0, tiled=True)
     shares, log_all = merge(
         c.astype(jnp.int32).reshape(1), got, gates, out_weight, other_weight

time: 145 us -> 146 us (level)
  blocking collectives: 11.2 us -> 0 us
  starting transfers between devices: 75.7 us -> 84.1 us
  local copies, waits for them, and re-layouts: 9.54 us -> 13.7 us
  waiting for transfers between devices: 24.5 us -> 28.1 us
  matrix products: 4.79 us -> 1.75 us
    all_gather x1 -> x0, blocking collectives: 11.2 us -> none  [shards(): near = lax.all_gather(sent, 'y', axis=0, tiled=False)]
    unnamed x36 -> x38, local copies, waits for them, and re-layouts: 1.75 us -> 11.4 us
    ppermute x0 -> x3, starting transfers between devices: none -> 9.5 us  [shards(): near.append(lax.ppermute(sent, 'y', pairs))]
    dot_general x3 -> x1, matrix products: 3.16 us -> 0.12 us  [block_lists(): rank = jnp.dot(present.astype(f32), earlier).astype(jnp.int32)]
    all_to_all x1, starting transfers between devices: 12.3 us -> 9.67 us  [shards(): got = lax.all_to_all(partial, ('y', 'c'), 0, 0, tiled=True)]
    pallas_call x0 -> x1, Pallas kernels: none -> 2.04 us  [project(): pl.pallas_call(project_kernel, grid_spec=pltpu.PrefetchScalarGridSpec(num...]
    pallas_call x1, Pallas kernels: 9.4 us -> 7.45 us  [attend(): pl.pallas_call(attend_kernel, grid_spec=pltpu.PrefetchScalarGridSpec(num_...]
    ppermute x8, waiting for transfers between devices: 3.85 us -> 5.46 us  [shards(): up = lax.ppermute(up, 'z', ring_up)]
  transfers between devices with their start and end apart: 18 -> 21, of which waited for: 5 -> 7; matrix products, arithmetic and copies ran while one was open for 6% -> 4% of each run, Pallas kernels for 7% -> 5%
where the time goes in v3:
time: 146 us; the launch traced here: 144 us
  starting transfers between devices  84.1 us (58%)
  waiting for transfers between devices  28.1 us (19%)
  local copies, waits for them, and re-layouts  13.7 us (9%)
  Pallas kernels  13.4 us (9%)
  other arithmetic  2.3 us (2%)
  matrix products  1.75 us (1%)
    ppermute x7, starting transfers between devices, shards(): down = lax.ppermute(down, 'z', ring_down)  39.4 us
    ppermute x8, starting transfers between devices, shards(): up = lax.ppermute(up, 'z', ring_up)  17.8 us
    all_to_all x1, waiting for transfers between devices, shards(): got = lax.all_to_all(partial, ('y', 'c'), 0, 0, tiled=True)  14.4 us
    unnamed x38, local copies, waits for them, and re-layouts  11.4 us
    all_to_all x1, starting transfers between devices, shards(): got = lax.all_to_all(partial, ('y', 'c'), 0, 0, tiled=True)  9.67 us
    ppermute x3, starting transfers between devices, shards(): near.append(lax.ppermute(sent, 'y', pairs))  9.5 us
    pallas_call x1, Pallas kernels, attend(): pl.pallas_call(attend_kernel, grid_spec=pltpu.PrefetchScalarGridSpec(num_...  7.45 us
    all_to_all x1, waiting for transfers between devices, shards(): pieces = lax.all_to_all(shares.reshape(4, 32, -1), 'x', 0, 0, tiled=True)  7.3 us
  transfers between devices with their start and end apart: 21, of which 7 were waited for; matrix products, arithmetic and copies ran while one was open for 4% of the time, Pallas kernels for 5%

profile of v3, /device:TPU:1, one launch (start us, length us, event | category | flops | bytes accessed | tf_op | source)
XLA Modules:
  0.0 144.5 jit_solution(10861449232564725757)
XLA Ops:
  0.7 0.8 copy.37.kmix_ref
  1.5 0.8 copy.38.vmix_ref
  2.3 1.2 copy-done.1
  3.6 1.0 copy-done.3
  4.6 1.0 copy-done.4
  5.6 1.0 copy-done.5
  6.6 0.8 copy-done.12
  7.4 2.0 %project.1.refs_4_ = bf16[272,256]{1,0:T(8,128)(2,1)S(1)} custom-call(s32[2]{0:T(128)S(1)} %pad_add_fusion.1.meta_ref, bf16[256,2048]{1,0:T(8,128)(2,1)S(1)} %copy-done.1, bf16[2048,128]{1,0:T(8,128)(2,1)S(1)} %copy-done.3, bf16[2048,128]{1,0:T(8,128)(2,1)S(1)} %copy-done.4, f32[16,8]{1,0:T(8,128)S(1)} %copy.37.kmix_ref, f32[16,8]{1,0:T(8,128)S(1)} %copy.38.vmix_ref, ...), custom_call_target="tpu_custom_call" | custom-call | tf_op jit(solution)/shard_map/project/pallas_call | solution.py:102
  9.5 4.4 %collective-permute-start.3 = (bf16[272,256]{1,0:T(8,128)(2,1)S(1)}, bf16[272,256]{1,0:T(8,128)(2,1)S(1)}, u32[]{:S(2)}, u32[]{:S(2)}) collective-permute-start(bf16[272,256]{1,0:T(8,128)(2,1)S(1)} %project.1.refs_4_), channel_id=1, source_target_pairs={{0,32},{32,64},{64,96},{96,128},{128,160},{160,192},{192,224},{224... | collective-permute-start | bytes 417800 | tf_op jit(solution)/shard_map/ppermute | solution.py:429
  13.9 0.5 fusion.20
  14.4 0.7 fusion.18
  16.1 4.6 %collective-permute-start = (bf16[528,128]{1,0:T(8,128)(2,1)S(1)}, bf16[528,128]{1,0:T(8,128)(2,1)S(1)}, u32[]{:S(2)}, u32[]{:S(2)}) collective-permute-start(bf16[528,128]{1,0:T(8,128)(2,1)S(1)} %fusion.5.refs_0_), channel_id=1, source_target_pairs={{0,24},{8,0},{16,8},{24,16},{1,25},{9,1},{17,9},{25,17},{2,26},{10... | collective-permute-start | bytes 405512 | tf_op jit(solution)/shard_map/ppermute | solution.py:436
  20.8 2.3 %collective-permute-start.1 = (bf16[528,128]{1,0:T(8,128)(2,1)S(1)}, bf16[528,128]{1,0:T(8,128)(2,1)S(1)}, u32[]{:S(2)}, u32[]{:S(2)}) collective-permute-start(bf16[528,128]{1,0:T(8,128)(2,1)S(1)} %fusion.5.refs_0_), channel_id=1, source_target_pairs={{0,16},{8,24},{16,0},{24,8},{1,17},{9,25},{17,1},{25,9},{2,18},{10... | collective-permute-start | bytes 405512 | tf_op jit(solution)/shard_map/ppermute | solution.py:436
  23.0 2.6 %collective-permute-start.2 = (bf16[528,128]{1,0:T(8,128)(2,1)S(1)}, bf16[528,128]{1,0:T(8,128)(2,1)S(1)}, u32[]{:S(2)}, u32[]{:S(2)}) collective-permute-start(bf16[528,128]{1,0:T(8,128)(2,1)S(1)} %fusion.5.refs_0_), channel_id=1, source_target_pairs={{0,8},{8,16},{16,24},{24,0},{1,9},{9,17},{17,25},{25,1},{2,10},{10... | collective-permute-start | bytes 405512 | tf_op jit(solution)/shard_map/ppermute | solution.py:436
  25.6 9.5 %collective-permute-start.11 = (bf16[272,256]{1,0:T(8,128)(2,1)S(1)}, bf16[272,256]{1,0:T(8,128)(2,1)S(1)}, u32[]{:S(2)}, u32[]{:S(2)}) collective-permute-start(bf16[272,256]{1,0:T(8,128)(2,1)S(1)} %project.1.refs_4_), channel_id=1, source_target_pairs={{0,480},{32,0},{64,32},{96,64},{128,96},{160,128},{192,160},{224,1... | collective-permute-start | bytes 417800 | tf_op jit(solution)/shard_map/ppermute | solution.py:432
  35.1 1.9 %collective-permute-start.4 = (bf16[272,256]{1,0:T(8,128)(2,1)S(1)}, bf16[272,256]{1,0:T(8,128)(2,1)S(1)}, u32[]{:S(2)}, u32[]{:S(2)}) collective-permute-start(bf16[272,256]{1,0:T(8,128)(2,1)S(1)} %collective-permute-done.3.refs_5_), channel_id=1, source_target_pairs={{0,32},{32,64},{64,96},{96,128},{128,160},{160,192},{192,224},{224... | collective-permute-start | bytes 417800 | tf_op jit(solution)/shard_map/ppermute | solution.py:429
  37.1 3.7 %collective-permute-start.18 = (bf16[256,2048]{1,0:T(8,128)(2,1)}, bf16[256,2048]{1,0:T(8,128)(2,1)}, u32[]{:S(2)}, u32[]{:S(2)}) collective-permute-start(bf16[256,2048]{1,0:T(8,128)(2,1)} %own_ref.1), channel_id=1, source_target_pairs={{0,1},{1,0},{2,3},{3,2},{4,5},{5,4},{6,7},{7,6},{8,9},{9,8},{10,11... | collective-permute-start | bytes 3145736 | tf_op jit(solution)/shard_map/ppermute | solution.py:438
  40.8 0.6 copy-done.6
  41.5 0.6 copy-done.8
  42.1 0.7 copy-done.10
  42.9 4.8 %collective-permute-start.12 = (bf16[272,256]{1,0:T(8,128)(2,1)S(1)}, bf16[272,256]{1,0:T(8,128)(2,1)S(1)}, u32[]{:S(2)}, u32[]{:S(2)}) collective-permute-start(bf16[272,256]{1,0:T(8,128)(2,1)S(1)} %collective-permute-done.11.refs_19_), channel_id=1, source_target_pairs={{0,480},{32,0},{64,32},{96,64},{128,96},{160,128},{192,160},{224,1... | collective-permute-start | bytes 417800 | tf_op jit(solution)/shard_map/ppermute | solution.py:432
  47.7 1.9 %collective-permute-start.5 = (bf16[272,256]{1,0:T(8,128)(2,1)S(1)}, bf16[272,256]{1,0:T(8,128)(2,1)S(1)}, u32[]{:S(2)}, u32[]{:S(2)}) collective-permute-start(bf16[272,256]{1,0:T(8,128)(2,1)S(1)} %collective-permute-done.4.refs_6_), channel_id=1, source_target_pairs={{0,32},{32,64},{64,96},{96,128},{128,160},{160,192},{192,224},{224... | collective-permute-start | bytes 417800 | tf_op jit(solution)/shard_map/ppermute | solution.py:429
  49.8 0.9 collective-permute-done.12.refs_18_
  50.7 5.3 %collective-permute-start.13 = (bf16[272,256]{1,0:T(8,128)(2,1)S(1)}, bf16[272,256]{1,0:T(8,128)(2,1)S(1)}, u32[]{:S(2)}, u32[]{:S(2)}) collective-permute-start(bf16[272,256]{1,0:T(8,128)(2,1)S(1)} %collective-permute-done.12.refs_18_), channel_id=1, source_target_pairs={{0,480},{32,0},{64,32},{96,64},{128,96},{160,128},{192,160},{224,1... | collective-permute-start | bytes 417800 | tf_op jit(solution)/shard_map/ppermute | solution.py:432
  56.0 1.9 %collective-permute-start.6 = (bf16[272,256]{1,0:T(8,128)(2,1)S(1)}, bf16[272,256]{1,0:T(8,128)(2,1)S(1)}, u32[]{:S(2)}, u32[]{:S(2)}) collective-permute-start(bf16[272,256]{1,0:T(8,128)(2,1)S(1)} %collective-permute-done.5.refs_7_), channel_id=1, source_target_pairs={{0,32},{32,64},{64,96},{96,128},{128,160},{160,192},{192,224},{224... | collective-permute-start | bytes 417800 | tf_op jit(solution)/shard_map/ppermute | solution.py:429
  58.1 5.4 %collective-permute-start.14 = (bf16[272,256]{1,0:T(8,128)(2,1)S(1)}, bf16[272,256]{1,0:T(8,128)(2,1)S(1)}, u32[]{:S(2)}, u32[]{:S(2)}) collective-permute-start(bf16[272,256]{1,0:T(8,128)(2,1)S(1)} %collective-permute-done.13.refs_17_), channel_id=1, source_target_pairs={{0,480},{32,0},{64,32},{96,64},{128,96},{160,128},{192,160},{224,1... | collective-permute-start | bytes 417800 | tf_op jit(solution)/shard_map/ppermute | solution.py:432
  63.5 1.9 %collective-permute-start.7 = (bf16[272,256]{1,0:T(8,128)(2,1)S(1)}, bf16[272,256]{1,0:T(8,128)(2,1)}, u32[]{:S(2)}, u32[]{:S(2)}) collective-permute-start(bf16[272,256]{1,0:T(8,128)(2,1)S(1)} %collective-permute-done.6.refs_8_), channel_id=1, source_target_pairs={{0,32},{32,64},{64,96},{96,128},{128,160},{160,192},{192,224},{224... | collective-permute-start | bytes 417800 | tf_op jit(solution)/shard_map/ppermute | solution.py:429
  65.8 0.6 select_reduce_fusion
  66.4 4.6 %collective-permute-start.15 = (bf16[272,256]{1,0:T(8,128)(2,1)S(1)}, bf16[272,256]{1,0:T(8,128)(2,1)S(1)}, u32[]{:S(2)}, u32[]{:S(2)}) collective-permute-start(bf16[272,256]{1,0:T(8,128)(2,1)S(1)} %collective-permute-done.14.refs_16_), channel_id=1, source_target_pairs={{0,480},{32,0},{64,32},{96,64},{128,96},{160,128},{192,160},{224,1... | collective-permute-start | bytes 417800 | tf_op jit(solution)/shard_map/ppermute | solution.py:432
  71.0 1.9 %collective-permute-start.8 = (bf16[272,256]{1,0:T(8,128)(2,1)}, bf16[272,256]{1,0:T(8,128)(2,1)S(1)}, u32[]{:S(2)}, u32[]{:S(2)}) collective-permute-start(bf16[272,256]{1,0:T(8,128)(2,1)} %collective-permute-done.7.refs_9_), channel_id=1, source_target_pairs={{0,32},{32,64},{64,96},{96,128},{128,160},{160,192},{192,224},{224... | collective-permute-start | bytes 417800 | tf_op jit(solution)/shard_map/ppermute | solution.py:429
  73.0 5.0 %collective-permute-start.16 = (bf16[272,256]{1,0:T(8,128)(2,1)S(1)}, bf16[272,256]{1,0:T(8,128)(2,1)S(1)}, u32[]{:S(2)}, u32[]{:S(2)}) collective-permute-start(bf16[272,256]{1,0:T(8,128)(2,1)S(1)} %collective-permute-done.15.refs_15_), channel_id=1, source_target_pairs={{0,480},{32,0},{64,32},{96,64},{128,96},{160,128},{192,160},{224,1... | collective-permute-start | bytes 417800 | tf_op jit(solution)/shard_map/ppermute | solution.py:432
  78.0 0.2 collective-permute-done.8.refs_10_
  78.2 1.9 %collective-permute-start.9 = (bf16[272,256]{1,0:T(8,128)(2,1)S(1)}, bf16[272,256]{1,0:T(8,128)(2,1)S(1)}, u32[]{:S(2)}, u32[]{:S(2)}) collective-permute-start(bf16[272,256]{1,0:T(8,128)(2,1)S(1)} %collective-permute-done.8.refs_10_), channel_id=1, source_target_pairs={{0,32},{32,64},{64,96},{96,128},{128,160},{160,192},{192,224},{224... | collective-permute-start | bytes 417800 | tf_op jit(solution)/shard_map/ppermute | solution.py:429
  80.2 4.8 %collective-permute-start.17 = (bf16[272,256]{1,0:T(8,128)(2,1)S(1)}, bf16[272,256]{1,0:T(8,128)(2,1)S(1)}, u32[]{:S(2)}, u32[]{:S(2)}) collective-permute-start(bf16[272,256]{1,0:T(8,128)(2,1)S(1)} %collective-permute-done.16.refs_14_), channel_id=1, source_target_pairs={{0,480},{32,0},{64,32},{96,64},{128,96},{160,128},{192,160},{224,1... | collective-permute-start | bytes 417800 | tf_op jit(solution)/shard_map/ppermute | solution.py:432
  85.2 1.9 %collective-permute-start.10 = (bf16[272,256]{1,0:T(8,128)(2,1)S(1)}, bf16[272,256]{1,0:T(8,128)(2,1)S(1)}, u32[]{:S(2)}, u32[]{:S(2)}) collective-permute-start(bf16[272,256]{1,0:T(8,128)(2,1)S(1)} %collective-permute-done.9.refs_11_), channel_id=1, source_target_pairs={{0,32},{32,64},{64,96},{96,128},{128,160},{160,192},{192,224},{224... | collective-permute-start | bytes 417800 | tf_op jit(solution)/shard_map/ppermute | solution.py:429
  87.2 5.0 %collective-permute-done.10.refs_12_ = bf16[272,256]{1,0:T(8,128)(2,1)S(1)} collective-permute-done((bf16[272,256]{1,0:T(8,128)(2,1)S(1)}, bf16[272,256]{1,0:T(8,128)(2,1)S(1)}, u32[]{:S(2)}, u32[]{:S(2)}) %collective-permute-start.10) | collective-permute-done | bytes 139296 | tf_op jit(solution)/shard_map/ppermute | solution.py:429
  92.2 0.9 copy-done.7
  93.1 0.9 copy-done.9
  94.0 0.9 copy-done.11
  94.9 7.4 %attend.1 = bf16[8,272,256]{2,1,0:T(8,128)(2,1)} custom-call(s32[6]{0:T(128)S(1)} %pad_add_fusion.meta_ref, s32[16,32]{1,0:T(8,128)S(1)} %broadcast_add_fusion.ids_ref, f32[16,32]{1,0:T(8,128)S(1)} %convert_log_fusion.bias_ref, bf16[528,128]{1,0:T(8,128)(2,1)S(1)} %fusion.5.refs_0_, bf16[528,128]{1,0:T(8,128)(2,1)S(1)} %copy-done.7, ...), custom_call_target="tpu_custom_call" | custom-call | tf_op jit(solution)/shard_map/attend/pallas_call | solution.py:281
  102.4 9.7 %all-to-all-start = ((bf16[8,272,256]{2,1,0:T(8,128)(2,1)}), bf16[8,272,256]{2,1,0:T(8,128)(2,1)S(1)}, u32[]{:S(2)}, u32[]{:S(2)}) async-start(bf16[8,272,256]{2,1,0:T(8,128)(2,1)} %attend.1), calls=%async_computation | async-start | bytes 2228224 | tf_op jit(solution)/shard_map/all_to_all | solution.py:451
  112.1 1.1 fusion.2
  113.3 14.4 %all-to-all-done.got_ref = bf16[8,272,256]{2,1,0:T(8,128)(2,1)S(1)} async-done(((bf16[8,272,256]{2,1,0:T(8,128)(2,1)}), bf16[8,272,256]{2,1,0:T(8,128)(2,1)S(1)}, u32[]{:S(2)}, u32[]{:S(2)}) %all-to-all-start) | async-done | bytes 1114144 | tf_op jit(solution)/shard_map/all_to_all | solution.py:451
  127.8 3.9 %merge.1 = (bf16[128,2048]{1,0:T(8,128)(2,1)}, f32[2,2,256]{2,1,0:T(2,128)S(1)}) custom-call(s32[1]{0:T(128)} %bitcast.1.meta_ref, bf16[8,272,256]{2,1,0:T(8,128)(2,1)S(1)} %all-to-all-done.got_ref, f32[128,8]{1,0:T(8,128)S(1)} %copy.40.gate_ref, bf16[256,2048]{1,0:T(8,128)(2,1)} %own_ref.1, bf16[256,2048]{1,0:T(8,128)(2,1)} %collective-permute-done.18.other_ref), custom_call_target="tpu_custom_call" | custom-call | tf_op jit(solution)/shard_map/merge/pallas_call | solution.py:348
  131.6 4.0 %all-to-all-start.1 = ((bf16[4,32,2048]{2,1,0:T(8,128)(2,1)}), bf16[4,32,2048]{2,1,0:T(8,128)(2,1)S(1)}, u32[]{:S(2)}, u32[]{:S(2)}) async-start(bf16[4,32,2048]{2,1,0:T(8,128)(2,1)} %bitcast.15), calls=%async_computation.1 | async-start | bytes 1048576 | tf_op jit(solution)/shard_map/all_to_all | solution.py:457
  135.8 0.7 reshape.132
  136.4 7.3 %all-to-all-done.1 = bf16[4,32,2048]{2,1,0:T(8,128)(2,1)S(1)} async-done(((bf16[4,32,2048]{2,1,0:T(8,128)(2,1)}), bf16[4,32,2048]{2,1,0:T(8,128)(2,1)S(1)}, u32[]{:S(2)}, u32[]{:S(2)}) %all-to-all-start.1) | async-done | bytes 524320 | tf_op jit(solution)/shard_map/all_to_all | solution.py:457
  143.7 0.7 reduce_sum.52
  (71 shorter events, 2.3 us)
Async XLA Ops:
  0.6 13.2 %copy-start = (bf16[2048,256]{1,0:T(8,128)(2,1)S(1)}, bf16[2048,256]{1,0:T(8,128)(2,1)}, u32[]{:S(2)}) copy-start(bf16[2048,256]{1,0:T(8,128)(2,1)} %param.20) | copy-start | bytes 3145732
  2.3 1.2 copy-start.1
  3.6 1.0 copy-start.3
  4.6 1.0 copy-start.4
  5.6 1.0 copy-start.5
  6.6 0.8 copy-start.12
  7.4 6.4 %copy-start.2 = (bf16[256,2048]{1,0:T(8,128)(2,1)S(1)}, bf16[256,2048]{1,0:T(8,128)(2,1)}, u32[]{:S(2)}) copy-start(bf16[256,2048]{1,0:T(8,128)(2,1)} %tok_ref.1) | copy-start | bytes 3145732
  9.5 25.6 %collective-permute-start.3 = (bf16[272,256]{1,0:T(8,128)(2,1)S(1)}, bf16[272,256]{1,0:T(8,128)(2,1)S(1)}, u32[]{:S(2)}, u32[]{:S(2)}) collective-permute-start(bf16[272,256]{1,0:T(8,128)(2,1)S(1)} %project.1.refs_4_), channel_id=1, source_target_pairs={{0,32},{32,64},{64,96},{96,128},{128,160},{160,192},{192,224},{224... | collective-permute-start | bytes 417800 | tf_op jit(solution)/shard_map/ppermute | solution.py:429
  13.9 1.3 copy-start.13
  13.9 1.3 copy-start.14
  14.4 1.5 %copy-start.16 = (s32[4,32]{1,0:T(4,128)S(1)}, s32[4,32]{1,0:T(4,128)}, u32[]{:S(2)}) copy-start(s32[4,32]{1,0:T(4,128)} %param.27) | copy-start | bytes 1540
  15.3 50.2 %copy-start.15 = (bf16[64,64]{1,0:T(8,128)(2,1)S(1)}, bf16[64,64]{1,0:T(8,128)(2,1)}, u32[]{:S(2)}) copy-start(bf16[64,64]{1,0:T(8,128)(2,1)} %constant.194) | copy-start | bytes 24580
  15.3 50.5 %copy-start.17 = (s32[64]{0:T(128)S(1)}, s32[64]{0:T(128)}, u32[]{:S(2)}) copy-start(s32[64]{0:T(128)} %constant.142) | copy-start | bytes 772
  16.1 21.0 %collective-permute-start = (bf16[528,128]{1,0:T(8,128)(2,1)S(1)}, bf16[528,128]{1,0:T(8,128)(2,1)S(1)}, u32[]{:S(2)}, u32[]{:S(2)}) collective-permute-start(bf16[528,128]{1,0:T(8,128)(2,1)S(1)} %fusion.5.refs_0_), channel_id=1, source_target_pairs={{0,24},{8,0},{16,8},{24,16},{1,25},{9,1},{17,9},{25,17},{2,26},{10... | collective-permute-start | bytes 405512 | tf_op jit(solution)/shard_map/ppermute | solution.py:436
  20.8 20.7 %collective-permute-start.1 = (bf16[528,128]{1,0:T(8,128)(2,1)S(1)}, bf16[528,128]{1,0:T(8,128)(2,1)S(1)}, u32[]{:S(2)}, u32[]{:S(2)}) collective-permute-start(bf16[528,128]{1,0:T(8,128)(2,1)S(1)} %fusion.5.refs_0_), channel_id=1, source_target_pairs={{0,16},{8,24},{16,0},{24,8},{1,17},{9,25},{17,1},{25,9},{2,18},{10... | collective-permute-start | bytes 405512 | tf_op jit(solution)/shard_map/ppermute | solution.py:436
  23.0 19.1 %collective-permute-start.2 = (bf16[528,128]{1,0:T(8,128)(2,1)S(1)}, bf16[528,128]{1,0:T(8,128)(2,1)S(1)}, u32[]{:S(2)}, u32[]{:S(2)}) collective-permute-start(bf16[528,128]{1,0:T(8,128)(2,1)S(1)} %fusion.5.refs_0_), channel_id=1, source_target_pairs={{0,8},{8,16},{16,24},{24,0},{1,9},{9,17},{17,25},{25,1},{2,10},{10... | collective-permute-start | bytes 405512 | tf_op jit(solution)/shard_map/ppermute | solution.py:436
  25.6 17.2 %collective-permute-start.11 = (bf16[272,256]{1,0:T(8,128)(2,1)S(1)}, bf16[272,256]{1,0:T(8,128)(2,1)S(1)}, u32[]{:S(2)}, u32[]{:S(2)}) collective-permute-start(bf16[272,256]{1,0:T(8,128)(2,1)S(1)} %project.1.refs_4_), channel_id=1, source_target_pairs={{0,480},{32,0},{64,32},{96,64},{128,96},{160,128},{192,160},{224,1... | collective-permute-start | bytes 417800 | tf_op jit(solution)/shard_map/ppermute | solution.py:432
  35.1 12.6 %collective-permute-start.4 = (bf16[272,256]{1,0:T(8,128)(2,1)S(1)}, bf16[272,256]{1,0:T(8,128)(2,1)S(1)}, u32[]{:S(2)}, u32[]{:S(2)}) collective-permute-start(bf16[272,256]{1,0:T(8,128)(2,1)S(1)} %collective-permute-done.3.refs_5_), channel_id=1, source_target_pairs={{0,32},{32,64},{64,96},{96,128},{128,160},{160,192},{192,224},{224... | collective-permute-start | bytes 417800 | tf_op jit(solution)/shard_map/ppermute | solution.py:429
  37.1 76.2 %collective-permute-start.18 = (bf16[256,2048]{1,0:T(8,128)(2,1)}, bf16[256,2048]{1,0:T(8,128)(2,1)}, u32[]{:S(2)}, u32[]{:S(2)}) collective-permute-start(bf16[256,2048]{1,0:T(8,128)(2,1)} %own_ref.1), channel_id=1, source_target_pairs={{0,1},{1,0},{2,3},{3,2},{4,5},{5,4},{6,7},{7,6},{8,9},{9,8},{10,11... | collective-permute-start | bytes 3145736 | tf_op jit(solution)/shard_map/ppermute | solution.py:438
  40.8 0.7 copy-start.6
  41.5 0.6 copy-start.8
  42.1 0.7 copy-start.10
  42.9 7.8 %collective-permute-start.12 = (bf16[272,256]{1,0:T(8,128)(2,1)S(1)}, bf16[272,256]{1,0:T(8,128)(2,1)S(1)}, u32[]{:S(2)}, u32[]{:S(2)}) collective-permute-start(bf16[272,256]{1,0:T(8,128)(2,1)S(1)} %collective-permute-done.11.refs_19_), channel_id=1, source_target_pairs={{0,480},{32,0},{64,32},{96,64},{128,96},{160,128},{192,160},{224,1... | collective-permute-start | bytes 417800 | tf_op jit(solution)/shard_map/ppermute | solution.py:432
  47.7 8.3 %collective-permute-start.5 = (bf16[272,256]{1,0:T(8,128)(2,1)S(1)}, bf16[272,256]{1,0:T(8,128)(2,1)S(1)}, u32[]{:S(2)}, u32[]{:S(2)}) collective-permute-start(bf16[272,256]{1,0:T(8,128)(2,1)S(1)} %collective-permute-done.4.refs_6_), channel_id=1, source_target_pairs={{0,32},{32,64},{64,96},{96,128},{128,160},{160,192},{192,224},{224... | collective-permute-start | bytes 417800 | tf_op jit(solution)/shard_map/ppermute | solution.py:429
  50.7 7.4 %collective-permute-start.13 = (bf16[272,256]{1,0:T(8,128)(2,1)S(1)}, bf16[272,256]{1,0:T(8,128)(2,1)S(1)}, u32[]{:S(2)}, u32[]{:S(2)}) collective-permute-start(bf16[272,256]{1,0:T(8,128)(2,1)S(1)} %collective-permute-done.12.refs_18_), channel_id=1, source_target_pairs={{0,480},{32,0},{64,32},{96,64},{128,96},{160,128},{192,160},{224,1... | collective-permute-start | bytes 417800 | tf_op jit(solution)/shard_map/ppermute | solution.py:432
  56.0 7.4 %collective-permute-start.6 = (bf16[272,256]{1,0:T(8,128)(2,1)S(1)}, bf16[272,256]{1,0:T(8,128)(2,1)S(1)}, u32[]{:S(2)}, u32[]{:S(2)}) collective-permute-start(bf16[272,256]{1,0:T(8,128)(2,1)S(1)} %collective-permute-done.5.refs_7_), channel_id=1, source_target_pairs={{0,32},{32,64},{64,96},{96,128},{128,160},{160,192},{192,224},{224... | collective-permute-start | bytes 417800 | tf_op jit(solution)/shard_map/ppermute | solution.py:429
  58.1 8.3 %collective-permute-start.14 = (bf16[272,256]{1,0:T(8,128)(2,1)S(1)}, bf16[272,256]{1,0:T(8,128)(2,1)S(1)}, u32[]{:S(2)}, u32[]{:S(2)}) collective-permute-start(bf16[272,256]{1,0:T(8,128)(2,1)S(1)} %collective-permute-done.13.refs_17_), channel_id=1, source_target_pairs={{0,480},{32,0},{64,32},{96,64},{128,96},{160,128},{192,160},{224,1... | collective-permute-start | bytes 417800 | tf_op jit(solution)/shard_map/ppermute | solution.py:432
  63.5 7.5 %collective-permute-start.7 = (bf16[272,256]{1,0:T(8,128)(2,1)S(1)}, bf16[272,256]{1,0:T(8,128)(2,1)}, u32[]{:S(2)}, u32[]{:S(2)}) collective-permute-start(bf16[272,256]{1,0:T(8,128)(2,1)S(1)} %collective-permute-done.6.refs_8_), channel_id=1, source_target_pairs={{0,32},{32,64},{64,96},{96,128},{128,160},{160,192},{192,224},{224... | collective-permute-start | bytes 417800 | tf_op jit(solution)/shard_map/ppermute | solution.py:429
  66.4 6.6 %collective-permute-start.15 = (bf16[272,256]{1,0:T(8,128)(2,1)S(1)}, bf16[272,256]{1,0:T(8,128)(2,1)S(1)}, u32[]{:S(2)}, u32[]{:S(2)}) collective-permute-start(bf16[272,256]{1,0:T(8,128)(2,1)S(1)} %collective-permute-done.14.refs_16_), channel_id=1, source_target_pairs={{0,480},{32,0},{64,32},{96,64},{128,96},{160,128},{192,160},{224,1... | collective-permute-start | bytes 417800 | tf_op jit(solution)/shard_map/ppermute | solution.py:432
  71.0 7.2 %collective-permute-start.8 = (bf16[272,256]{1,0:T(8,128)(2,1)}, bf16[272,256]{1,0:T(8,128)(2,1)S(1)}, u32[]{:S(2)}, u32[]{:S(2)}) collective-permute-start(bf16[272,256]{1,0:T(8,128)(2,1)} %collective-permute-done.7.refs_9_), channel_id=1, source_target_pairs={{0,32},{32,64},{64,96},{96,128},{128,160},{160,192},{192,224},{224... | collective-permute-start | bytes 417800 | tf_op jit(solution)/shard_map/ppermute | solution.py:429
  73.0 7.2 %collective-permute-start.16 = (bf16[272,256]{1,0:T(8,128)(2,1)S(1)}, bf16[272,256]{1,0:T(8,128)(2,1)S(1)}, u32[]{:S(2)}, u32[]{:S(2)}) collective-permute-start(bf16[272,256]{1,0:T(8,128)(2,1)S(1)} %collective-permute-done.15.refs_15_), channel_id=1, source_target_pairs={{0,480},{32,0},{64,32},{96,64},{128,96},{160,128},{192,160},{224,1... | collective-permute-start | bytes 417800 | tf_op jit(solution)/shard_map/ppermute | solution.py:432
  78.2 7.0 %collective-permute-start.9 = (bf16[272,256]{1,0:T(8,128)(2,1)S(1)}, bf16[272,256]{1,0:T(8,128)(2,1)S(1)}, u32[]{:S(2)}, u32[]{:S(2)}) collective-permute-start(bf16[272,256]{1,0:T(8,128)(2,1)S(1)} %collective-permute-done.8.refs_10_), channel_id=1, source_target_pairs={{0,32},{32,64},{64,96},{96,128},{128,160},{160,192},{192,224},{224... | collective-permute-start | bytes 417800 | tf_op jit(solution)/shard_map/ppermute | solution.py:429
  80.2 7.1 %collective-permute-start.17 = (bf16[272,256]{1,0:T(8,128)(2,1)S(1)}, bf16[272,256]{1,0:T(8,128)(2,1)S(1)}, u32[]{:S(2)}, u32[]{:S(2)}) collective-permute-start(bf16[272,256]{1,0:T(8,128)(2,1)S(1)} %collective-permute-done.16.refs_14_), channel_id=1, source_target_pairs={{0,480},{32,0},{64,32},{96,64},{128,96},{160,128},{192,160},{224,1... | collective-permute-start | bytes 417800 | tf_op jit(solution)/shard_map/ppermute | solution.py:432
  85.2 7.0 %collective-permute-start.10 = (bf16[272,256]{1,0:T(8,128)(2,1)S(1)}, bf16[272,256]{1,0:T(8,128)(2,1)S(1)}, u32[]{:S(2)}, u32[]{:S(2)}) collective-permute-start(bf16[272,256]{1,0:T(8,128)(2,1)S(1)} %collective-permute-done.9.refs_11_), channel_id=1, source_target_pairs={{0,32},{32,64},{64,96},{96,128},{128,160},{160,192},{192,224},{224... | collective-permute-start | bytes 417800 | tf_op jit(solution)/shard_map/ppermute | solution.py:429
  92.2 0.9 copy-start.7
  93.1 0.9 copy-start.9
  94.0 0.9 copy-start.11
  102.4 25.4 %all-to-all-start = ((bf16[8,272,256]{2,1,0:T(8,128)(2,1)}), bf16[8,272,256]{2,1,0:T(8,128)(2,1)S(1)}, u32[]{:S(2)}, u32[]{:S(2)}) async-start(bf16[8,272,256]{2,1,0:T(8,128)(2,1)} %attend.1), calls=%async_computation | async-start | bytes 2228224 | tf_op jit(solution)/shard_map/all_to_all | solution.py:451
  131.6 12.1 %all-to-all-start.1 = ((bf16[4,32,2048]{2,1,0:T(8,128)(2,1)}), bf16[4,32,2048]{2,1,0:T(8,128)(2,1)S(1)}, u32[]{:S(2)}, u32[]{:S(2)}) async-start(bf16[4,32,2048]{2,1,0:T(8,128)(2,1)} %bitcast.15), calls=%async_computation.1 | async-start | bytes 1048576 | tf_op jit(solution)/shard_map/all_to_all | solution.py:457

commit v4 on v3

--- a/solution.py
+++ b/solution.py
@@ -17,10 +17,11 @@
 KV = ("z", "y")
 SPAN = 256
 STATS = 16
-PER_STEP = 4
+PER_STEP = 10
+PEERS = 1
 POOLED = 16
 RING = 16
-LIST = 32
+QROWS = 528
 SCALE = HEAD_SIZE**-0.5
 
 
@@ -70,8 +71,12 @@
             return value * cosines + jnp.where(sign, -turned, turned) * sines
 
         def pooled(value, mix_ref):
-            lane = lax.broadcasted_iota(jnp.int32, (POOL_STRIDE, 8), 1)
-            mix = jnp.sum(jnp.where(lane == group, mix_ref[...], 0.0), axis=1, keepdims=True)
+            shape = (POOL_STRIDE, POOL_STRIDE)
+            eye = lax.broadcasted_iota(jnp.int32, shape, 0) == lax.broadcasted_iota(
+                jnp.int32, shape, 1
+            )
+            mix = jnp.where(eye, mix_ref[pl.ds(group, 1), :], 0.0)
+            mix = jnp.sum(mix, axis=1, keepdims=True)
             mixed = value.reshape(POOLED, POOL_STRIDE, HEAD_SIZE) * mix[None]
             return jnp.sum(mixed, axis=1)
 
@@ -108,8 +113,8 @@
                 pl.BlockSpec((SPAN, depth), lambda i, *_: (0, i)),
                 pl.BlockSpec((depth, HEAD_SIZE), lambda i, *_: (i, 0)),
                 pl.BlockSpec((depth, HEAD_SIZE), lambda i, *_: (i, 0)),
-                pl.BlockSpec((POOL_STRIDE, 8), lambda i, *_: (0, 0)),
-                pl.BlockSpec((POOL_STRIDE, 8), lambda i, *_: (0, 0)),
+                pl.BlockSpec((8, POOL_STRIDE), lambda i, *_: (0, 0)),
+                pl.BlockSpec((8, POOL_STRIDE), lambda i, *_: (0, 0)),
                 pl.BlockSpec((2, SPAN + POOLED, HEAD_SIZE), lambda i, *_: (0, 0, 0)),
                 pl.BlockSpec((2, 64, HEAD_SIZE), lambda i, *_: (0, 0, 0)),
             ],
@@ -120,7 +125,6 @@
             ],
         ),
         out_shape=jax.ShapeDtypeStruct((SPAN + POOLED, 2 * HEAD_SIZE), jnp.bfloat16),
-        compiler_params=pltpu.CompilerParams(vmem_limit_bytes=12 << 20),
         name="project",
     )(meta, tokens, key_matrix, value_matrix, key_mix, value_mix, local, spans)
 
@@ -133,12 +137,13 @@
 
 
 def attend_kernel(meta_ref, ids_ref, bias_ref, *refs):
-    q_refs = refs[:4]
-    chunk_refs = refs[4 : 4 + RING]
-    out_ref, kv_ref, pool_ref, acc_ref, m_ref, l_ref, lse_ref = refs[4 + RING :]
-    z = meta_ref[0]
-    y = meta_ref[1]
-    owners = [(y + peer) % 4 for peer in range(4)]
+    own_ref, side_ref, far_ref = refs[:3]
+    chunk_refs = refs[3 : 3 + RING]
+    out_ref, kv_ref, pool_ref, acc_ref, m_ref, l_ref, lse_ref = refs[3 + RING :]
+    z = meta_ref[0, 0]
+    y = meta_ref[0, 1]
+    q_refs = [own_ref, side_ref, far_ref.at[:QROWS], far_ref.at[QROWS:]]
+    owners = [y ^ peer for peer in range(4)]
     for o in range(RING):
         kv_ref[o * SPAN : (o + 1) * SPAN, :] = chunk_refs[o][:SPAN, :]
         pool_ref[o * POOLED : (o + 1) * POOLED, :] = chunk_refs[o][SPAN:, :]
@@ -198,14 +203,15 @@
             g = 16 + peer * 4 + qb
             lse_ref[g : g + 1, :] = jnp.sum(spread, axis=0, keepdims=True)
 
-    for peer in range(4):
-        for qb in range(4):
-            acc_ref[qb] = jnp.zeros((HEAD_SIZE, HEAD_SIZE), jnp.float32)
-            m_ref[qb] = jnp.full((1, HEAD_SIZE), FLOOR, jnp.float32)
-            l_ref[qb] = jnp.zeros((1, HEAD_SIZE), jnp.float32)
-
-        def group(k, carry, peer=peer):
-            for qb in range(4):
+    for first_peer in range(0, 4, PEERS):
+        members = [(first_peer + i // 4, i % 4) for i in range(4 * PEERS)]
+        for slot in range(4 * PEERS):
+            acc_ref[slot] = jnp.zeros((HEAD_SIZE, HEAD_SIZE), jnp.float32)
+            m_ref[slot] = jnp.full((1, HEAD_SIZE), FLOOR, jnp.float32)
+            l_ref[slot] = jnp.zeros((1, HEAD_SIZE), jnp.float32)
+
+        def group(k, carry, members=members):
+            for slot, (peer, qb) in enumerate(members):
                 g = peer * 4 + qb
                 qpos = (z * 4 + owners[peer]) * SPAN + qb * BLOCK + lane
                 keys, values, bases, biases = [], [], [], []
@@ -233,29 +239,33 @@
                     seen = row <= (qpos - bases[e])
                     slabs.append(jnp.where(seen, slab, NEGATIVE))
                 s = jnp.concatenate(slabs, 0)
-                m_old = m_ref[qb]
+                m_old = m_ref[slot]
                 m_new = jnp.maximum(m_old, jnp.max(s, axis=0, keepdims=True))
                 alpha = jnp.exp(m_old - m_new)
                 p = jnp.exp(s - m_new)
-                l_ref[qb] = l_ref[qb] * alpha + jnp.sum(p, axis=0, keepdims=True)
-                m_ref[qb] = m_new
+                total = l_ref[slot] * alpha + jnp.sum(p, axis=0, keepdims=True)
                 pv = lax.dot_general(
                     vg,
                     p.astype(jnp.bfloat16),
                     (((0,), (0,)), ((), ())),
                     preferred_element_type=jnp.float32,
                 )
-                acc_ref[qb] = acc_ref[qb] * alpha + pv
+                acc_ref[slot] = acc_ref[slot] * alpha + pv
+                m_ref[slot] = m_new
+                l_ref[slot] = total
             return carry
 
-        lax.fori_loop(0, meta_ref[2 + peer], group, 0)
-        for qb in range(4):
-            total = l_ref[qb]
+        steps = meta_ref[0, 2 + first_peer]
+        for peer in range(first_peer + 1, first_peer + PEERS):
+            steps = jnp.maximum(steps, meta_ref[0, 2 + peer])
+        lax.fori_loop(0, steps, group, 0)
+        for slot, (peer, qb) in enumerate(members):
+            total = l_ref[slot]
             some = total > 0.0
             total = jnp.where(some, total, 1.0)
-            store(peer, qb, 0, acc_ref[qb] / total)
+            store(peer, qb, 0, acc_ref[slot] / total)
             g = peer * 4 + qb
-            lse_ref[g : g + 1, :] = jnp.where(some, m_ref[qb] + jnp.log(total), FLOOR)
+            lse_ref[g : g + 1, :] = jnp.where(some, m_ref[slot] + jnp.log(total), FLOOR)
 
     for peer in range(4):
         rows = []
@@ -283,15 +293,16 @@
         grid_spec=pltpu.PrefetchScalarGridSpec(
             num_scalar_prefetch=3,
             grid=(1,),
-            in_specs=[whole((528, HEAD_SIZE))] * 4
+            in_specs=[whole((QROWS, HEAD_SIZE))] * 2
+            + [whole((2 * QROWS, HEAD_SIZE))]
             + [whole((SPAN + POOLED, 2 * HEAD_SIZE))] * RING,
             out_specs=whole((8, SPAN + STATS, 2 * HEAD_SIZE)),
             scratch_shapes=[
                 pltpu.VMEM((RING * SPAN, 2 * HEAD_SIZE), jnp.bfloat16),
                 pltpu.VMEM((RING * POOLED, 2 * HEAD_SIZE), jnp.bfloat16),
-                pltpu.VMEM((4, HEAD_SIZE, HEAD_SIZE), jnp.float32),
-                pltpu.VMEM((4, 1, HEAD_SIZE), jnp.float32),
-                pltpu.VMEM((4, 1, HEAD_SIZE), jnp.float32),
+                pltpu.VMEM((4 * PEERS, HEAD_SIZE, HEAD_SIZE), jnp.float32),
+                pltpu.VMEM((4 * PEERS, 1, HEAD_SIZE), jnp.float32),
+                pltpu.VMEM((4 * PEERS, 1, HEAD_SIZE), jnp.float32),
                 pltpu.VMEM((32, HEAD_SIZE), jnp.float32),
             ],
         ),
@@ -371,24 +382,67 @@
     )(meta, got, gates, own_weight, other_weight)
 
 
-def block_lists(near, z, y):
+def lists_kernel(
+    place_ref, own_ref, side_ref, far_ref, last_ref, meta_ref, ids_ref, bias_ref
+):
     f32 = jnp.float32
-    near_chosen = jnp.stack([v[512] for v in near]).reshape(16, 32).astype(jnp.int32)
-    mine = (near_chosen // 4) % 4 == y
-    slot = ((z - near_chosen // 16) % RING) * 4 + near_chosen % 4
-    slot = jnp.where(mine, slot, -1)
-    counts = jnp.sum((slot[:, :, None] == np.arange(BLOCK)[None, None, :]).astype(jnp.int32), axis=1)
-    present = counts > 0
-    earlier = (np.arange(BLOCK)[:, None] < np.arange(BLOCK)[None, :]).astype(np.float32)
-    rank = jnp.dot(present.astype(f32), earlier).astype(jnp.int32)
-    hit = present[:, :, None] & (rank[:, :, None] == np.arange(LIST)[None, None, :])
-    ids = jnp.sum(jnp.where(hit, np.arange(1, BLOCK + 1)[None, :, None], 0), axis=1) - 1
-    times = jnp.sum(jnp.where(hit, counts[:, :, None], 0), axis=1)
-    bias = jnp.log(jnp.maximum(times, 1).astype(f32))
-    lengths = jnp.sum(present.astype(jnp.int32), axis=1)
-    steps = (jnp.max(lengths.reshape(4, 4), axis=1) + PER_STEP - 1) // PER_STEP
-    meta = jnp.concatenate([jnp.stack([z, y]).astype(jnp.int32), steps.astype(jnp.int32)])
-    return meta, ids, bias
+    z = place_ref[2]
+    y = place_ref[3]
+    kb = lax.broadcasted_iota(jnp.int32, (BLOCK, 128), 0)
+    lane = lax.broadcasted_iota(jnp.int32, (BLOCK, 128), 1)
+    pick_row = lax.broadcasted_iota(jnp.int32, (128, 128), 0)
+    pick_lane = lax.broadcasted_iota(jnp.int32, (128, 128), 1)
+    per_list = (pick_row // 32 == pick_lane).astype(f32)
+    square = (BLOCK, BLOCK)
+    earlier = lax.broadcasted_iota(jnp.int32, square, 1) < lax.broadcasted_iota(
+        jnp.int32, square, 0
+    )
+    meta_lane = lax.broadcasted_iota(jnp.int32, (8, 128), 1)
+    meta = jnp.where(meta_lane == 0, z, jnp.where(meta_lane == 1, y, 0))
+    for peer, ref in enumerate((own_ref, side_ref, far_ref, last_ref)):
+        picks = ref[0:1, :].astype(f32).astype(jnp.int32)
+        mine = ((picks >> 2) & 3) == y
+        slot = ((z - (picks >> 4)) & (RING - 1)) * 4 + (picks & 3)
+        slot = jnp.where(mine, slot, -1)
+        counts = jnp.dot((slot == kb).astype(f32), per_list, preferred_element_type=f32)
+        present = jnp.where(counts > 0.5, 1.0, 0.0)
+        rank = jnp.dot(earlier.astype(f32), present, preferred_element_type=f32)
+        rank = jnp.where(counts > 0.5, rank, 1000.0).astype(jnp.int32)
+        for qb in range(4):
+            hit = rank[:, qb : qb + 1] == lane
+            g = peer * 4 + qb
+            ids_ref[g : g + 1, :] = (
+                jnp.sum(jnp.where(hit, kb + 1, 0), axis=0, keepdims=True) - 1
+            )
+            times = jnp.sum(
+                jnp.where(hit, counts[:, qb : qb + 1], 0.0), axis=0, keepdims=True
+            )
+            bias_ref[g : g + 1, :] = jnp.log(jnp.maximum(times, 1.0))
+        longest = jnp.max(jnp.sum(present, axis=0, keepdims=True)).astype(jnp.int32)
+        steps = (longest + PER_STEP - 1) // PER_STEP
+        meta = jnp.where(meta_lane == 2 + peer, steps, meta)
+    meta_ref[...] = meta
+
+
+def block_lists(place, own, side, far):
+    last = lambda at: pl.BlockSpec((16, 128), lambda i, *_: (at, 0))
+    whole = lambda rows: pl.BlockSpec((rows, 128), lambda i, *_: (0, 0))
+    return pl.pallas_call(
+        lists_kernel,
+        grid_spec=pltpu.PrefetchScalarGridSpec(
+            num_scalar_prefetch=1,
+            grid=(1,),
+            in_specs=[last(32), last(32), last(32), last(65)],
+            out_specs=[whole(8), whole(16), whole(16)],
+        ),
+        out_shape=[
+            jax.ShapeDtypeStruct((8, 128), jnp.int32),
+            jax.ShapeDtypeStruct((16, 128), jnp.int32),
+            jax.ShapeDtypeStruct((16, 128), jnp.float32),
+        ],
+        compiler_params=pltpu.CompilerParams(vmem_limit_bytes=8 << 20),
+        name="lists",
+    )(place, own, side, far, far)
 
 
 def shards(
@@ -409,8 +463,8 @@
     f32, bf16 = jnp.float32, jnp.bfloat16
 
     cosines, sines = rotary_tables(own, np.arange(SPAN))
-    place = jnp.stack([own, group]).astype(jnp.int32)
-    chunk = project(place, tokens, key_matrix, value_matrix, key_pool_weight, value_pool_weight)
+    place = jnp.stack([own, group, z, y]).astype(jnp.int32)
+    chunk = project(place, tokens, key_matrix, value_matrix, key_pool_weight.T, value_pool_weight.T)
     query_proj = jnp.dot(tokens, query_weight, preferred_element_type=f32)
     query_proj = query_proj.reshape(SPAN, 2, HEAD_SIZE)
     queries = rotate(query_proj, cosines[:, None, :], sines[:, None, :]).astype(bf16)
@@ -418,26 +472,22 @@
     picks = jnp.pad(chosen.astype(bf16).reshape(1, 128), ((0, 15), (0, 0)))
     sent = jnp.concatenate([by_block.reshape(512, HEAD_SIZE), picks], 0)
 
-    ring_up = [(i, (i + 1) % RING) for i in range(RING)]
-    ring_down = [(i, (i - 1) % RING) for i in range(RING)]
-    chunks = [None] * RING
-    chunks[0] = chunk
+    chunks = [chunk] + [None] * (RING - 1)
     up = down = chunk
-    near = [sent]
-
     for k in range(1, RING // 2 + 1):
-        up = lax.ppermute(up, "z", ring_up)
+        up = lax.ppermute(up, "z", [(i, i + 1) for i in range(k - 1, RING - 1)])
         chunks[k] = up
         if k < RING // 2:
-            down = lax.ppermute(down, "z", ring_down)
+            moved = [(i - k) % RING for i in range(RING // 2 - 1)]
+            down = lax.ppermute(down, "z", [((i + 1) % RING, i) for i in moved])
             chunks[RING - k] = down
-        if 1 <= k <= 3:
-            pairs = [(i, (i - k) % 4) for i in range(4)]
-            near.append(lax.ppermute(sent, "y", pairs))
+        if k == 2:
+            side = lax.ppermute(sent, "y", [(i, i ^ 1) for i in range(4)])
         if k == 4:
-            other_weight = lax.ppermute(out_weight, "c", [(0, 1), (1, 0)])
-
-    meta, ids, bias = block_lists(near, z, y)
+            both = jnp.concatenate([sent, side], 0)
+            far = lax.ppermute(both, "y", [(i, i ^ 2) for i in range(4)])
+    other_weight = lax.ppermute(out_weight, "c", [(0, 1), (1, 0)])
+    meta, ids, bias = block_lists(place, sent, side, far)
 
     own_tokens = lax.dynamic_index_in_dim(
         tokens.reshape(4, 2, 32, -1), c, 1, keepdims=False
@@ -447,7 +497,7 @@
         jnp.einsum("td,bdh->tbh", own_tokens, gate_cols, preferred_element_type=f32)
     ).reshape(128, 8)
 
-    partial = attend(meta, ids, bias, near, chunks)
+    partial = attend(meta, ids, bias, (sent, side, far), chunks)
     got = lax.all_to_all(partial, ("y", "c"), 0, 0, tiled=True)
     shares, log_all = merge(
         c.astype(jnp.int32).reshape(1), got, gates, out_weight, other_weight

time: 146 us -> 134 us (0.918)
  the two profiles are of different devices: /device:TPU:1 before, /device:TPU:384 now
where the time goes in v4:
time: 134 us; the launch traced here: 133 us
  starting transfers between devices  53.2 us (40%)
  waiting for transfers between devices  44.6 us (33%)
  Pallas kernels  16.6 us (12%)
  local copies, waits for them, and re-layouts  8.03 us (6%)
  other arithmetic  6.8 us (5%)
  matrix products  2.32 us (2%)
    ppermute x8, waiting for transfers between devices, shards(): up = lax.ppermute(up, 'z', [(i, i + 1) for i in range(k - 1, RING - 1)])  22 us
    ppermute x7, starting transfers between devices, shards(): down = lax.ppermute(down, 'z', [((i + 1) % RING, i) for i in moved])  18.7 us
    ppermute x8, starting transfers between devices, shards(): up = lax.ppermute(up, 'z', [(i, i + 1) for i in range(k - 1, RING - 1)])  16.4 us
    all_to_all x1, waiting for transfers between devices, shards(): got = lax.all_to_all(partial, ('y', 'c'), 0, 0, tiled=True)  14.2 us
    all_to_all x1, waiting for transfers between devices, shards(): pieces = lax.all_to_all(shares.reshape(4, 32, -1), 'x', 0, 0, tiled=True)  8.43 us
    pallas_call x1, Pallas kernels, attend(): pl.pallas_call(attend_kernel, grid_spec=pltpu.PrefetchScalarGridSpec(num_...  7.5 us
    pallas_call x1, Pallas kernels, project(): pl.pallas_call(project_kernel, grid_spec=pltpu.PrefetchScalarGridSpec(num...  4.91 us
    ppermute x1, starting transfers between devices, shards(): far = lax.ppermute(both, 'y', [(i, i ^ 2) for i in range(4)])  4.81 us
  transfers between devices with their start and end apart: 20, of which 7 were waited for; matrix products, arithmetic and copies ran while one was open for 11% of the time, Pallas kernels for 7%

profile of v4, /device:TPU:384, one launch (start us, length us, event | category | flops | bytes accessed | tf_op | source)
XLA Modules:
  0.0 132.6 jit_solution(3448154522068753444)
XLA Ops:
  0.7 0.7 pad_add_fusion.place_ref.meta_ref
  1.3 4.9 %project.1.refs_3_ = bf16[272,256]{1,0:T(8,128)(2,1)} custom-call(s32[4]{0:T(128)} %pad_add_fusion.place_ref.meta_ref, bf16[256,2048]{1,0:T(8,128)(2,1)} %tok_ref.1, bf16[2048,128]{1,0:T(8,128)(2,1)} %wk_ref.1, bf16[2048,128]{1,0:T(8,128)(2,1)} %wv_ref.1, f32[8,16]{1,0:T(8,128)} %bitcast.42, f32[8,16]{1,0:T(8,128)} %bitcast.43, ...), custom_call_target="tpu_custom_call" | custom-call | tf_op jit(solution)/shard_map/project/pallas_call | solution.py:107
  6.2 3.1 %collective-permute-start.2 = (bf16[272,256]{1,0:T(8,128)(2,1)}, bf16[272,256]{1,0:T(8,128)(2,1)S(1)}, u32[]{:S(2)}, u32[]{:S(2)}) collective-permute-start(bf16[272,256]{1,0:T(8,128)(2,1)} %project.1.refs_3_), channel_id=1, source_target_pairs={{0,32},{32,64},{64,96},{96,128},{128,160},{160,192},{192,224},{224... | collective-permute-start | bytes 417800 | tf_op jit(solution)/shard_map/ppermute | solution.py:478
  9.3 0.7 collective-permute-start.10
  10.0 5.1 %collective-permute-done.2.refs_4_ = bf16[272,256]{1,0:T(8,128)(2,1)S(1)} collective-permute-done((bf16[272,256]{1,0:T(8,128)(2,1)}, bf16[272,256]{1,0:T(8,128)(2,1)S(1)}, u32[]{:S(2)}, u32[]{:S(2)}) %collective-permute-start.2) | collective-permute-done | bytes 139296 | tf_op jit(solution)/shard_map/ppermute | solution.py:478
  15.1 1.9 %collective-permute-start.3 = (bf16[272,256]{1,0:T(8,128)(2,1)S(1)}, bf16[272,256]{1,0:T(8,128)(2,1)S(1)}, u32[]{:S(2)}, u32[]{:S(2)}) collective-permute-start(bf16[272,256]{1,0:T(8,128)(2,1)S(1)} %collective-permute-done.2.refs_4_), channel_id=1, source_target_pairs={{32,64},{64,96},{96,128},{128,160},{160,192},{192,224},{224,256},{... | collective-permute-start | bytes 417800 | tf_op jit(solution)/shard_map/ppermute | solution.py:478
  17.0 0.7 collective-permute-start.11
  17.7 5.5 %collective-permute-done.3.refs_5_ = bf16[272,256]{1,0:T(8,128)(2,1)S(1)} collective-permute-done((bf16[272,256]{1,0:T(8,128)(2,1)S(1)}, bf16[272,256]{1,0:T(8,128)(2,1)S(1)}, u32[]{:S(2)}, u32[]{:S(2)}) %collective-permute-start.3) | collective-permute-done | bytes 139296 | tf_op jit(solution)/shard_map/ppermute | solution.py:478
  23.2 1.9 %collective-permute-start.4 = (bf16[272,256]{1,0:T(8,128)(2,1)S(1)}, bf16[272,256]{1,0:T(8,128)(2,1)S(1)}, u32[]{:S(2)}, u32[]{:S(2)}) collective-permute-start(bf16[272,256]{1,0:T(8,128)(2,1)S(1)} %collective-permute-done.3.refs_5_), channel_id=1, source_target_pairs={{64,96},{96,128},{128,160},{160,192},{192,224},{224,256},{256,288}... | collective-permute-start | bytes 417800 | tf_op jit(solution)/shard_map/ppermute | solution.py:478
  25.2 1.2 fusion.7
  26.4 0.7 fusion.5
  27.1 0.7 collective-permute-start.12
  27.8 3.6 %collective-permute-done.4.refs_6_ = bf16[272,256]{1,0:T(8,128)(2,1)S(1)} collective-permute-done((bf16[272,256]{1,0:T(8,128)(2,1)S(1)}, bf16[272,256]{1,0:T(8,128)(2,1)S(1)}, u32[]{:S(2)}, u32[]{:S(2)}) %collective-permute-start.4) | collective-permute-done | bytes 139296 | tf_op jit(solution)/shard_map/ppermute | solution.py:478
  31.4 1.9 %collective-permute-start.5 = (bf16[272,256]{1,0:T(8,128)(2,1)S(1)}, bf16[272,256]{1,0:T(8,128)(2,1)S(1)}, u32[]{:S(2)}, u32[]{:S(2)}) collective-permute-start(bf16[272,256]{1,0:T(8,128)(2,1)S(1)} %collective-permute-done.4.refs_6_), channel_id=1, source_target_pairs={{96,128},{128,160},{160,192},{192,224},{224,256},{256,288},{288,32... | collective-permute-start | bytes 417800 | tf_op jit(solution)/shard_map/ppermute | solution.py:478
  33.4 1.3 collective-permute-start.13
  34.7 4.8 %collective-permute-done.5.refs_7_ = bf16[272,256]{1,0:T(8,128)(2,1)S(1)} collective-permute-done((bf16[272,256]{1,0:T(8,128)(2,1)S(1)}, bf16[272,256]{1,0:T(8,128)(2,1)S(1)}, u32[]{:S(2)}, u32[]{:S(2)}) %collective-permute-start.5) | collective-permute-done | bytes 139296 | tf_op jit(solution)/shard_map/ppermute | solution.py:478
  39.5 1.9 %collective-permute-start.6 = (bf16[272,256]{1,0:T(8,128)(2,1)S(1)}, bf16[272,256]{1,0:T(8,128)(2,1)S(1)}, u32[]{:S(2)}, u32[]{:S(2)}) collective-permute-start(bf16[272,256]{1,0:T(8,128)(2,1)S(1)} %collective-permute-done.5.refs_7_), channel_id=1, source_target_pairs={{128,160},{160,192},{192,224},{224,256},{256,288},{288,320},{320,3... | collective-permute-start | bytes 417800 | tf_op jit(solution)/shard_map/ppermute | solution.py:478
  41.5 1.7 %subtract_convert_fusion = (bf16[256,2,64]{0,2,1:T(8,128)(2,1)}, bf16[256,2,64]{0,2,1:T(8,128)(2,1)}) fusion(f32[256,2,128]{0,2,1:T(8,128)} %bitcast.39, f32[256,64]{0,1:T(8,128)S(1)} %get-tuple-element.15, f32[256,64]{0,1:T(8,128)S(1)} %get-tuple-element.14), kind=kLoop, calls=%fused_computation.8 | loop fusion | flops 262144 | bytes 524288 | tf_op jit(solution)/shard_map/convert.4
  43.1 1.0 concatenate.16
  44.2 1.6 %concatenate.17 = bf16[4,64,2,64]{1,0,3,2:T(4,128)(2,1)} reshape(bf16[256,2,64]{0,2,1:T(8,128)(2,1)} %get-tuple-element.13) | data formatting | bytes 131072 | tf_op jit(solution)/shard_map/concatenate | solution.py:43
  45.8 1.8 %maximum_bitcast_fusion = bf16[4,2,64,128]{2,0,3,1:T(4,128)(2,1)} fusion(bf16[4,64,2,64]{1,0,3,2:T(4,128)(2,1)} %concatenate.17, bf16[4,64,2,64]{1,0,3,2:T(4,128)(2,1)S(1)} %concatenate.16), kind=kLoop, calls=%fused_computation.5 | loop fusion | flops 65536 | bytes 262144 | tf_op jit(solution)/shard_map/transpose | solution.py:471
  47.6 1.8 %copy.22 = bf16[4,2,64,128]{3,2,1,0:T(8,128)(2,1)} copy(bf16[4,2,64,128]{2,0,3,1:T(4,128)(2,1)} %maximum_bitcast_fusion) | data formatting | bytes 262144 | tf_op jit(solution)/shard_map/transpose | solution.py:471
  49.4 0.1 reshape.46
  49.5 5.1 %collective-permute-start.14 = (bf16[272,256]{1,0:T(8,128)(2,1)S(1)}, bf16[272,256]{1,0:T(8,128)(2,1)S(1)}, u32[]{:S(2)}, u32[]{:S(2)}) collective-permute-start(bf16[272,256]{1,0:T(8,128)(2,1)S(1)} %collective-permute-done.13.refs_15_), channel_id=1, source_target_pairs={{384,352},{416,384},{448,416},{480,448},{0,480},{32,0},{64,32},{38... | collective-permute-start | bytes 417800 | tf_op jit(solution)/shard_map/ppermute | solution.py:482
  54.6 1.9 %collective-permute-start.7 = (bf16[272,256]{1,0:T(8,128)(2,1)S(1)}, bf16[272,256]{1,0:T(8,128)(2,1)S(1)}, u32[]{:S(2)}, u32[]{:S(2)}) collective-permute-start(bf16[272,256]{1,0:T(8,128)(2,1)S(1)} %collective-permute-done.6.refs_8_), channel_id=1, source_target_pairs={{160,192},{192,224},{224,256},{256,288},{288,320},{320,352},{352,3... | collective-permute-start | bytes 417800 | tf_op jit(solution)/shard_map/ppermute | solution.py:478
  56.6 0.9 pad_maximum_fusion.1.own_ref.refs_0_
  57.5 3.5 %collective-permute-start = (bf16[528,128]{1,0:T(8,128)(2,1)S(1)}, bf16[528,128]{1,0:T(8,128)(2,1)S(1)}, u32[]{:S(2)}, u32[]{:S(2)}) collective-permute-start(bf16[528,128]{1,0:T(8,128)(2,1)S(1)} %pad_maximum_fusion.1.own_ref.refs_0_), channel_id=1, source_target_pairs={{0,8},{8,0},{16,24},{24,16},{1,9},{9,1},{17,25},{25,17},{2,10},{10... | collective-permute-start | bytes 405512 | tf_op jit(solution)/shard_map/ppermute | solution.py:485
  61.0 5.1 %collective-permute-start.15 = (bf16[272,256]{1,0:T(8,128)(2,1)S(1)}, bf16[272,256]{1,0:T(8,128)(2,1)S(1)}, u32[]{:S(2)}, u32[]{:S(2)}) collective-permute-start(bf16[272,256]{1,0:T(8,128)(2,1)S(1)} %collective-permute-done.14.refs_14_), channel_id=1, source_target_pairs={{352,320},{384,352},{416,384},{448,416},{480,448},{0,480},{32,0},{... | collective-permute-start | bytes 417800 | tf_op jit(solution)/shard_map/ppermute | solution.py:482
  66.2 1.9 %collective-permute-start.8 = (bf16[272,256]{1,0:T(8,128)(2,1)S(1)}, bf16[272,256]{1,0:T(8,128)(2,1)S(1)}, u32[]{:S(2)}, u32[]{:S(2)}) collective-permute-start(bf16[272,256]{1,0:T(8,128)(2,1)S(1)} %collective-permute-done.7.refs_9_), channel_id=1, source_target_pairs={{192,224},{224,256},{256,288},{288,320},{320,352},{352,384},{384,4... | collective-permute-start | bytes 417800 | tf_op jit(solution)/shard_map/ppermute | solution.py:478
  68.1 0.9 pad_maximum_fusion
  69.0 4.8 %collective-permute-start.1 = (bf16[1056,128]{1,0:T(8,128)(2,1)S(1)}, bf16[1056,128]{1,0:T(8,128)(2,1)S(1)}, u32[]{:S(2)}, u32[]{:S(2)}) collective-permute-start(bf16[1056,128]{1,0:T(8,128)(2,1)S(1)} %pad_maximum_fusion), channel_id=1, source_target_pairs={{0,16},{8,24},{16,0},{24,8},{1,17},{9,25},{17,1},{25,9},{2,18},{10... | collective-permute-start | bytes 811016 | tf_op jit(solution)/shard_map/ppermute | solution.py:488
  73.8 5.1 %collective-permute-start.16 = (bf16[272,256]{1,0:T(8,128)(2,1)S(1)}, bf16[272,256]{1,0:T(8,128)(2,1)S(1)}, u32[]{:S(2)}, u32[]{:S(2)}) collective-permute-start(bf16[272,256]{1,0:T(8,128)(2,1)S(1)} %collective-permute-done.15.refs_13_), channel_id=1, source_target_pairs={{320,288},{352,320},{384,352},{416,384},{448,416},{480,448},{0,480... | collective-permute-start | bytes 417800 | tf_op jit(solution)/shard_map/ppermute | solution.py:482
  79.0 1.9 %collective-permute-start.9 = (bf16[272,256]{1,0:T(8,128)(2,1)S(1)}, bf16[272,256]{1,0:T(8,128)(2,1)S(1)}, u32[]{:S(2)}, u32[]{:S(2)}) collective-permute-start(bf16[272,256]{1,0:T(8,128)(2,1)S(1)} %collective-permute-done.8.refs_10_), channel_id=1, source_target_pairs={{224,256},{256,288},{288,320},{320,352},{352,384},{384,416},{416,4... | collective-permute-start | bytes 417800 | tf_op jit(solution)/shard_map/ppermute | solution.py:478
  80.9 1.9 %collective-permute-start.17 = (bf16[256,2048]{1,0:T(8,128)(2,1)S(1)}, bf16[256,2048]{1,0:T(8,128)(2,1)}, u32[]{:S(2)}, u32[]{:S(2)}) collective-permute-start(bf16[256,2048]{1,0:T(8,128)(2,1)S(1)} %copy-done.1), channel_id=1, source_target_pairs={{0,1},{1,0},{2,3},{3,2},{4,5},{5,4},{6,7},{7,6},{8,9},{9,8},{10,11... | collective-permute-start | bytes 3145736 | tf_op jit(solution)/shard_map/ppermute | solution.py:489
  82.9 1.4 %lists.1 = (s32[8,128]{1,0:T(8,128)S(1)}, s32[16,128]{1,0:T(8,128)S(1)}, f32[16,128]{1,0:T(8,128)S(1)}) custom-call(s32[4]{0:T(128)S(1)} %copy-done.4, bf16[528,128]{1,0:T(8,128)(2,1)S(1)} %pad_maximum_fusion.1.own_ref.refs_0_, bf16[528,128]{1,0:T(8,128)(2,1)S(1)} %collective-permute-done.side_ref.refs_1_, ...), custom_call_target="tpu_custom_call" | custom-call | tf_op jit(solution)/shard_map/lists/pallas_call | solution.py:430
  84.3 2.9 %collective-permute-done.9.refs_11_ = bf16[272,256]{1,0:T(8,128)(2,1)S(1)} collective-permute-done((bf16[272,256]{1,0:T(8,128)(2,1)S(1)}, bf16[272,256]{1,0:T(8,128)(2,1)S(1)}, u32[]{:S(2)}, u32[]{:S(2)}) %collective-permute-start.9) | collective-permute-done | bytes 139296 | tf_op jit(solution)/shard_map/ppermute | solution.py:478
  87.2 7.5 %attend.1 = bf16[8,272,256]{2,1,0:T(8,128)(2,1)} custom-call(s32[8,128]{1,0:T(8,128)S(1)} %get-tuple-element.7.meta_ref, s32[16,128]{1,0:T(8,128)S(1)} %get-tuple-element.8.ids_ref, f32[16,128]{1,0:T(8,128)S(1)} %get-tuple-element.9.bias_ref, bf16[528,128]{1,0:T(8,128)(2,1)S(1)} %pad_maximum_fusion.1.own_ref.refs_0_, ...), custom_call_target="tpu_custom_call" | custom-call | tf_op jit(solution)/shard_map/attend/pallas_call | solution.py:291
  94.7 3.6 %all-to-all-start = ((bf16[8,272,256]{2,1,0:T(8,128)(2,1)}), bf16[8,272,256]{2,1,0:T(8,128)(2,1)S(1)}, u32[]{:S(2)}, u32[]{:S(2)}) async-start(bf16[8,272,256]{2,1,0:T(8,128)(2,1)} %attend.1), calls=%async_computation | async-start | bytes 2228224 | tf_op jit(solution)/shard_map/all_to_all | solution.py:501
  98.2 1.1 constant_dynamic-slice_fusion.1
  99.3 1.1 fusion.2
  100.4 0.1 copy.24.gate_ref
  100.6 14.2 %all-to-all-done.got_ref = bf16[8,272,256]{2,1,0:T(8,128)(2,1)S(1)} async-done(((bf16[8,272,256]{2,1,0:T(8,128)(2,1)}), bf16[8,272,256]{2,1,0:T(8,128)(2,1)S(1)}, u32[]{:S(2)}, u32[]{:S(2)}) %all-to-all-start) | async-done | bytes 1114144 | tf_op jit(solution)/shard_map/all_to_all | solution.py:501
  114.8 2.8 %merge.1 = (bf16[128,2048]{1,0:T(8,128)(2,1)S(1)}, f32[2,2,256]{2,1,0:T(2,128)S(1)}) custom-call(s32[1]{0:T(128)} %bitcast.1.meta_ref, bf16[8,272,256]{2,1,0:T(8,128)(2,1)S(1)} %all-to-all-done.got_ref, f32[128,8]{1,0:T(8,128)S(1)} %copy.24.gate_ref, bf16[256,2048]{1,0:T(8,128)(2,1)S(1)} %copy-done.1, bf16[256,2048]{1,0:T(8,128)(2,1)} %collective-permute-done.17.other_ref), custom_call_target="tpu_custom_call" | custom-call | tf_op jit(solution)/shard_map/merge/pallas_call | solution.py:359
  117.6 0.8 copy-done.3
  118.3 4.3 %all-to-all-start.1 = ((bf16[4,32,2048]{2,1,0:T(8,128)(2,1)}), bf16[4,32,2048]{2,1,0:T(8,128)(2,1)S(1)}, u32[]{:S(2)}, u32[]{:S(2)}) async-start(bf16[4,32,2048]{2,1,0:T(8,128)(2,1)} %bitcast.34), calls=%async_computation.1 | async-start | bytes 1048576 | tf_op jit(solution)/shard_map/all_to_all | solution.py:507
  122.7 0.7 reshape.52
  123.4 8.4 %all-to-all-done.1 = bf16[4,32,2048]{2,1,0:T(8,128)(2,1)S(1)} async-done(((bf16[4,32,2048]{2,1,0:T(8,128)(2,1)}), bf16[4,32,2048]{2,1,0:T(8,128)(2,1)S(1)}, u32[]{:S(2)}, u32[]{:S(2)}) %all-to-all-start.1) | async-done | bytes 524320 | tf_op jit(solution)/shard_map/all_to_all | solution.py:507
  131.8 0.7 reduce_sum.12
  (36 shorter events, 0.3 us)
Async XLA Ops:
  0.6 24.5 %copy-start = (bf16[2048,256]{1,0:T(8,128)(2,1)S(1)}, bf16[2048,256]{1,0:T(8,128)(2,1)}, u32[]{:S(2)}) copy-start(bf16[2048,256]{1,0:T(8,128)(2,1)} %param.16) | copy-start | bytes 3145732
  1.3 23.9 %copy-start.5 = (bf16[256,2048]{1,0:T(8,128)(2,1)S(1)}, bf16[256,2048]{1,0:T(8,128)(2,1)}, u32[]{:S(2)}) copy-start(bf16[256,2048]{1,0:T(8,128)(2,1)} %tok_ref.1) | copy-start | bytes 3145732
  6.2 27.1 %copy-start.6 = (f32[256,64]{0,1:T(8,128)S(1)}, f32[256,64]{0,1:T(8,128)}, u32[]{:S(2)}) copy-start(f32[256,64]{0,1:T(8,128)} %constant.53.clone) | copy-start | bytes 196612
  6.2 27.1 %copy-start.7 = (f32[256,64]{0,1:T(8,128)S(1)}, f32[256,64]{0,1:T(8,128)}, u32[]{:S(2)}) copy-start(f32[256,64]{0,1:T(8,128)} %constant.54.clone) | copy-start | bytes 196612
  6.2 8.9 %collective-permute-start.2 = (bf16[272,256]{1,0:T(8,128)(2,1)}, bf16[272,256]{1,0:T(8,128)(2,1)S(1)}, u32[]{:S(2)}, u32[]{:S(2)}) collective-permute-start(bf16[272,256]{1,0:T(8,128)(2,1)} %project.1.refs_3_), channel_id=1, source_target_pairs={{0,32},{32,64},{64,96},{96,128},{128,160},{160,192},{192,224},{224... | collective-permute-start | bytes 417800 | tf_op jit(solution)/shard_map/ppermute | solution.py:478
  9.3 7.7 %collective-permute-start.10 = (bf16[272,256]{1,0:T(8,128)(2,1)}, bf16[272,256]{1,0:T(8,128)(2,1)S(1)}, u32[]{:S(2)}, u32[]{:S(2)}) collective-permute-start(bf16[272,256]{1,0:T(8,128)(2,1)} %project.1.refs_3_), channel_id=1, source_target_pairs={{0,480},{32,0},{64,32},{96,64},{128,96},{160,128},{192,160},{1,481... | collective-permute-start | bytes 417800 | tf_op jit(solution)/shard_map/ppermute | solution.py:482
  15.1 8.1 %collective-permute-start.3 = (bf16[272,256]{1,0:T(8,128)(2,1)S(1)}, bf16[272,256]{1,0:T(8,128)(2,1)S(1)}, u32[]{:S(2)}, u32[]{:S(2)}) collective-permute-start(bf16[272,256]{1,0:T(8,128)(2,1)S(1)} %collective-permute-done.2.refs_4_), channel_id=1, source_target_pairs={{32,64},{64,96},{96,128},{128,160},{160,192},{192,224},{224,256},{... | collective-permute-start | bytes 417800 | tf_op jit(solution)/shard_map/ppermute | solution.py:478
  17.0 10.1 %collective-permute-start.11 = (bf16[272,256]{1,0:T(8,128)(2,1)S(1)}, bf16[272,256]{1,0:T(8,128)(2,1)S(1)}, u32[]{:S(2)}, u32[]{:S(2)}) collective-permute-start(bf16[272,256]{1,0:T(8,128)(2,1)S(1)} %collective-permute-done.10.refs_18_), channel_id=1, source_target_pairs={{480,448},{0,480},{32,0},{64,32},{96,64},{128,96},{160,128},{481,4... | collective-permute-start | bytes 417800 | tf_op jit(solution)/shard_map/ppermute | solution.py:482
  23.2 8.1 %collective-permute-start.4 = (bf16[272,256]{1,0:T(8,128)(2,1)S(1)}, bf16[272,256]{1,0:T(8,128)(2,1)S(1)}, u32[]{:S(2)}, u32[]{:S(2)}) collective-permute-start(bf16[272,256]{1,0:T(8,128)(2,1)S(1)} %collective-permute-done.3.refs_5_), channel_id=1, source_target_pairs={{64,96},{96,128},{128,160},{160,192},{192,224},{224,256},{256,288}... | collective-permute-start | bytes 417800 | tf_op jit(solution)/shard_map/ppermute | solution.py:478
  26.4 23.0 %copy-start.8 = (s32[4,32]{1,0:T(4,128)S(1)}, s32[4,32]{1,0:T(4,128)}, u32[]{:S(2)}) copy-start(s32[4,32]{1,0:T(4,128)} %param.23) | copy-start | bytes 1540
  27.1 6.3 %collective-permute-start.12 = (bf16[272,256]{1,0:T(8,128)(2,1)S(1)}, bf16[272,256]{1,0:T(8,128)(2,1)S(1)}, u32[]{:S(2)}, u32[]{:S(2)}) collective-permute-start(bf16[272,256]{1,0:T(8,128)(2,1)S(1)} %collective-permute-done.11.refs_17_), channel_id=1, source_target_pairs={{448,416},{480,448},{0,480},{32,0},{64,32},{96,64},{128,96},{449,4... | collective-permute-start | bytes 417800 | tf_op jit(solution)/shard_map/ppermute | solution.py:482
  31.4 8.1 %collective-permute-start.5 = (bf16[272,256]{1,0:T(8,128)(2,1)S(1)}, bf16[272,256]{1,0:T(8,128)(2,1)S(1)}, u32[]{:S(2)}, u32[]{:S(2)}) collective-permute-start(bf16[272,256]{1,0:T(8,128)(2,1)S(1)} %collective-permute-done.4.refs_6_), channel_id=1, source_target_pairs={{96,128},{128,160},{160,192},{192,224},{224,256},{256,288},{288,32... | collective-permute-start | bytes 417800 | tf_op jit(solution)/shard_map/ppermute | solution.py:478
  33.4 16.1 %collective-permute-start.13 = (bf16[272,256]{1,0:T(8,128)(2,1)S(1)}, bf16[272,256]{1,0:T(8,128)(2,1)S(1)}, u32[]{:S(2)}, u32[]{:S(2)}) collective-permute-start(bf16[272,256]{1,0:T(8,128)(2,1)S(1)} %collective-permute-done.12.refs_16_), channel_id=1, source_target_pairs={{416,384},{448,416},{480,448},{0,480},{32,0},{64,32},{96,64},{417,... | collective-permute-start | bytes 417800 | tf_op jit(solution)/shard_map/ppermute | solution.py:482
  39.5 15.1 %collective-permute-start.6 = (bf16[272,256]{1,0:T(8,128)(2,1)S(1)}, bf16[272,256]{1,0:T(8,128)(2,1)S(1)}, u32[]{:S(2)}, u32[]{:S(2)}) collective-permute-start(bf16[272,256]{1,0:T(8,128)(2,1)S(1)} %collective-permute-done.5.refs_7_), channel_id=1, source_target_pairs={{128,160},{160,192},{192,224},{224,256},{256,288},{288,320},{320,3... | collective-permute-start | bytes 417800 | tf_op jit(solution)/shard_map/ppermute | solution.py:478
  43.1 37.8 %copy-start.1 = (bf16[256,2048]{1,0:T(8,128)(2,1)S(1)}, bf16[256,2048]{1,0:T(8,128)(2,1)}, u32[]{:S(2)}) copy-start(bf16[256,2048]{1,0:T(8,128)(2,1)} %own_ref.1) | copy-start | bytes 3145732
  43.1 39.7 %copy-start.4 = (s32[4]{0:T(128)S(1)}, s32[4]{0:T(128)}, u32[]{:S(2)}) copy-start(s32[4]{0:T(128)} %pad_add_fusion.place_ref.meta_ref) | copy-start | bytes 52
  47.6 39.6 %copy-start.2 = (bf16[272,256]{1,0:T(8,128)(2,1)S(1)}, bf16[272,256]{1,0:T(8,128)(2,1)}, u32[]{:S(2)}) copy-start(bf16[272,256]{1,0:T(8,128)(2,1)} %project.1.refs_3_) | copy-start | bytes 417796
  49.5 11.5 %collective-permute-start.14 = (bf16[272,256]{1,0:T(8,128)(2,1)S(1)}, bf16[272,256]{1,0:T(8,128)(2,1)S(1)}, u32[]{:S(2)}, u32[]{:S(2)}) collective-permute-start(bf16[272,256]{1,0:T(8,128)(2,1)S(1)} %collective-permute-done.13.refs_15_), channel_id=1, source_target_pairs={{384,352},{416,384},{448,416},{480,448},{0,480},{32,0},{64,32},{38... | collective-permute-start | bytes 417800 | tf_op jit(solution)/shard_map/ppermute | solution.py:482
  54.6 11.5 %collective-permute-start.7 = (bf16[272,256]{1,0:T(8,128)(2,1)S(1)}, bf16[272,256]{1,0:T(8,128)(2,1)S(1)}, u32[]{:S(2)}, u32[]{:S(2)}) collective-permute-start(bf16[272,256]{1,0:T(8,128)(2,1)S(1)} %collective-permute-done.6.refs_8_), channel_id=1, source_target_pairs={{160,192},{192,224},{224,256},{256,288},{288,320},{320,352},{352,3... | collective-permute-start | bytes 417800 | tf_op jit(solution)/shard_map/ppermute | solution.py:478
  57.5 10.6 %collective-permute-start = (bf16[528,128]{1,0:T(8,128)(2,1)S(1)}, bf16[528,128]{1,0:T(8,128)(2,1)S(1)}, u32[]{:S(2)}, u32[]{:S(2)}) collective-permute-start(bf16[528,128]{1,0:T(8,128)(2,1)S(1)} %pad_maximum_fusion.1.own_ref.refs_0_), channel_id=1, source_target_pairs={{0,8},{8,0},{16,24},{24,16},{1,9},{9,1},{17,25},{25,17},{2,10},{10... | collective-permute-start | bytes 405512 | tf_op jit(solution)/shard_map/ppermute | solution.py:485
  61.0 12.8 %collective-permute-start.15 = (bf16[272,256]{1,0:T(8,128)(2,1)S(1)}, bf16[272,256]{1,0:T(8,128)(2,1)S(1)}, u32[]{:S(2)}, u32[]{:S(2)}) collective-permute-start(bf16[272,256]{1,0:T(8,128)(2,1)S(1)} %collective-permute-done.14.refs_14_), channel_id=1, source_target_pairs={{352,320},{384,352},{416,384},{448,416},{480,448},{0,480},{32,0},{... | collective-permute-start | bytes 417800 | tf_op jit(solution)/shard_map/ppermute | solution.py:482
  66.2 12.8 %collective-permute-start.8 = (bf16[272,256]{1,0:T(8,128)(2,1)S(1)}, bf16[272,256]{1,0:T(8,128)(2,1)S(1)}, u32[]{:S(2)}, u32[]{:S(2)}) collective-permute-start(bf16[272,256]{1,0:T(8,128)(2,1)S(1)} %collective-permute-done.7.refs_9_), channel_id=1, source_target_pairs={{192,224},{224,256},{256,288},{288,320},{320,352},{352,384},{384,4... | collective-permute-start | bytes 417800 | tf_op jit(solution)/shard_map/ppermute | solution.py:478
  69.0 13.8 %collective-permute-start.1 = (bf16[1056,128]{1,0:T(8,128)(2,1)S(1)}, bf16[1056,128]{1,0:T(8,128)(2,1)S(1)}, u32[]{:S(2)}, u32[]{:S(2)}) collective-permute-start(bf16[1056,128]{1,0:T(8,128)(2,1)S(1)} %pad_maximum_fusion), channel_id=1, source_target_pairs={{0,16},{8,24},{16,0},{24,8},{1,17},{9,25},{17,1},{25,9},{2,18},{10... | collective-permute-start | bytes 811016 | tf_op jit(solution)/shard_map/ppermute | solution.py:488
  73.8 10.4 %collective-permute-start.16 = (bf16[272,256]{1,0:T(8,128)(2,1)S(1)}, bf16[272,256]{1,0:T(8,128)(2,1)S(1)}, u32[]{:S(2)}, u32[]{:S(2)}) collective-permute-start(bf16[272,256]{1,0:T(8,128)(2,1)S(1)} %collective-permute-done.15.refs_13_), channel_id=1, source_target_pairs={{320,288},{352,320},{384,352},{416,384},{448,416},{480,448},{0,480... | collective-permute-start | bytes 417800 | tf_op jit(solution)/shard_map/ppermute | solution.py:482
  79.0 8.2 %collective-permute-start.9 = (bf16[272,256]{1,0:T(8,128)(2,1)S(1)}, bf16[272,256]{1,0:T(8,128)(2,1)S(1)}, u32[]{:S(2)}, u32[]{:S(2)}) collective-permute-start(bf16[272,256]{1,0:T(8,128)(2,1)S(1)} %collective-permute-done.8.refs_10_), channel_id=1, source_target_pairs={{224,256},{256,288},{288,320},{320,352},{352,384},{384,416},{416,4... | collective-permute-start | bytes 417800 | tf_op jit(solution)/shard_map/ppermute | solution.py:478
  80.9 19.6 %collective-permute-start.17 = (bf16[256,2048]{1,0:T(8,128)(2,1)S(1)}, bf16[256,2048]{1,0:T(8,128)(2,1)}, u32[]{:S(2)}, u32[]{:S(2)}) collective-permute-start(bf16[256,2048]{1,0:T(8,128)(2,1)S(1)} %copy-done.1), channel_id=1, source_target_pairs={{0,1},{1,0},{2,3},{3,2},{4,5},{5,4},{6,7},{7,6},{8,9},{9,8},{10,11... | collective-permute-start | bytes 3145736 | tf_op jit(solution)/shard_map/ppermute | solution.py:489
  94.7 20.1 %all-to-all-start = ((bf16[8,272,256]{2,1,0:T(8,128)(2,1)}), bf16[8,272,256]{2,1,0:T(8,128)(2,1)S(1)}, u32[]{:S(2)}, u32[]{:S(2)}) async-start(bf16[8,272,256]{2,1,0:T(8,128)(2,1)} %attend.1), calls=%async_computation | async-start | bytes 2228224 | tf_op jit(solution)/shard_map/all_to_all | solution.py:501
  117.6 0.8 copy-start.3
  118.3 13.5 %all-to-all-start.1 = ((bf16[4,32,2048]{2,1,0:T(8,128)(2,1)}), bf16[4,32,2048]{2,1,0:T(8,128)(2,1)S(1)}, u32[]{:S(2)}, u32[]{:S(2)}) async-start(bf16[4,32,2048]{2,1,0:T(8,128)(2,1)} %bitcast.34), calls=%async_computation.1 | async-start | bytes 1048576 | tf_op jit(solution)/shard_map/all_to_all | solution.py:507

commit v5 on v4

--- a/solution.py
+++ b/solution.py
@@ -18,10 +18,12 @@
 SPAN = 256
 STATS = 16
 PER_STEP = 10
-PEERS = 1
+PEERS = 2
 POOLED = 16
 RING = 16
 QROWS = 528
+UP_LEAPS = (3,)
+DOWN_LEAPS = (3,)
 SCALE = HEAD_SIZE**-0.5
 
 
@@ -53,8 +55,10 @@
         k_ref[...] = jnp.zeros_like(k_ref)
         v_ref[...] = jnp.zeros_like(v_ref)
 
-    k_ref[...] += jnp.dot(tok_ref[...], wk_ref[...], preferred_element_type=jnp.float32)
-    v_ref[...] += jnp.dot(tok_ref[...], wv_ref[...], preferred_element_type=jnp.float32)
+    both = jnp.concatenate([wk_ref[...], wv_ref[...]], 1)
+    kv = jnp.dot(tok_ref[...], both, preferred_element_type=jnp.float32)
+    k_ref[...] += kv[:, :HEAD_SIZE]
+    v_ref[...] += kv[:, HEAD_SIZE:]
 
     @pl.when(step == pl.num_programs(0) - 1)
     def _():
@@ -103,7 +107,7 @@
     spans = np.arange(64, dtype=np.float64)[:, None] * SPAN * inverse[None, :]
     local = jnp.asarray(np.stack([np.cos(local), np.sin(local)]), jnp.float32)
     spans = jnp.asarray(np.stack([np.cos(spans), np.sin(spans)]), jnp.float32)
-    depth = 512
+    depth = 2048
     return pl.pallas_call(
         project_kernel,
         grid_spec=pltpu.PrefetchScalarGridSpec(
@@ -473,19 +477,27 @@
     sent = jnp.concatenate([by_block.reshape(512, HEAD_SIZE), picks], 0)
 
     chunks = [chunk] + [None] * (RING - 1)
-    up = down = chunk
+
+    def step_up(k):
+        leap = k if k in UP_LEAPS else 1
+        pairs = [(i, i + leap) for i in range(k - leap, RING - leap)]
+        source = chunk if k == leap else chunks[k - 1]
+        chunks[k] = lax.ppermute(source, "z", pairs)
+
+    def step_down(k):
+        leap = k if k in DOWN_LEAPS else 1
+        ends = [(i - k) % RING for i in range(RING // 2 - 1)]
+        pairs = [((i + leap) % RING, i) for i in ends]
+        source = chunk if k == leap else chunks[RING - k + 1]
+        chunks[RING - k] = lax.ppermute(source, "z", pairs)
+
     for k in range(1, RING // 2 + 1):
-        up = lax.ppermute(up, "z", [(i, i + 1) for i in range(k - 1, RING - 1)])
-        chunks[k] = up
+        step_up(k)
         if k < RING // 2:
-            moved = [(i - k) % RING for i in range(RING // 2 - 1)]
-            down = lax.ppermute(down, "z", [((i + 1) % RING, i) for i in moved])
-            chunks[RING - k] = down
-        if k == 2:
-            side = lax.ppermute(sent, "y", [(i, i ^ 1) for i in range(4)])
-        if k == 4:
-            both = jnp.concatenate([sent, side], 0)
-            far = lax.ppermute(both, "y", [(i, i ^ 2) for i in range(4)])
+            step_down(k)
+    side = lax.ppermute(sent, "y", [(i, i ^ 1) for i in range(4)])
+    both = jnp.concatenate([sent, side], 0)
+    far = lax.ppermute(both, "y", [(i, i ^ 2) for i in range(4)])
     other_weight = lax.ppermute(out_weight, "c", [(0, 1), (1, 0)])
     meta, ids, bias = block_lists(place, sent, side, far)
 

time: 134 us -> 118 us (0.88)
  the two profiles are of different devices: /device:TPU:384 before, /device:TPU:1 now
where the time goes in v5:
time: 118 us; the launch traced here: 116 us
  starting transfers between devices  68.9 us (58%)
  waiting for transfers between devices  24.4 us (21%)
  Pallas kernels  14.7 us (12%)
  local copies, waits for them, and re-layouts  3.98 us (3%)
  other arithmetic  1.71 us (1%)
  matrix products  1.63 us (1%)
    ppermute x7, starting transfers between devices, step_down(): chunks[RING - k] = lax.ppermute(source, 'z', pairs)  35.2 us
    all_to_all x1, waiting for transfers between devices, shards(): got = lax.all_to_all(partial, ('y', 'c'), 0, 0, tiled=True)  13.3 us
    ppermute x8, starting transfers between devices, step_up(): chunks[k] = lax.ppermute(source, 'z', pairs)  12.4 us
    all_to_all x1, waiting for transfers between devices, shards(): pieces = lax.all_to_all(shares.reshape(4, 32, -1), 'x', 0, 0, tiled=True)  7.31 us
    pallas_call x1, Pallas kernels, attend(): pl.pallas_call(attend_kernel, grid_spec=pltpu.PrefetchScalarGridSpec(num_...  6.95 us
    ppermute x1, starting transfers between devices, shards(): other_weight = lax.ppermute(out_weight, 'c', [(0, 1), (1, 0)])  6.06 us
    ppermute x1, starting transfers between devices, shards(): far = lax.ppermute(both, 'y', [(i, i ^ 2) for i in range(4)])  4.53 us
    all_to_all x1, starting transfers between devices, shards(): pieces = lax.all_to_all(shares.reshape(4, 32, -1), 'x', 0, 0, tiled=True)  4.03 us
  transfers between devices with their start and end apart: 20, of which 3 were waited for; matrix products, arithmetic and copies ran while one was open for 4% of the time, Pallas kernels for 7%

profile of v5, /device:TPU:1, one launch (start us, length us, event | category | flops | bytes accessed | tf_op | source)
XLA Modules:
  0.0 116.5 jit_solution(3235068319273487256)
XLA Ops:
  0.6 0.0 copy-start
  0.7 0.6 pad_add_fusion.place_ref.meta_ref
  1.3 3.6 %project.1.refs_3_ = bf16[272,256]{1,0:T(8,128)(2,1)} custom-call(s32[4]{0:T(128)} %pad_add_fusion.place_ref.meta_ref, bf16[256,2048]{1,0:T(8,128)(2,1)} %tok_ref.1, bf16[2048,128]{1,0:T(8,128)(2,1)} %wk_ref.1, bf16[2048,128]{1,0:T(8,128)(2,1)} %wv_ref.1, f32[8,16]{1,0:T(8,128)} %bitcast.42, f32[8,16]{1,0:T(8,128)} %bitcast.43, ...), custom_call_target="tpu_custom_call" | custom-call | tf_op jit(solution)/shard_map/project/pallas_call | solution.py:111
  4.8 7.1 %collective-permute-start.4 = (bf16[272,256]{1,0:T(8,128)(2,1)}, bf16[272,256]{1,0:T(8,128)(2,1)S(1)}, u32[]{:S(2)}, u32[]{:S(2)}) collective-permute-start(bf16[272,256]{1,0:T(8,128)(2,1)} %project.1.refs_3_), channel_id=1, source_target_pairs={{0,96},{32,128},{64,160},{96,192},{128,224},{160,256},{192,288},{2... | collective-permute-start | bytes 417800 | tf_op jit(solution)/shard_map/ppermute | solution.py:485
  11.9 7.0 %collective-permute-start.10 = (bf16[272,256]{1,0:T(8,128)(2,1)}, bf16[272,256]{1,0:T(8,128)(2,1)S(1)}, u32[]{:S(2)}, u32[]{:S(2)}) collective-permute-start(bf16[272,256]{1,0:T(8,128)(2,1)} %project.1.refs_3_), channel_id=1, source_target_pairs={{0,416},{32,448},{64,480},{96,0},{128,32},{160,64},{192,96},{1,417... | collective-permute-start | bytes 417800 | tf_op jit(solution)/shard_map/ppermute | solution.py:492
  19.0 0.0 copy-start.6
  19.0 0.0 copy-start.7
  19.0 0.5 fusion.7
  19.5 0.0 copy-start.8
  19.6 0.7 fusion.5
  20.3 0.1 multiply_subtract_fusion
  20.4 0.7 collective-permute-start.5
  21.1 0.0 copy-start.1
  21.1 0.1 concatenate.16
  21.3 0.1 concatenate.17
  21.4 0.2 maximum_bitcast_fusion
  21.6 0.2 copy.22
  21.8 0.1 reshape.46
  21.9 3.7 %collective-permute-done.10.refs_16_ = bf16[272,256]{1,0:T(8,128)(2,1)S(1)} collective-permute-done((bf16[272,256]{1,0:T(8,128)(2,1)}, bf16[272,256]{1,0:T(8,128)(2,1)S(1)}, u32[]{:S(2)}, u32[]{:S(2)}) %collective-permute-start.10) | collective-permute-done | bytes 139296 | tf_op jit(solution)/shard_map/ppermute | solution.py:492
  25.6 7.3 %collective-permute-start.11 = (bf16[272,256]{1,0:T(8,128)(2,1)S(1)}, bf16[272,256]{1,0:T(8,128)(2,1)S(1)}, u32[]{:S(2)}, u32[]{:S(2)}) collective-permute-start(bf16[272,256]{1,0:T(8,128)(2,1)S(1)} %collective-permute-done.10.refs_16_), channel_id=1, source_target_pairs={{416,384},{448,416},{480,448},{0,480},{32,0},{64,32},{96,64},{417,... | collective-permute-start | bytes 417800 | tf_op jit(solution)/shard_map/ppermute | solution.py:492
  33.0 0.7 collective-permute-start.6
  33.7 3.2 %collective-permute-start = (bf16[528,128]{1,0:T(8,128)(2,1)S(1)}, bf16[528,128]{1,0:T(8,128)(2,1)S(1)}, u32[]{:S(2)}, u32[]{:S(2)}) collective-permute-start(bf16[528,128]{1,0:T(8,128)(2,1)S(1)} %pad_maximum_fusion.1.own_ref.refs_0_), channel_id=1, source_target_pairs={{0,8},{8,0},{16,24},{24,16},{1,9},{9,1},{17,25},{25,17},{2,10},{10... | collective-permute-start | bytes 405512 | tf_op jit(solution)/shard_map/ppermute | solution.py:498
  36.9 4.7 %collective-permute-start.12 = (bf16[272,256]{1,0:T(8,128)(2,1)S(1)}, bf16[272,256]{1,0:T(8,128)(2,1)S(1)}, u32[]{:S(2)}, u32[]{:S(2)}) collective-permute-start(bf16[272,256]{1,0:T(8,128)(2,1)S(1)} %collective-permute-done.11.refs_15_), channel_id=1, source_target_pairs={{384,352},{416,384},{448,416},{480,448},{0,480},{32,0},{64,32},{38... | collective-permute-start | bytes 417800 | tf_op jit(solution)/shard_map/ppermute | solution.py:492
  41.6 0.7 collective-permute-start.7
  42.4 4.5 %collective-permute-start.1 = (bf16[1056,128]{1,0:T(8,128)(2,1)S(1)}, bf16[1056,128]{1,0:T(8,128)(2,1)S(1)}, u32[]{:S(2)}, u32[]{:S(2)}) collective-permute-start(bf16[1056,128]{1,0:T(8,128)(2,1)S(1)} %pad_maximum_fusion), channel_id=1, source_target_pairs={{0,16},{8,24},{16,0},{24,8},{1,17},{9,25},{17,1},{25,9},{2,18},{10... | collective-permute-start | bytes 811016 | tf_op jit(solution)/shard_map/ppermute | solution.py:500
  46.9 4.6 %collective-permute-start.15 = (bf16[272,256]{1,0:T(8,128)(2,1)S(1)}, bf16[272,256]{1,0:T(8,128)(2,1)S(1)}, u32[]{:S(2)}, u32[]{:S(2)}) collective-permute-start(bf16[272,256]{1,0:T(8,128)(2,1)S(1)} %copy-done.2), channel_id=1, source_target_pairs={{0,480},{32,0},{64,32},{96,64},{128,96},{160,128},{192,160},{1,481... | collective-permute-start | bytes 417800 | tf_op jit(solution)/shard_map/ppermute | solution.py:492
  51.5 1.3 %collective-permute-start.2 = (bf16[272,256]{1,0:T(8,128)(2,1)S(1)}, bf16[272,256]{1,0:T(8,128)(2,1)S(1)}, u32[]{:S(2)}, u32[]{:S(2)}) collective-permute-start(bf16[272,256]{1,0:T(8,128)(2,1)S(1)} %copy-done.2), channel_id=1, source_target_pairs={{0,32},{32,64},{64,96},{96,128},{128,160},{160,192},{192,224},{224... | collective-permute-start | bytes 417800 | tf_op jit(solution)/shard_map/ppermute | solution.py:485
  52.8 1.9 %collective-permute-start.13 = (bf16[272,256]{1,0:T(8,128)(2,1)S(1)}, bf16[272,256]{1,0:T(8,128)(2,1)S(1)}, u32[]{:S(2)}, u32[]{:S(2)}) collective-permute-start(bf16[272,256]{1,0:T(8,128)(2,1)S(1)} %collective-permute-done.12.refs_14_), channel_id=1, source_target_pairs={{352,320},{384,352},{416,384},{448,416},{480,448},{0,480},{32,0},{... | collective-permute-start | bytes 417800 | tf_op jit(solution)/shard_map/ppermute | solution.py:492
  54.8 0.7 collective-permute-start.8
  55.5 4.0 %collective-permute-start.16 = (bf16[272,256]{1,0:T(8,128)(2,1)S(1)}, bf16[272,256]{1,0:T(8,128)(2,1)S(1)}, u32[]{:S(2)}, u32[]{:S(2)}) collective-permute-start(bf16[272,256]{1,0:T(8,128)(2,1)S(1)} %collective-permute-done.15.refs_18_), channel_id=1, source_target_pairs={{480,448},{0,480},{32,0},{64,32},{96,64},{128,96},{160,128},{481,4... | collective-permute-start | bytes 417800 | tf_op jit(solution)/shard_map/ppermute | solution.py:492
  59.5 0.7 collective-permute-start.3
  60.2 5.5 %collective-permute-start.14 = (bf16[272,256]{1,0:T(8,128)(2,1)S(1)}, bf16[272,256]{1,0:T(8,128)(2,1)S(1)}, u32[]{:S(2)}, u32[]{:S(2)}) collective-permute-start(bf16[272,256]{1,0:T(8,128)(2,1)S(1)} %collective-permute-done.13.refs_13_), channel_id=1, source_target_pairs={{320,288},{352,320},{384,352},{416,384},{448,416},{480,448},{0,480... | collective-permute-start | bytes 417800 | tf_op jit(solution)/shard_map/ppermute | solution.py:492
  65.7 0.7 collective-permute-start.9
  66.4 6.1 %collective-permute-start.17 = (bf16[256,2048]{1,0:T(8,128)(2,1)S(1)}, bf16[256,2048]{1,0:T(8,128)(2,1)}, u32[]{:S(2)}, u32[]{:S(2)}) collective-permute-start(bf16[256,2048]{1,0:T(8,128)(2,1)S(1)} %copy-done.1), channel_id=1, source_target_pairs={{0,1},{1,0},{2,3},{3,2},{4,5},{5,4},{6,7},{7,6},{8,9},{9,8},{10,11... | collective-permute-start | bytes 3145736 | tf_op jit(solution)/shard_map/ppermute | solution.py:501
  72.5 1.4 %lists.1 = (s32[8,128]{1,0:T(8,128)S(1)}, s32[16,128]{1,0:T(8,128)S(1)}, f32[16,128]{1,0:T(8,128)S(1)}) custom-call(s32[4]{0:T(128)S(1)} %copy-done.4, bf16[528,128]{1,0:T(8,128)(2,1)S(1)} %pad_maximum_fusion.1.own_ref.refs_0_, bf16[528,128]{1,0:T(8,128)(2,1)S(1)} %collective-permute-done.side_ref.refs_1_, ...), custom_call_target="tpu_custom_call" | custom-call | tf_op jit(solution)/shard_map/lists/pallas_call | solution.py:434
  73.9 6.9 %attend.1 = bf16[8,272,256]{2,1,0:T(8,128)(2,1)} custom-call(s32[8,128]{1,0:T(8,128)S(1)} %get-tuple-element.7.meta_ref, s32[16,128]{1,0:T(8,128)S(1)} %get-tuple-element.8.ids_ref, f32[16,128]{1,0:T(8,128)S(1)} %get-tuple-element.9.bias_ref, bf16[528,128]{1,0:T(8,128)(2,1)S(1)} %pad_maximum_fusion.1.own_ref.refs_0_, ...), custom_call_target="tpu_custom_call" | custom-call | tf_op jit(solution)/shard_map/attend/pallas_call | solution.py:295
  80.9 3.5 %all-to-all-start = ((bf16[8,272,256]{2,1,0:T(8,128)(2,1)}), bf16[8,272,256]{2,1,0:T(8,128)(2,1)S(1)}, u32[]{:S(2)}, u32[]{:S(2)}) async-start(bf16[8,272,256]{2,1,0:T(8,128)(2,1)} %attend.1), calls=%async_computation | async-start | bytes 2228224 | tf_op jit(solution)/shard_map/all_to_all | solution.py:513
  84.4 1.1 constant_dynamic-slice_fusion.1
  85.5 1.1 fusion.2
  86.6 0.1 copy.24.gate_ref
  86.7 13.3 %all-to-all-done.got_ref = bf16[8,272,256]{2,1,0:T(8,128)(2,1)S(1)} async-done(((bf16[8,272,256]{2,1,0:T(8,128)(2,1)}), bf16[8,272,256]{2,1,0:T(8,128)(2,1)S(1)}, u32[]{:S(2)}, u32[]{:S(2)}) %all-to-all-start) | async-done | bytes 1114144 | tf_op jit(solution)/shard_map/all_to_all | solution.py:513
  100.1 2.8 %merge.1 = (bf16[128,2048]{1,0:T(8,128)(2,1)S(1)}, f32[2,2,256]{2,1,0:T(2,128)S(1)}) custom-call(s32[1]{0:T(128)} %bitcast.1.meta_ref, bf16[8,272,256]{2,1,0:T(8,128)(2,1)S(1)} %all-to-all-done.got_ref, f32[128,8]{1,0:T(8,128)S(1)} %copy.24.gate_ref, bf16[256,2048]{1,0:T(8,128)(2,1)S(1)} %copy-done.1, bf16[256,2048]{1,0:T(8,128)(2,1)} %collective-permute-done.17.other_ref), custom_call_target="tpu_custom_call" | custom-call | tf_op jit(solution)/shard_map/merge/pallas_call | solution.py:363
  102.9 0.8 copy-done.3
  103.6 4.0 %all-to-all-start.1 = ((bf16[4,32,2048]{2,1,0:T(8,128)(2,1)}), bf16[4,32,2048]{2,1,0:T(8,128)(2,1)S(1)}, u32[]{:S(2)}, u32[]{:S(2)}) async-start(bf16[4,32,2048]{2,1,0:T(8,128)(2,1)} %bitcast.34), calls=%async_computation.1 | async-start | bytes 1048576 | tf_op jit(solution)/shard_map/all_to_all | solution.py:519
  107.7 0.1 reshape.51
  107.8 0.7 reshape.52
  108.4 7.3 %all-to-all-done.1 = bf16[4,32,2048]{2,1,0:T(8,128)(2,1)S(1)} async-done(((bf16[4,32,2048]{2,1,0:T(8,128)(2,1)}), bf16[4,32,2048]{2,1,0:T(8,128)(2,1)S(1)}, u32[]{:S(2)}, u32[]{:S(2)}) %all-to-all-start.1) | async-done | bytes 524320 | tf_op jit(solution)/shard_map/all_to_all | solution.py:519
  115.7 0.7 reduce_sum.12
  (36 shorter events, 0.2 us)
Async XLA Ops:
  0.6 18.3 %copy-start = (bf16[2048,256]{1,0:T(8,128)(2,1)S(1)}, bf16[2048,256]{1,0:T(8,128)(2,1)}, u32[]{:S(2)}) copy-start(bf16[2048,256]{1,0:T(8,128)(2,1)} %param.16) | copy-start | bytes 3145732
  1.3 17.7 %copy-start.5 = (bf16[256,2048]{1,0:T(8,128)(2,1)S(1)}, bf16[256,2048]{1,0:T(8,128)(2,1)}, u32[]{:S(2)}) copy-start(bf16[256,2048]{1,0:T(8,128)(2,1)} %tok_ref.1) | copy-start | bytes 3145732
  4.8 15.5 %collective-permute-start.4 = (bf16[272,256]{1,0:T(8,128)(2,1)}, bf16[272,256]{1,0:T(8,128)(2,1)S(1)}, u32[]{:S(2)}, u32[]{:S(2)}) collective-permute-start(bf16[272,256]{1,0:T(8,128)(2,1)} %project.1.refs_3_), channel_id=1, source_target_pairs={{0,96},{32,128},{64,160},{96,192},{128,224},{160,256},{192,288},{2... | collective-permute-start | bytes 417800 | tf_op jit(solution)/shard_map/ppermute | solution.py:485
  11.9 13.7 %collective-permute-start.10 = (bf16[272,256]{1,0:T(8,128)(2,1)}, bf16[272,256]{1,0:T(8,128)(2,1)S(1)}, u32[]{:S(2)}, u32[]{:S(2)}) collective-permute-start(bf16[272,256]{1,0:T(8,128)(2,1)} %project.1.refs_3_), channel_id=1, source_target_pairs={{0,416},{32,448},{64,480},{96,0},{128,32},{160,64},{192,96},{1,417... | collective-permute-start | bytes 417800 | tf_op jit(solution)/shard_map/ppermute | solution.py:492
  19.0 1.3 %copy-start.6 = (f32[256,64]{0,1:T(8,128)S(1)}, f32[256,64]{0,1:T(8,128)}, u32[]{:S(2)}) copy-start(f32[256,64]{0,1:T(8,128)} %constant.53.clone) | copy-start | bytes 196612
  19.0 1.3 %copy-start.7 = (f32[256,64]{0,1:T(8,128)S(1)}, f32[256,64]{0,1:T(8,128)}, u32[]{:S(2)}) copy-start(f32[256,64]{0,1:T(8,128)} %constant.54.clone) | copy-start | bytes 196612
  19.5 2.2 %copy-start.8 = (s32[4,32]{1,0:T(4,128)S(1)}, s32[4,32]{1,0:T(4,128)}, u32[]{:S(2)}) copy-start(s32[4,32]{1,0:T(4,128)} %param.23) | copy-start | bytes 1540
  20.4 12.6 %collective-permute-start.5 = (bf16[272,256]{1,0:T(8,128)(2,1)S(1)}, bf16[272,256]{1,0:T(8,128)(2,1)S(1)}, u32[]{:S(2)}, u32[]{:S(2)}) collective-permute-start(bf16[272,256]{1,0:T(8,128)(2,1)S(1)} %collective-permute-done.4.refs_6_), channel_id=1, source_target_pairs={{96,128},{128,160},{160,192},{192,224},{224,256},{256,288},{288,32... | collective-permute-start | bytes 417800 | tf_op jit(solution)/shard_map/ppermute | solution.py:485
  21.1 25.8 %copy-start.2 = (bf16[272,256]{1,0:T(8,128)(2,1)S(1)}, bf16[272,256]{1,0:T(8,128)(2,1)}, u32[]{:S(2)}) copy-start(bf16[272,256]{1,0:T(8,128)(2,1)} %project.1.refs_3_) | copy-start | bytes 417796
  21.1 45.3 %copy-start.1 = (bf16[256,2048]{1,0:T(8,128)(2,1)S(1)}, bf16[256,2048]{1,0:T(8,128)(2,1)}, u32[]{:S(2)}) copy-start(bf16[256,2048]{1,0:T(8,128)(2,1)} %own_ref.1) | copy-start | bytes 3145732
  21.1 51.4 %copy-start.4 = (s32[4]{0:T(128)S(1)}, s32[4]{0:T(128)}, u32[]{:S(2)}) copy-start(s32[4]{0:T(128)} %pad_add_fusion.place_ref.meta_ref) | copy-start | bytes 52
  25.6 11.3 %collective-permute-start.11 = (bf16[272,256]{1,0:T(8,128)(2,1)S(1)}, bf16[272,256]{1,0:T(8,128)(2,1)S(1)}, u32[]{:S(2)}, u32[]{:S(2)}) collective-permute-start(bf16[272,256]{1,0:T(8,128)(2,1)S(1)} %collective-permute-done.10.refs_16_), channel_id=1, source_target_pairs={{416,384},{448,416},{480,448},{0,480},{32,0},{64,32},{96,64},{417,... | collective-permute-start | bytes 417800 | tf_op jit(solution)/shard_map/ppermute | solution.py:492
  33.0 8.7 %collective-permute-start.6 = (bf16[272,256]{1,0:T(8,128)(2,1)S(1)}, bf16[272,256]{1,0:T(8,128)(2,1)S(1)}, u32[]{:S(2)}, u32[]{:S(2)}) collective-permute-start(bf16[272,256]{1,0:T(8,128)(2,1)S(1)} %collective-permute-done.5.refs_7_), channel_id=1, source_target_pairs={{128,160},{160,192},{192,224},{224,256},{256,288},{288,320},{320,3... | collective-permute-start | bytes 417800 | tf_op jit(solution)/shard_map/ppermute | solution.py:485
  33.7 8.7 %collective-permute-start = (bf16[528,128]{1,0:T(8,128)(2,1)S(1)}, bf16[528,128]{1,0:T(8,128)(2,1)S(1)}, u32[]{:S(2)}, u32[]{:S(2)}) collective-permute-start(bf16[528,128]{1,0:T(8,128)(2,1)S(1)} %pad_maximum_fusion.1.own_ref.refs_0_), channel_id=1, source_target_pairs={{0,8},{8,0},{16,24},{24,16},{1,9},{9,1},{17,25},{25,17},{2,10},{10... | collective-permute-start | bytes 405512 | tf_op jit(solution)/shard_map/ppermute | solution.py:498
  36.9 15.9 %collective-permute-start.12 = (bf16[272,256]{1,0:T(8,128)(2,1)S(1)}, bf16[272,256]{1,0:T(8,128)(2,1)S(1)}, u32[]{:S(2)}, u32[]{:S(2)}) collective-permute-start(bf16[272,256]{1,0:T(8,128)(2,1)S(1)} %collective-permute-done.11.refs_15_), channel_id=1, source_target_pairs={{384,352},{416,384},{448,416},{480,448},{0,480},{32,0},{64,32},{38... | collective-permute-start | bytes 417800 | tf_op jit(solution)/shard_map/ppermute | solution.py:492
  41.6 13.1 %collective-permute-start.7 = (bf16[272,256]{1,0:T(8,128)(2,1)S(1)}, bf16[272,256]{1,0:T(8,128)(2,1)S(1)}, u32[]{:S(2)}, u32[]{:S(2)}) collective-permute-start(bf16[272,256]{1,0:T(8,128)(2,1)S(1)} %collective-permute-done.6.refs_8_), channel_id=1, source_target_pairs={{160,192},{192,224},{224,256},{256,288},{288,320},{320,352},{352,3... | collective-permute-start | bytes 417800 | tf_op jit(solution)/shard_map/ppermute | solution.py:485
  42.4 24.1 %collective-permute-start.1 = (bf16[1056,128]{1,0:T(8,128)(2,1)S(1)}, bf16[1056,128]{1,0:T(8,128)(2,1)S(1)}, u32[]{:S(2)}, u32[]{:S(2)}) collective-permute-start(bf16[1056,128]{1,0:T(8,128)(2,1)S(1)} %pad_maximum_fusion), channel_id=1, source_target_pairs={{0,16},{8,24},{16,0},{24,8},{1,17},{9,25},{17,1},{25,9},{2,18},{10... | collective-permute-start | bytes 811016 | tf_op jit(solution)/shard_map/ppermute | solution.py:500
  46.9 8.6 %collective-permute-start.15 = (bf16[272,256]{1,0:T(8,128)(2,1)S(1)}, bf16[272,256]{1,0:T(8,128)(2,1)S(1)}, u32[]{:S(2)}, u32[]{:S(2)}) collective-permute-start(bf16[272,256]{1,0:T(8,128)(2,1)S(1)} %copy-done.2), channel_id=1, source_target_pairs={{0,480},{32,0},{64,32},{96,64},{128,96},{160,128},{192,160},{1,481... | collective-permute-start | bytes 417800 | tf_op jit(solution)/shard_map/ppermute | solution.py:492
  51.5 8.0 %collective-permute-start.2 = (bf16[272,256]{1,0:T(8,128)(2,1)S(1)}, bf16[272,256]{1,0:T(8,128)(2,1)S(1)}, u32[]{:S(2)}, u32[]{:S(2)}) collective-permute-start(bf16[272,256]{1,0:T(8,128)(2,1)S(1)} %copy-done.2), channel_id=1, source_target_pairs={{0,32},{32,64},{64,96},{96,128},{128,160},{160,192},{192,224},{224... | collective-permute-start | bytes 417800 | tf_op jit(solution)/shard_map/ppermute | solution.py:485
  52.8 7.3 %collective-permute-start.13 = (bf16[272,256]{1,0:T(8,128)(2,1)S(1)}, bf16[272,256]{1,0:T(8,128)(2,1)S(1)}, u32[]{:S(2)}, u32[]{:S(2)}) collective-permute-start(bf16[272,256]{1,0:T(8,128)(2,1)S(1)} %collective-permute-done.12.refs_14_), channel_id=1, source_target_pairs={{352,320},{384,352},{416,384},{448,416},{480,448},{0,480},{32,0},{... | collective-permute-start | bytes 417800 | tf_op jit(solution)/shard_map/ppermute | solution.py:492
  54.8 11.0 %collective-permute-start.8 = (bf16[272,256]{1,0:T(8,128)(2,1)S(1)}, bf16[272,256]{1,0:T(8,128)(2,1)S(1)}, u32[]{:S(2)}, u32[]{:S(2)}) collective-permute-start(bf16[272,256]{1,0:T(8,128)(2,1)S(1)} %collective-permute-done.7.refs_9_), channel_id=1, source_target_pairs={{192,224},{224,256},{256,288},{288,320},{320,352},{352,384},{384,4... | collective-permute-start | bytes 417800 | tf_op jit(solution)/shard_map/ppermute | solution.py:485
  55.5 18.4 %collective-permute-start.16 = (bf16[272,256]{1,0:T(8,128)(2,1)S(1)}, bf16[272,256]{1,0:T(8,128)(2,1)S(1)}, u32[]{:S(2)}, u32[]{:S(2)}) collective-permute-start(bf16[272,256]{1,0:T(8,128)(2,1)S(1)} %collective-permute-done.15.refs_18_), channel_id=1, source_target_pairs={{480,448},{0,480},{32,0},{64,32},{96,64},{128,96},{160,128},{481,4... | collective-permute-start | bytes 417800 | tf_op jit(solution)/shard_map/ppermute | solution.py:492
  59.5 14.4 %collective-permute-start.3 = (bf16[272,256]{1,0:T(8,128)(2,1)S(1)}, bf16[272,256]{1,0:T(8,128)(2,1)S(1)}, u32[]{:S(2)}, u32[]{:S(2)}) collective-permute-start(bf16[272,256]{1,0:T(8,128)(2,1)S(1)} %collective-permute-done.2.refs_4_), channel_id=1, source_target_pairs={{32,64},{64,96},{96,128},{128,160},{160,192},{192,224},{224,256},{... | collective-permute-start | bytes 417800 | tf_op jit(solution)/shard_map/ppermute | solution.py:485
  60.2 13.8 %collective-permute-start.14 = (bf16[272,256]{1,0:T(8,128)(2,1)S(1)}, bf16[272,256]{1,0:T(8,128)(2,1)S(1)}, u32[]{:S(2)}, u32[]{:S(2)}) collective-permute-start(bf16[272,256]{1,0:T(8,128)(2,1)S(1)} %collective-permute-done.13.refs_13_), channel_id=1, source_target_pairs={{320,288},{352,320},{384,352},{416,384},{448,416},{480,448},{0,480... | collective-permute-start | bytes 417800 | tf_op jit(solution)/shard_map/ppermute | solution.py:492
  65.7 8.2 %collective-permute-start.9 = (bf16[272,256]{1,0:T(8,128)(2,1)S(1)}, bf16[272,256]{1,0:T(8,128)(2,1)S(1)}, u32[]{:S(2)}, u32[]{:S(2)}) collective-permute-start(bf16[272,256]{1,0:T(8,128)(2,1)S(1)} %collective-permute-done.8.refs_10_), channel_id=1, source_target_pairs={{224,256},{256,288},{288,320},{320,352},{352,384},{384,416},{416,4... | collective-permute-start | bytes 417800 | tf_op jit(solution)/shard_map/ppermute | solution.py:485
  66.4 20.3 %collective-permute-start.17 = (bf16[256,2048]{1,0:T(8,128)(2,1)S(1)}, bf16[256,2048]{1,0:T(8,128)(2,1)}, u32[]{:S(2)}, u32[]{:S(2)}) collective-permute-start(bf16[256,2048]{1,0:T(8,128)(2,1)S(1)} %copy-done.1), channel_id=1, source_target_pairs={{0,1},{1,0},{2,3},{3,2},{4,5},{5,4},{6,7},{7,6},{8,9},{9,8},{10,11... | collective-permute-start | bytes 3145736 | tf_op jit(solution)/shard_map/ppermute | solution.py:501
  80.9 19.2 %all-to-all-start = ((bf16[8,272,256]{2,1,0:T(8,128)(2,1)}), bf16[8,272,256]{2,1,0:T(8,128)(2,1)S(1)}, u32[]{:S(2)}, u32[]{:S(2)}) async-start(bf16[8,272,256]{2,1,0:T(8,128)(2,1)} %attend.1), calls=%async_computation | async-start | bytes 2228224 | tf_op jit(solution)/shard_map/all_to_all | solution.py:513
  102.8 0.8 copy-start.3
  103.6 12.1 %all-to-all-start.1 = ((bf16[4,32,2048]{2,1,0:T(8,128)(2,1)}), bf16[4,32,2048]{2,1,0:T(8,128)(2,1)S(1)}, u32[]{:S(2)}, u32[]{:S(2)}) async-start(bf16[4,32,2048]{2,1,0:T(8,128)(2,1)} %bitcast.34), calls=%async_computation.1 | async-start | bytes 1048576 | tf_op jit(solution)/shard_map/all_to_all | solution.py:519
